TPU v7x, 256 devices: a whole 4x4x8 slice. The times are simulated.
256 devices in a mesh: gr: 2 (over z_hi), fs: 16 (over z_lo, y), tp: 8 (over x, core).
Axes of the slice: x: 4, y: 4, z: 8 (z_hi: 2, z_lo: 4; z = z_hi * 4 + z_lo), core: 2. Of those that a mesh axis runs over, the one named last changes fastest.
Arguments:
- tokens: bfloat16 [8192, 2048], P(('gr', 'tp'), 'fs'), may hold values from -6 to 6
- routes: int32 [8192, 2], P(('gr', 'tp')), may hold values from 0 to 7, all different within a row; in each aligned block of 512 rows (0 to 511, 512 to 1023, ...) at most 192 rows name the same one
- route_weight: float32 [8192, 2], P(('gr', 'tp')), may hold values from 0.25 to 1
- norm_gain: float32 [2048], P(('gr', 'fs')), may hold values from 0.1 to 1.9
- gate_master: float32 [8, 2048, 2816], P(None, ('gr', 'fs'), 'tp'), may hold values from -0.125 to 0.125
- up_master: float32 [8, 2048, 2816], P(None, ('gr', 'fs'), 'tp'), may hold values from -0.125 to 0.125
- down_master: float32 [8, 2048, 2816], P(None, ('gr', 'fs'), 'tp'), may hold values from -0.109375 to 0.109375
Outputs:
- mixed_output: bfloat16 [8192, 2048], P(('gr', 'tp'), 'fs')
- gate_serving: bfloat16 [8, 2048, 2816], P('tp', None, 'fs')
- up_serving: bfloat16 [8, 2048, 2816], P('tp', None, 'fs')
- down_serving: bfloat16 [8, 2048, 2816], P('tp', None, 'fs')
Inputs may be any that keep to these rules, and one draw needn't show every extreme that they name: `routes`: each row names two different experts. Within the rows of one block of 512 tokens (one index of gr+tp) no expert is named by more than 192 rows, and in some blocks one expert is named by exactly 192.
All inputs are finite; a program needn't handle non-finite values.
Results may differ from a plain program's by a relative error of at most 0.0082.
Values may be sent and summed in bfloat16 or wider, within the bound.
No kernel may reach another device: no remote copies, remote signals or barrier semaphores. Data moves between devices by JAX's collectives and lax.ppermute only.
A program may use at most 128 MiB of HBM per device.

v0:
```python
import jax
import jax.numpy as jnp
from jax import lax
from jax.experimental import pallas as pl
from jax.experimental.pallas import tpu as pltpu
from jax.sharding import PartitionSpec as P


norm_eps = 1e-06
BF = jnp.bfloat16
F32 = jnp.float32
CAP, TOK, D, F = 192, 512, 2048, 176
MAIN, REM = 128, 48
PACK_GU, PACK_D = 176, 96
PACK = PACK_GU + PACK_D
TRIPS = ((4, 5, 3, 7), (0, 1, 2, 6))
ROWS = CAP * 8
HALF = CAP * 4


def spec_vmem():
    return pl.BlockSpec(memory_space=pltpu.VMEM)


def call(body, outs, args, scratch=(), after=(), in_hbm=0):
    n, m = len(args), len(after)

    def run(*refs):
        body(*refs[:n], *refs[n + m :])

    return pl.pallas_call(
        run,
        out_shape=outs,
        in_specs=[pl.BlockSpec(memory_space=pltpu.SMEM)]
        + [spec_vmem()] * (n - 1 - in_hbm)
        + [pl.BlockSpec(memory_space=pltpu.HBM)] * in_hbm
        + [pl.BlockSpec(memory_space=pl.ANY)] * m,
        out_specs=jax.tree.map(lambda _: spec_vmem(), outs),
        scratch_shapes=list(scratch),
        compiler_params=pltpu.CompilerParams(vmem_limit_bytes=48 * 2**20),
    )(*args, *after)


def sds(*shape, dtype=BF):
    return jax.ShapeDtypeStruct(shape, dtype)


def peer(where, r):
    return ((where[0] + r // 2) % 4) * 2 + (where[1] + r % 2) % 2


def pack_body(where, gain, gate_hbm, up_hbm, down_hbm, *refs):
    outs, (gate, up, down, sems) = refs[:4], refs[4:]
    copies = [
        pltpu.make_async_copy(src, dst, sems.at[i])
        for i, (src, dst) in enumerate(((gate_hbm, gate), (up_hbm, up), (down_hbm, down)))
    ]
    for copy in copies:
        copy.start()
    g = gain[...]
    for copy in copies:
        copy.wait()
    for r in range(8):
        e = peer(where, r)
        for top, mats in ((0, (gate[e] * g, up[e] * g)), (PACK_GU, (down[e],))):
            for h in range(2):
                pieces = []
                for m, mat in enumerate(mats):
                    at = top + 64 * m
                    outs[r // 2][r % 2, h, at : at + 64, :] = mat[:, h * F : h * F + MAIN].astype(BF)
                    rest = mat[:, h * F + MAIN : (h + 1) * F]
                    pieces += [rest[16 * i : 16 * i + 16] for i in range(4)]
                if len(mats) == 1:
                    pieces.append(jnp.zeros((16, 64), F32))
                row = jnp.concatenate(pieces, axis=1).astype(BF)
                for i in range(row.shape[1] // 128):
                    at = top + 64 * len(mats) + 16 * i
                    outs[r // 2][r % 2, h, at : at + 16, :] = row[:, 128 * i : 128 * i + 128]


def swap_body(where, *refs):
    for dx in range(4):
        refs[4][dx] = refs[dx][1]


def by_y_body(where, *refs):
    got, swapped, outs, held = refs[:4], refs[4], refs[5:9], refs[9]
    for dx in range(4):
        held[2 * dx] = got[dx][0]
        held[2 * dx + 1] = swapped[dx]
    x, c, z, y = where[0], where[1], where[2], where[3]
    for dy in range(4):
        to_y = (y + dy) % 4
        for k in range(4):
            dx = (x + 8 - z - k) % 4
            r = dx * 2 + (c + to_y // 2) % 2
            outs[dy][k] = held[r, to_y % 2]


def by_z_body(where, *refs):
    got, out = refs[:4], refs[4]
    for z8 in range(8):
        k = (z8 + 4 - where[2]) % 4
        for j in range(4):
            out[z8, j] = got[j][k]


def unpack_body(where, got, *outs):
    z, y = where[2], where[3]

    @pl.loop(0, 8)
    def _(z8):
        for j in range(4):
            block = z8 * 4 + (y + 4 - j) % 4
            at = pl.multiple_of(block * 64, 64)
            part = block // 2
            near = ((part // 4 + 4 - z) % 4) * 128 + (block % 2) * 64
            near = pl.multiple_of(near, 64)
            q = (part % 4 + 4 - y) % 4
            for top, mats in ((0, (0, 1)), (PACK_GU, (2,))):
                first = top + 64 * len(mats)
                row = jnp.concatenate(
                    [
                        got[z8, j, first + 16 * i : first + 16 * i + 16, :].astype(F32)
                        for i in range(3 if len(mats) == 2 else 2)
                    ],
                    axis=1,
                )
                for i, m in enumerate(mats):
                    main = got[z8, j, top + 64 * i : top + 64 * i + 64, :]
                    rest = jnp.concatenate(
                        [row[:, REM * p : REM * p + REM] for p in range(4 * i, 4 * i + 4)], axis=0
                    ).astype(BF)
                    outs[m][0, pl.ds(at, 64), 0:MAIN] = main
                    outs[m][0, pl.ds(at, 64), MAIN:F] = rest
                    outs[3 + m][q, pl.ds(near, 64), 0:MAIN] = main
                    outs[3 + m][q, pl.ds(near, 64), MAIN:F] = rest


def dispatch_body(where, routes, *refs):
    toks, outs, table, made = refs[:4], refs[4:8], refs[8], refs[9]
    r0, r1 = routes[0:1, :], routes[1:2, :]
    expert = lax.broadcasted_iota(jnp.int32, (8, TOK), 0)
    named = (r0 == expert) | (r1 == expert)
    before = (
        lax.broadcasted_iota(jnp.int32, (TOK, TOK), 0)
        < lax.broadcasted_iota(jnp.int32, (TOK, TOK), 1)
    ).astype(F32).astype(BF)
    count = jnp.dot(named.astype(F32).astype(BF), before, preferred_element_type=F32)
    table[...] = jnp.where(named, count, -1.0)
    x = jnp.concatenate([t[...] for t in toks], axis=1)
    slot = lax.broadcasted_iota(jnp.int32, (CAP, TOK), 0).astype(F32)

    @pl.loop(0, 8)
    def _(r):
        pick = (slot == table[pl.ds(peer(where, r), 1), :]).astype(F32).astype(BF)
        made[r] = jnp.dot(pick, x, preferred_element_type=F32).astype(BF)

    for r in range(8):
        outs[r // 2][r % 2] = made[r]


def rows_body(where, *refs):
    got, swapped, out = refs[:4], refs[4], refs[5]
    for i, r in enumerate(TRIPS[0] + TRIPS[1]):
        part = swapped[r // 2] if r % 2 else got[r // 2][0]
        out[CAP * i : CAP * i + CAP, :] = part


def ffn_body(where, *refs):
    xs, (wg, wu, wd), (own, plus, minus, keep) = refs[:4], refs[4:7], refs[7:]
    g = u = total = None
    for q in range(4):
        x = xs[q][...]
        xf = x.astype(F32)
        dg = jnp.dot(x, wg[q], preferred_element_type=F32)
        du = jnp.dot(x, wu[q], preferred_element_type=F32)
        s = xf * xf
        g, u, total = (dg, du, s) if g is None else (g + dg, u + du, total + s)
    scale = lax.rsqrt(jnp.sum(total, axis=1, keepdims=True) / D + norm_eps)
    g = g * scale
    u = u * scale
    hidden = (g / (1.0 + jnp.exp(-g)) * u).astype(BF)

    def out(q, half):
        w = wd[q, 256 * half : 256 * half + 256, :]
        return lax.dot_general(
            hidden, w, (((1,), (1,)), ((), ())), preferred_element_type=F32
        ).astype(BF)

    plus[:, 0:256] = out(2, 0)
    plus[:, 256:512] = out(1, 1)
    minus[:, 0:256] = out(3, 0)
    minus[:, 256:512] = out(2, 1)
    keep[:, 0:256] = out(1, 0)
    keep[:, 256:512] = out(3, 1)
    own[:, 0:256] = out(0, 0)
    own[:, 256:512] = out(0, 1)


def by_rows(body, where, tiled, whole, widths, n, block, after=()):
    tile = n // 2
    rows = lambda w, first=0: pl.BlockSpec((tile, w), lambda i: (i + first, 0))
    m = len(tiled) + len(whole) + 1

    def run(*refs):
        body(*refs[:m], *refs[m + len(after) :])

    return pl.pallas_call(
        run,
        grid=(2,),
        in_specs=[pl.BlockSpec(memory_space=pltpu.SMEM)]
        + [rows(a.shape[1], 2 * block) for a in tiled]
        + [pl.BlockSpec(a.shape, lambda i: (0, 0, 0)) for a in whole]
        + [pl.BlockSpec(memory_space=pl.ANY)] * len(after),
        out_specs=[rows(w) for w in widths],
        out_shape=[sds(n, w) for w in widths],
        compiler_params=pltpu.CompilerParams(vmem_limit_bytes=48 * 2**20),
    )(where, *tiled, *whole, *after)


def add_body(where, keep, from_left, from_right, out0, out1):
    out0[...] = (keep[:, 0:256].astype(F32) + from_left[:, 0:256].astype(F32)).astype(BF)
    out1[...] = (keep[:, 256:512].astype(F32) + from_right[:, 256:512].astype(F32)).astype(BF)


def sums_body(where, own, from_left, from_right, left, right, *outs):
    for i, out in enumerate(outs):
        at = slice(CAP * i, CAP * i + CAP)
        a = own[at, 0:256].astype(F32) + left[at, :].astype(F32)
        out[:, 0:256] = (a + from_right[at, 0:256].astype(F32)).astype(BF)
        b = own[at, 256:512].astype(F32) + right[at, :].astype(F32)
        out[:, 256:512] = (b + from_left[at, 256:512].astype(F32)).astype(BF)


def plan_body(where, routes, weight, out):
    r0, r1 = routes[:, 0:1], routes[:, 1:2]
    w0, w1 = weight[:, 0:1], weight[:, 1:2]
    expert = lax.broadcasted_iota(jnp.int32, (TOK, 128), 1)
    one0, one1 = (r0 == expert).astype(F32), (r1 == expert).astype(F32)
    before = (
        lax.broadcasted_iota(jnp.int32, (TOK, TOK), 1)
        < lax.broadcasted_iota(jnp.int32, (TOK, TOK), 0)
    ).astype(F32).astype(BF)
    count = jnp.dot(before, (one0 + one1).astype(BF), preferred_element_type=F32)
    slot0 = jnp.sum(one0 * count, axis=1, keepdims=True)
    slot1 = jnp.sum(one1 * count, axis=1, keepdims=True)
    table = jnp.zeros((TOK, 128), F32)
    for r in range(8):
        e = peer(where, r)
        at = jnp.where(r0 == e, slot0, jnp.where(r1 == e, slot1, -1.0))
        w = jnp.where(r0 == e, w0, jnp.where(r1 == e, w1, 0.0))
        table = jnp.where(expert == r, at, jnp.where(expert == 8 + r, w, table))
    out[...] = table


def combine_body(relative, plan, *refs):
    n = len(relative)
    got, outs = refs[:n], refs[n:]
    slot = lax.broadcasted_iota(jnp.int32, (TOK, CAP), 1).astype(F32)
    total = None
    if len(outs) == 5:
        total, outs = outs[0][...], outs[1:]
    for i, r in enumerate(relative):
        pick = (slot == plan[:, r : r + 1]).astype(F32).astype(BF)
        part = plan[:, 8 + r : 9 + r] * jnp.dot(pick, got[i][...], preferred_element_type=F32)
        total = part if total is None else total + part
    if len(outs) == 1:
        outs[0][...] = total
        return
    outs[0][...] = total[:, 0:128]
    for k in range(1, 4):
        outs[k][...] = total[:, 128 * k : 128 * k + 128].astype(BF)


def shift_tp(a, r, sign=1):
    dx, dc = sign * (r // 2), r % 2
    return lax.ppermute(
        a, "tp", [(2 * x + c, 2 * ((x + dx) % 4) + (c + dc) % 2) for x in range(4) for c in range(2)]
    )


def shift_fs(a, dz, dy):
    return lax.ppermute(
        a, "fs", [(4 * z + y, 4 * ((z + dz) % 4) + (y + dy) % 4) for z in range(4) for y in range(4)]
    )


def local(tokens, routes, route_weight, norm_gain, gate_master, up_master, down_master):
    tp, fs, gr = lax.axis_index("tp"), lax.axis_index("fs"), lax.axis_index("gr")
    where = jnp.stack([tp // 2, tp % 2, fs // 4, fs % 4, gr]).astype(jnp.int32)
    by_k = [tokens] * 4
    for k in (2, 1, 3):
        by_k[k] = shift_fs(tokens, -k, 0)
    packed = call(
        pack_body,
        [sds(2, 2, PACK, 128)] * 4,
        (where, norm_gain[:, None], gate_master, up_master, down_master),
        scratch=[pltpu.VMEM(gate_master.shape, F32)] * 3 + [pltpu.SemaphoreType.DMA((3,))],
        in_hbm=3,
    )

    def over_x(parts):
        out = list(parts)
        for dx in (2, 1, 3):
            out[dx] = shift_tp(parts[dx], 2 * dx)
        return out

    def swap(parts, after):
        shape = (4, *parts[0].shape[1:])
        mine = call(swap_body, [sds(*shape)], (where, *parts), after=after)[0]
        return mine, shift_tp(mine, 1)

    w_x = over_x(packed)
    slots = call(
        dispatch_body,
        [sds(2, CAP, 512)] * 4,
        (where, routes.T, *by_k),
        scratch=[pltpu.VMEM((8, TOK), F32), pltpu.VMEM((8, CAP, 512), BF)],
        after=(packed[0],),
    )
    t_x = over_x(slots)
    _, w_core = swap(w_x, (slots[0],))

    to_y = call(
        by_y_body,
        [sds(4, PACK, 128)] * 4,
        (where, *w_x, w_core),
        scratch=[pltpu.VMEM((8, 2, PACK, 128), BF)],
    )
    w_y = list(to_y)
    for dy in (2, 1, 3):
        w_y[dy] = shift_fs(to_y[dy], 0, dy)
    plan = call(
        plan_body, [sds(TOK, 128, dtype=F32)], (where, routes, route_weight), after=(to_y[0],)
    )[0]
    _, t_core = swap(t_x, (plan,))
    own = call(rows_body, [sds(ROWS, 512)], (where, *t_x, t_core))[0]
    two, plus, minus = shift_fs(own, 0, 2), shift_fs(own, 0, 1), shift_fs(own, 0, -1)
    rows = (own, minus, two, plus)
    to_z = call(by_z_body, [sds(8, 4, PACK, 128)], (where, *w_y), after=(own,))[0]
    w_z = lax.all_to_all(
        to_z,
        ("gr", "fs"),
        0,
        0,
        axis_index_groups=[[4 * z + y for z in range(8)] for y in range(4)],
        tiled=True,
    )
    gate_w, up_w, down_w, *ordered = call(
        unpack_body, [sds(1, D, F)] * 3 + [sds(4, 512, F)] * 3, (where, w_z)
    )
    made = []
    for t in range(2):
        last = [m[0] for m in made[-1:]]
        made.append(by_rows(ffn_body, where, rows, ordered, (512,) * 4, HALF, t, after=last))

    def out_y(t):
        return shift_fs(made[t][1], 0, 1), shift_fs(made[t][2], 0, -1)

    def sum_y(t, got, after):
        sums = call(add_body, [sds(HALF, 256)] * 2, (where, made[t][3], *got), after=after)
        return sums[0], (shift_fs(sums[0], 0, 1), shift_fs(sums[1], 0, -1))

    def home(t, got, ends, after):
        places = TRIPS[t]
        sums = call(
            sums_body, [sds(CAP, 512)] * len(places), (where, made[t][0], *got, *ends), after=after
        )
        return sums[0], [p if r == 0 else shift_tp(p, r, -1) for r, p in zip(places, sums)]

    def combine(t, parts, outs, after=()):
        return call(
            lambda where, plan, *refs: combine_body(TRIPS[t], plan, *refs),
            outs,
            (where, plan, *parts),
            after=after,
        )

    got = [out_y(t) for t in range(2)]
    add0, ends0 = sum_y(0, got[0], (made[1][0],))
    add1, ends1 = sum_y(1, got[1], (add0,))
    sums0, home0 = home(0, got[0], ends0, (add1,))
    sums1, home1 = home(1, got[1], ends1, (sums0,))
    part = combine(0, home0, [sds(TOK, 512, dtype=F32)], (sums1,))
    mixed = combine(1, (*home1, *part), [sds(TOK, 128, dtype=F32)] + [sds(TOK, 128)] * 3)
    out = mixed[0]
    for k in (2, 1, 3):
        got = shift_fs(mixed[k], k, 0)
        out = out + got.astype(F32)
    return (out.astype(BF), gate_w, up_w, down_w)


def solution(mesh):
    placed = (
        P(("gr", "tp"), "fs"),
        P(("gr", "tp"), None),
        P(("gr", "tp"), None),
        P(("gr", "fs")),
        P(None, ("gr", "fs"), "tp"),
        P(None, ("gr", "fs"), "tp"),
        P(None, ("gr", "fs"), "tp"),
    )

    return jax.shard_map(
        local,
        mesh=mesh,
        in_specs=placed,
        out_specs=(
            P(("gr", "tp"), "fs"),
            P("tp", None, "fs"),
            P("tp", None, "fs"),
            P("tp", None, "fs"),
        ),
        check_vma=False,
    )
```

profile of v0, /device:TPU:1, one launch (start us, length us, event | category | flops | bytes accessed | tf_op | source)
XLA Modules:
  0.0 241.1 jit_solution(15161798478995599084)
XLA Ops:
  6.2 2.1 collective-permute-start
  8.3 2.5 %collective-permute-start.1 = (bf16[2,2,272,128]{3,2,1,0:T(8,128)(2,1)S(1)}, bf16[2,2,272,128]{3,2,1,0:T(8,128)(2,1)S(1)}, u32[]{:S(2)}, u32[]{:S(2)}) collective-permute-start(bf16[2,2,272,128]{3,2,1,0:T(8,128)(2,1)S(1)} %get-tuple-element.48), channel_id=1, source_target_pairs={{0,4},{1,5},{2,6},{3,7},{4,0},{5,1},{6,2},{7,3},{8,12},{9,13},{10,... | collective-permute-start | bytes 835592 | tf_op jit(solution)/shard_map/ppermute | solution.py:278
  11.9 3.0 %collective-permute-start.4 = (bf16[512,128]{1,0:T(8,128)(2,1)S(1)}, bf16[512,128]{1,0:T(8,128)(2,1)S(1)}, u32[]{:S(2)}, u32[]{:S(2)}) collective-permute-start(bf16[512,128]{1,0:T(8,128)(2,1)S(1)} %copy-done.9), channel_id=1, source_target_pairs={{0,64},{8,72},{16,80},{24,88},{32,96},{40,104},{48,112},{56,120},{... | collective-permute-start | bytes 393224 | tf_op jit(solution)/shard_map/ppermute | solution.py:284
  17.3 7.7 %collective-permute-start.5 = (bf16[512,128]{1,0:T(8,128)(2,1)S(1)}, bf16[512,128]{1,0:T(8,128)(2,1)S(1)}, u32[]{:S(2)}, u32[]{:S(2)}) collective-permute-start(bf16[512,128]{1,0:T(8,128)(2,1)S(1)} %copy-done.9), channel_id=1, source_target_pairs={{0,32},{8,40},{16,48},{24,56},{32,64},{40,72},{48,80},{56,88},{64,... | collective-permute-start | bytes 393224 | tf_op jit(solution)/shard_map/ppermute | solution.py:284
  24.9 6.2 %collective-permute-done.5.refs_5_ = bf16[512,128]{1,0:T(8,128)(2,1)S(1)} collective-permute-done((bf16[512,128]{1,0:T(8,128)(2,1)S(1)}, bf16[512,128]{1,0:T(8,128)(2,1)S(1)}, u32[]{:S(2)}, u32[]{:S(2)}) %collective-permute-start.5) | collective-permute-done | bytes 131104 | tf_op jit(solution)/shard_map/ppermute | solution.py:284
  31.1 3.9 %shard_map.103 = (bf16[2,192,512]{2,1,0:T(8,128)(2,1)S(1)}, bf16[2,192,512]{2,1,0:T(8,128)(2,1)}, bf16[2,192,512]{2,1,0:T(8,128)(2,1)}, bf16[2,192,512]{2,1,0:T(8,128)(2,1)}) custom-call(s32[5]{0:T(128)S(1)} %stack.23.refs_0_, s32[2,512]{1,0:T(2,128)S(1)} %bitcast.7, bf16[512,128]{1,0:T(8,128)(2,1)S(1)} %copy-done.9, ...), custom_call_target="tpu_custom_call" | custom-call | tf_op jit(solution)/shard_map/pallas_call | solution.py:31
  42.5 3.6 %shard_map.106.refs_5_.refs_1_ = f32[512,128]{1,0:T(8,128)S(1)} custom-call(s32[5]{0:T(128)S(1)} %stack.23.refs_0_, s32[512,2]{1,0:T(8,128)S(1)} %copy.12.refs_1_, f32[512,2]{1,0:T(8,128)S(1)} %copy-done.5, bf16[4,272,128]{2,1,0:T(8,128)(2,1)S(1)} %get-tuple-element.51.refs_3_.refs_1_), custom_call_target="tpu_custom_call" | custom-call | tf_op jit(solution)/shard_map/pallas_call | solution.py:31
  46.1 11.9 %collective-permute-done.7.refs_2_ = bf16[2,192,512]{2,1,0:T(8,128)(2,1)S(1)} collective-permute-done((bf16[2,192,512]{2,1,0:T(8,128)(2,1)}, bf16[2,192,512]{2,1,0:T(8,128)(2,1)S(1)}, u32[]{:S(2)}, u32[]{:S(2)}) %collective-permute-start.7) | collective-permute-done | bytes 393248 | tf_op jit(solution)/shard_map/ppermute | solution.py:278
  61.5 2.6 %collective-permute-start.15 = (bf16[4,272,128]{2,1,0:T(8,128)(2,1)S(1)}, bf16[4,272,128]{2,1,0:T(8,128)(2,1)S(1)}, u32[]{:S(2)}, u32[]{:S(2)}) collective-permute-start(bf16[4,272,128]{2,1,0:T(8,128)(2,1)S(1)} %get-tuple-element.56), channel_id=1, source_target_pairs={{0,16},{8,24},{16,0},{24,8},{32,48},{40,56},{48,32},{56,40},{64,80... | collective-permute-start | bytes 835592 | tf_op jit(solution)/shard_map/ppermute | solution.py:284
  65.8 3.6 %collective-permute-done.14.refs_2_ = bf16[4,272,128]{2,1,0:T(8,128)(2,1)S(1)} collective-permute-done((bf16[4,272,128]{2,1,0:T(8,128)(2,1)S(1)}, bf16[4,272,128]{2,1,0:T(8,128)(2,1)S(1)}, u32[]{:S(2)}, u32[]{:S(2)}) %collective-permute-start.14) | collective-permute-done | bytes 278560 | tf_op jit(solution)/shard_map/ppermute | solution.py:284
  69.4 7.1 %collective-permute-done.15.refs_3_ = bf16[4,272,128]{2,1,0:T(8,128)(2,1)S(1)} collective-permute-done((bf16[4,272,128]{2,1,0:T(8,128)(2,1)S(1)}, bf16[4,272,128]{2,1,0:T(8,128)(2,1)S(1)}, u32[]{:S(2)}, u32[]{:S(2)}) %collective-permute-start.15) | collective-permute-done | bytes 278560 | tf_op jit(solution)/shard_map/ppermute | solution.py:284
  78.6 5.5 %all-to-all-start = ((bf16[8,4,272,128]{3,2,1,0:T(8,128)(2,1)}), bf16[8,4,272,128]{3,2,1,0:T(8,128)(2,1)}, u32[]{:S(2)}, u32[]{:S(2)}) async-start(bf16[8,4,272,128]{3,2,1,0:T(8,128)(2,1)} %copy-done.1), calls=%async_computation | async-start | bytes 4456448 | tf_op jit(solution)/shard_map/all_to_all | solution.py:342
  84.8 2.9 %collective-permute-start.12 = (bf16[1536,512]{1,0:T(8,128)(2,1)S(1)}, bf16[1536,512]{1,0:T(8,128)(2,1)}, u32[]{:S(2)}, u32[]{:S(2)}) collective-permute-start(bf16[1536,512]{1,0:T(8,128)(2,1)S(1)} %shard_map.108.refs_5_.refs_1_), channel_id=1, source_target_pairs={{0,16},{8,24},{16,0},{24,8},{32,48},{40,56},{48,32},{56,40},{64,80... | collective-permute-start | bytes 4718600 | tf_op jit(solution)/shard_map/ppermute | solution.py:284
  88.2 50.4 %all-to-all-done.refs_1_ = bf16[8,4,272,128]{3,2,1,0:T(8,128)(2,1)} async-done(((bf16[8,4,272,128]{3,2,1,0:T(8,128)(2,1)}), bf16[8,4,272,128]{3,2,1,0:T(8,128)(2,1)}, u32[]{:S(2)}, u32[]{:S(2)}) %all-to-all-start) | async-done | bytes 2228256 | tf_op jit(solution)/shard_map/all_to_all | solution.py:342
  138.7 4.6 %shard_map.110 = (bf16[1,2048,176]{2,1,0:T(8,128)(2,1)S(1)}, bf16[1,2048,176]{2,1,0:T(8,128)(2,1)S(1)}, bf16[1,2048,176]{2,1,0:T(8,128)(2,1)S(1)}, bf16[4,512,17...) custom-call(s32[5]{0:T(128)S(1)} %stack.23.refs_0_, ...), custom_call_target="tpu_custom_call" | custom-call | tf_op jit(solution)/shard_map/pallas_call | solution.py:31
  143.3 11.9 %collective-permute-done.12.refs_3_ = bf16[1536,512]{1,0:T(8,128)(2,1)} collective-permute-done((bf16[1536,512]{1,0:T(8,128)(2,1)S(1)}, bf16[1536,512]{1,0:T(8,128)(2,1)}, u32[]{:S(2)}, u32[]{:S(2)}) %collective-permute-start.12) | collective-permute-done | bytes 1572896 | tf_op jit(solution)/shard_map/ppermute | solution.py:284
  155.2 5.1 %shard_map.111 = (bf16[768,512]{1,0:T(8,128)(2,1)S(1)}, bf16[768,512]{1,0:T(8,128)(2,1)S(1)}, bf16[768,512]{1,0:T(8,128)(2,1)S(1)}, bf16[768,512]{1,0:T(8,128)(2,1)S(1)}) custom-call(s32[5]{0:T(128)S(1)} %stack.23.refs_0_, bf16[1536,512]{1,0:T(8,128)(2,1)} %copy-done, bf16[1536,512]{1,0:T(8,128)(2,1)} %collective-permute-done.11.refs_2_, ...), custom_call_target="tpu_custom_call" | custom-call | tf_op jit(solution)/shard_map/pallas_call | solution.py:209
  160.4 2.3 collective-permute-start.19
  163.7 5.1 %shard_map.112 = (bf16[768,512]{1,0:T(8,128)(2,1)S(1)}, bf16[768,512]{1,0:T(8,128)(2,1)S(1)}, bf16[768,512]{1,0:T(8,128)(2,1)S(1)}, bf16[768,512]{1,0:T(8,128)(2,1)S(1)}) custom-call(s32[5]{0:T(128)S(1)} %stack.23.refs_0_, bf16[1536,512]{1,0:T(8,128)(2,1)} %copy-done, bf16[1536,512]{1,0:T(8,128)(2,1)} %collective-permute-done.11.refs_2_, ...), custom_call_target="tpu_custom_call" | custom-call | tf_op jit(solution)/shard_map/pallas_call | solution.py:209
  169.4 2.2 collective-permute-start.18
  171.6 8.6 %collective-permute-done.19.refs_2_ = bf16[768,512]{1,0:T(8,128)(2,1)S(1)} collective-permute-done((bf16[768,512]{1,0:T(8,128)(2,1)S(1)}, bf16[768,512]{1,0:T(8,128)(2,1)S(1)}, u32[]{:S(2)}, u32[]{:S(2)}) %collective-permute-start.19) | collective-permute-done | bytes 786464 | tf_op jit(solution)/shard_map/ppermute | solution.py:284
  183.5 13.5 %collective-permute-done.17.refs_2_ = bf16[768,512]{1,0:T(8,128)(2,1)S(1)} collective-permute-done((bf16[768,512]{1,0:T(8,128)(2,1)S(1)}, bf16[768,512]{1,0:T(8,128)(2,1)S(1)}, u32[]{:S(2)}, u32[]{:S(2)}) %collective-permute-start.17) | collective-permute-done | bytes 786464 | tf_op jit(solution)/shard_map/ppermute | solution.py:284
  198.6 1.9 collective-permute-start.22
  200.6 5.8 %collective-permute-done.24.refs_5_ = bf16[768,256]{1,0:T(8,128)(2,1)S(1)} collective-permute-done((bf16[768,256]{1,0:T(8,128)(2,1)S(1)}, bf16[768,256]{1,0:T(8,128)(2,1)S(1)}, u32[]{:S(2)}, u32[]{:S(2)}) %collective-permute-start.24) | collective-permute-done | bytes 393248 | tf_op jit(solution)/shard_map/ppermute | solution.py:284
  207.2 3.4 %collective-permute-start.29 = (bf16[192,512]{1,0:T(8,128)(2,1)S(1)}, bf16[192,512]{1,0:T(8,128)(2,1)S(1)}, u32[]{:S(2)}, u32[]{:S(2)}) collective-permute-start(bf16[192,512]{1,0:T(8,128)(2,1)S(1)} %get-tuple-element.78), channel_id=1, source_target_pairs={{0,5},{1,4},{2,7},{3,6},{4,1},{5,0},{6,3},{7,2},{8,13},{9,12},{10,... | collective-permute-start | bytes 589832 | tf_op jit(solution)/shard_map/ppermute | solution.py:278
  212.3 2.4 collective-permute-done.22.refs_5_
  216.2 2.0 collective-permute-start.25
  219.9 2.1 collective-permute-start.27
  222.0 3.0 %collective-permute-done.31.refs_5_ = bf16[192,512]{1,0:T(8,128)(2,1)S(1)} collective-permute-done((bf16[192,512]{1,0:T(8,128)(2,1)S(1)}, bf16[192,512]{1,0:T(8,128)(2,1)S(1)}, u32[]{:S(2)}, u32[]{:S(2)}) %collective-permute-start.31) | collective-permute-done | bytes 196640 | tf_op jit(solution)/shard_map/ppermute | solution.py:278
  230.0 2.4 %collective-permute-start.32 = (bf16[512,128]{1,0:T(8,128)(2,1)S(1)}, bf16[512,128]{1,0:T(8,128)(2,1)S(1)}, u32[]{:S(2)}, u32[]{:S(2)}) collective-permute-start(bf16[512,128]{1,0:T(8,128)(2,1)S(1)} %get-tuple-element.82), channel_id=1, source_target_pairs={{0,64},{8,72},{16,80},{24,88},{32,96},{40,104},{48,112},{56,120},{... | collective-permute-start | bytes 393224 | tf_op jit(solution)/shard_map/ppermute | solution.py:284
  233.6 2.1 collective-permute-start.34
  235.7 2.2 copy.14
  (89 shorter events, 46.7 us)
Async XLA Ops:
  6.2 28.8 %collective-permute-start = (bf16[2,2,272,128]{3,2,1,0:T(8,128)(2,1)S(1)}, bf16[2,2,272,128]{3,2,1,0:T(8,128)(2,1)S(1)}, u32[]{:S(2)}, u32[]{:S(2)}) collective-permute-start(bf16[2,2,272,128]{3,2,1,0:T(8,128)(2,1)S(1)} %get-tuple-element.47), channel_id=1, source_target_pairs={{0,2},{1,3},{2,4},{3,5},{4,6},{5,7},{6,0},{7,1},{8,10},{9,11},{10,... | collective-permute-start | bytes 835592 | tf_op jit(solution)/shard_map/ppermute | solution.py:278
  8.3 26.7 %collective-permute-start.1 = (bf16[2,2,272,128]{3,2,1,0:T(8,128)(2,1)S(1)}, bf16[2,2,272,128]{3,2,1,0:T(8,128)(2,1)S(1)}, u32[]{:S(2)}, u32[]{:S(2)}) collective-permute-start(bf16[2,2,272,128]{3,2,1,0:T(8,128)(2,1)S(1)} %get-tuple-element.48), channel_id=1, source_target_pairs={{0,4},{1,5},{2,6},{3,7},{4,0},{5,1},{6,2},{7,3},{8,12},{9,13},{10,... | collective-permute-start | bytes 835592 | tf_op jit(solution)/shard_map/ppermute | solution.py:278
  10.7 24.3 %collective-permute-start.2 = (bf16[2,2,272,128]{3,2,1,0:T(8,128)(2,1)S(1)}, bf16[2,2,272,128]{3,2,1,0:T(8,128)(2,1)S(1)}, u32[]{:S(2)}, u32[]{:S(2)}) collective-permute-start(bf16[2,2,272,128]{3,2,1,0:T(8,128)(2,1)S(1)} %get-tuple-element.49), channel_id=1, source_target_pairs={{0,6},{1,7},{2,0},{3,1},{4,2},{5,3},{6,4},{7,5},{8,14},{9,15},{10,... | collective-permute-start | bytes 835592 | tf_op jit(solution)/shard_map/ppermute | solution.py:278
  14.9 10.0 %collective-permute-start.3 = (bf16[512,128]{1,0:T(8,128)(2,1)S(1)}, bf16[512,128]{1,0:T(8,128)(2,1)S(1)}, u32[]{:S(2)}, u32[]{:S(2)}) collective-permute-start(bf16[512,128]{1,0:T(8,128)(2,1)S(1)} %copy-done.9), channel_id=1, source_target_pairs={{0,96},{8,104},{16,112},{24,120},{32,0},{40,8},{48,16},{56,24},{64... | collective-permute-start | bytes 393224 | tf_op jit(solution)/shard_map/ppermute | solution.py:284
  17.3 13.8 %collective-permute-start.5 = (bf16[512,128]{1,0:T(8,128)(2,1)S(1)}, bf16[512,128]{1,0:T(8,128)(2,1)S(1)}, u32[]{:S(2)}, u32[]{:S(2)}) collective-permute-start(bf16[512,128]{1,0:T(8,128)(2,1)S(1)} %copy-done.9), channel_id=1, source_target_pairs={{0,32},{8,40},{16,48},{24,56},{32,64},{40,72},{48,80},{56,88},{64,... | collective-permute-start | bytes 393224 | tf_op jit(solution)/shard_map/ppermute | solution.py:284
  37.5 20.5 %collective-permute-start.7 = (bf16[2,192,512]{2,1,0:T(8,128)(2,1)}, bf16[2,192,512]{2,1,0:T(8,128)(2,1)S(1)}, u32[]{:S(2)}, u32[]{:S(2)}) collective-permute-start(bf16[2,192,512]{2,1,0:T(8,128)(2,1)} %get-tuple-element.52), channel_id=1, source_target_pairs={{0,2},{1,3},{2,4},{3,5},{4,6},{5,7},{6,0},{7,1},{8,10},{9,11},{10,... | collective-permute-start | bytes 1179656 | tf_op jit(solution)/shard_map/ppermute | solution.py:278
  37.8 20.2 %collective-permute-start.8 = (bf16[2,192,512]{2,1,0:T(8,128)(2,1)}, bf16[2,192,512]{2,1,0:T(8,128)(2,1)S(1)}, u32[]{:S(2)}, u32[]{:S(2)}) collective-permute-start(bf16[2,192,512]{2,1,0:T(8,128)(2,1)} %get-tuple-element.53), channel_id=1, source_target_pairs={{0,4},{1,5},{2,6},{3,7},{4,0},{5,1},{6,2},{7,3},{8,12},{9,13},{10,... | collective-permute-start | bytes 1179656 | tf_op jit(solution)/shard_map/ppermute | solution.py:278
  38.7 19.7 %collective-permute-start.9 = (bf16[2,192,512]{2,1,0:T(8,128)(2,1)}, bf16[2,192,512]{2,1,0:T(8,128)(2,1)S(1)}, u32[]{:S(2)}, u32[]{:S(2)}) collective-permute-start(bf16[2,192,512]{2,1,0:T(8,128)(2,1)} %get-tuple-element.54), channel_id=1, source_target_pairs={{0,6},{1,7},{2,0},{3,1},{4,2},{5,3},{6,4},{7,5},{8,14},{9,15},{10,... | collective-permute-start | bytes 1179656 | tf_op jit(solution)/shard_map/ppermute | solution.py:278
  60.2 9.3 %collective-permute-start.14 = (bf16[4,272,128]{2,1,0:T(8,128)(2,1)S(1)}, bf16[4,272,128]{2,1,0:T(8,128)(2,1)S(1)}, u32[]{:S(2)}, u32[]{:S(2)}) collective-permute-start(bf16[4,272,128]{2,1,0:T(8,128)(2,1)S(1)} %get-tuple-element.55), channel_id=1, source_target_pairs={{0,8},{8,16},{16,24},{24,0},{32,40},{40,48},{48,56},{56,32},{64,72... | collective-permute-start | bytes 835592 | tf_op jit(solution)/shard_map/ppermute | solution.py:284
  61.5 15.1 %collective-permute-start.15 = (bf16[4,272,128]{2,1,0:T(8,128)(2,1)S(1)}, bf16[4,272,128]{2,1,0:T(8,128)(2,1)S(1)}, u32[]{:S(2)}, u32[]{:S(2)}) collective-permute-start(bf16[4,272,128]{2,1,0:T(8,128)(2,1)S(1)} %get-tuple-element.56), channel_id=1, source_target_pairs={{0,16},{8,24},{16,0},{24,8},{32,48},{40,56},{48,32},{56,40},{64,80... | collective-permute-start | bytes 835592 | tf_op jit(solution)/shard_map/ppermute | solution.py:284
  64.1 12.4 %collective-permute-start.16 = (bf16[4,272,128]{2,1,0:T(8,128)(2,1)S(1)}, bf16[4,272,128]{2,1,0:T(8,128)(2,1)S(1)}, u32[]{:S(2)}, u32[]{:S(2)}) collective-permute-start(bf16[4,272,128]{2,1,0:T(8,128)(2,1)S(1)} %get-tuple-element.57), channel_id=1, source_target_pairs={{0,24},{8,0},{16,8},{24,16},{32,56},{40,32},{48,40},{56,48},{64,88... | collective-permute-start | bytes 835592 | tf_op jit(solution)/shard_map/ppermute | solution.py:284
  78.6 60.0 %all-to-all-start = ((bf16[8,4,272,128]{3,2,1,0:T(8,128)(2,1)}), bf16[8,4,272,128]{3,2,1,0:T(8,128)(2,1)}, u32[]{:S(2)}, u32[]{:S(2)}) async-start(bf16[8,4,272,128]{3,2,1,0:T(8,128)(2,1)} %copy-done.1), calls=%async_computation | async-start | bytes 4456448 | tf_op jit(solution)/shard_map/all_to_all | solution.py:342
  84.1 59.2 %collective-permute-start.13 = (bf16[1536,512]{1,0:T(8,128)(2,1)S(1)}, bf16[1536,512]{1,0:T(8,128)(2,1)}, u32[]{:S(2)}, u32[]{:S(2)}) collective-permute-start(bf16[1536,512]{1,0:T(8,128)(2,1)S(1)} %shard_map.108.refs_5_.refs_1_), channel_id=1, source_target_pairs={{0,8},{8,16},{16,24},{24,0},{32,40},{40,48},{48,56},{56,32},{64,72... | collective-permute-start | bytes 4718600 | tf_op jit(solution)/shard_map/ppermute | solution.py:284
  84.8 70.4 %collective-permute-start.12 = (bf16[1536,512]{1,0:T(8,128)(2,1)S(1)}, bf16[1536,512]{1,0:T(8,128)(2,1)}, u32[]{:S(2)}, u32[]{:S(2)}) collective-permute-start(bf16[1536,512]{1,0:T(8,128)(2,1)S(1)} %shard_map.108.refs_5_.refs_1_), channel_id=1, source_target_pairs={{0,16},{8,24},{16,0},{24,8},{32,48},{40,56},{48,32},{56,40},{64,80... | collective-permute-start | bytes 4718600 | tf_op jit(solution)/shard_map/ppermute | solution.py:284
  87.7 67.5 %collective-permute-start.11 = (bf16[1536,512]{1,0:T(8,128)(2,1)S(1)}, bf16[1536,512]{1,0:T(8,128)(2,1)}, u32[]{:S(2)}, u32[]{:S(2)}) collective-permute-start(bf16[1536,512]{1,0:T(8,128)(2,1)S(1)} %shard_map.108.refs_5_.refs_1_), channel_id=1, source_target_pairs={{0,24},{8,0},{16,8},{24,16},{32,56},{40,32},{48,40},{56,48},{64,88... | collective-permute-start | bytes 4718600 | tf_op jit(solution)/shard_map/ppermute | solution.py:284
  160.4 19.7 %collective-permute-start.19 = (bf16[768,512]{1,0:T(8,128)(2,1)S(1)}, bf16[768,512]{1,0:T(8,128)(2,1)S(1)}, u32[]{:S(2)}, u32[]{:S(2)}) collective-permute-start(bf16[768,512]{1,0:T(8,128)(2,1)S(1)} %get-tuple-element.67), channel_id=1, source_target_pairs={{0,8},{8,16},{16,24},{24,0},{32,40},{40,48},{48,56},{56,32},{64,72... | collective-permute-start | bytes 2359304 | tf_op jit(solution)/shard_map/ppermute | solution.py:284
  162.7 18.3 %collective-permute-start.20 = (bf16[768,512]{1,0:T(8,128)(2,1)S(1)}, bf16[768,512]{1,0:T(8,128)(2,1)S(1)}, u32[]{:S(2)}, u32[]{:S(2)}) collective-permute-start(bf16[768,512]{1,0:T(8,128)(2,1)S(1)} %get-tuple-element.68), channel_id=1, source_target_pairs={{0,24},{8,0},{16,8},{24,16},{32,56},{40,32},{48,40},{56,48},{64,88... | collective-permute-start | bytes 2359304 | tf_op jit(solution)/shard_map/ppermute | solution.py:284
  168.8 28.2 %collective-permute-start.17 = (bf16[768,512]{1,0:T(8,128)(2,1)S(1)}, bf16[768,512]{1,0:T(8,128)(2,1)S(1)}, u32[]{:S(2)}, u32[]{:S(2)}) collective-permute-start(bf16[768,512]{1,0:T(8,128)(2,1)S(1)} %get-tuple-element.63), channel_id=1, source_target_pairs={{0,8},{8,16},{16,24},{24,0},{32,40},{40,48},{48,56},{56,32},{64,72... | collective-permute-start | bytes 2359304 | tf_op jit(solution)/shard_map/ppermute | solution.py:284
  169.4 28.5 %collective-permute-start.18 = (bf16[768,512]{1,0:T(8,128)(2,1)S(1)}, bf16[768,512]{1,0:T(8,128)(2,1)S(1)}, u32[]{:S(2)}, u32[]{:S(2)}) collective-permute-start(bf16[768,512]{1,0:T(8,128)(2,1)S(1)} %get-tuple-element.64), channel_id=1, source_target_pairs={{0,24},{8,0},{16,8},{24,16},{32,56},{40,32},{48,40},{56,48},{64,88... | collective-permute-start | bytes 2359304 | tf_op jit(solution)/shard_map/ppermute | solution.py:284
  181.8 24.6 %collective-permute-start.24 = (bf16[768,256]{1,0:T(8,128)(2,1)S(1)}, bf16[768,256]{1,0:T(8,128)(2,1)S(1)}, u32[]{:S(2)}, u32[]{:S(2)}) collective-permute-start(bf16[768,256]{1,0:T(8,128)(2,1)S(1)} %get-tuple-element.72), channel_id=1, source_target_pairs={{0,24},{8,0},{16,8},{24,16},{32,56},{40,32},{48,40},{56,48},{64,88... | collective-permute-start | bytes 1179656 | tf_op jit(solution)/shard_map/ppermute | solution.py:284
  183.5 22.8 %collective-permute-start.23 = (bf16[768,256]{1,0:T(8,128)(2,1)S(1)}, bf16[768,256]{1,0:T(8,128)(2,1)S(1)}, u32[]{:S(2)}, u32[]{:S(2)}) collective-permute-start(bf16[768,256]{1,0:T(8,128)(2,1)S(1)} %get-tuple-element.69.refs_4_), channel_id=1, source_target_pairs={{0,8},{8,16},{16,24},{24,0},{32,40},{40,48},{48,56},{56,32},{64,72... | collective-permute-start | bytes 1179656 | tf_op jit(solution)/shard_map/ppermute | solution.py:284
  198.6 16.1 %collective-permute-start.22 = (bf16[768,256]{1,0:T(8,128)(2,1)S(1)}, bf16[768,256]{1,0:T(8,128)(2,1)S(1)}, u32[]{:S(2)}, u32[]{:S(2)}) collective-permute-start(bf16[768,256]{1,0:T(8,128)(2,1)S(1)} %get-tuple-element.71), channel_id=1, source_target_pairs={{0,24},{8,0},{16,8},{24,16},{32,56},{40,32},{48,40},{56,48},{64,88... | collective-permute-start | bytes 1179656 | tf_op jit(solution)/shard_map/ppermute | solution.py:284
  200.6 14.8 %collective-permute-start.21 = (bf16[768,256]{1,0:T(8,128)(2,1)S(1)}, bf16[768,256]{1,0:T(8,128)(2,1)S(1)}, u32[]{:S(2)}, u32[]{:S(2)}) collective-permute-start(bf16[768,256]{1,0:T(8,128)(2,1)S(1)} %get-tuple-element.70.refs_6_), channel_id=1, source_target_pairs={{0,8},{8,16},{16,24},{24,0},{32,40},{40,48},{48,56},{56,32},{64,72... | collective-permute-start | bytes 1179656 | tf_op jit(solution)/shard_map/ppermute | solution.py:284
  207.2 11.0 %collective-permute-start.29 = (bf16[192,512]{1,0:T(8,128)(2,1)S(1)}, bf16[192,512]{1,0:T(8,128)(2,1)S(1)}, u32[]{:S(2)}, u32[]{:S(2)}) collective-permute-start(bf16[192,512]{1,0:T(8,128)(2,1)S(1)} %get-tuple-element.78), channel_id=1, source_target_pairs={{0,5},{1,4},{2,7},{3,6},{4,1},{5,0},{6,3},{7,2},{8,13},{9,12},{10,... | collective-permute-start | bytes 589832 | tf_op jit(solution)/shard_map/ppermute | solution.py:278
  210.6 9.3 %collective-permute-start.30 = (bf16[192,512]{1,0:T(8,128)(2,1)S(1)}, bf16[192,512]{1,0:T(8,128)(2,1)S(1)}, u32[]{:S(2)}, u32[]{:S(2)}) collective-permute-start(bf16[192,512]{1,0:T(8,128)(2,1)S(1)} %get-tuple-element.79), channel_id=1, source_target_pairs={{0,7},{1,6},{2,1},{3,0},{4,3},{5,2},{6,5},{7,4},{8,15},{9,14},{10,... | collective-permute-start | bytes 589832 | tf_op jit(solution)/shard_map/ppermute | solution.py:278
  212.1 12.9 %collective-permute-start.31 = (bf16[192,512]{1,0:T(8,128)(2,1)S(1)}, bf16[192,512]{1,0:T(8,128)(2,1)S(1)}, u32[]{:S(2)}, u32[]{:S(2)}) collective-permute-start(bf16[192,512]{1,0:T(8,128)(2,1)S(1)} %get-tuple-element.80), channel_id=1, source_target_pairs={{0,3},{1,2},{2,5},{3,4},{4,7},{5,6},{6,1},{7,0},{8,11},{9,10},{10,... | collective-permute-start | bytes 589832 | tf_op jit(solution)/shard_map/ppermute | solution.py:278
  214.7 10.2 %collective-permute-start.28 = (bf16[192,512]{1,0:T(8,128)(2,1)S(1)}, bf16[192,512]{1,0:T(8,128)(2,1)S(1)}, u32[]{:S(2)}, u32[]{:S(2)}) collective-permute-start(bf16[192,512]{1,0:T(8,128)(2,1)S(1)} %get-tuple-element.73.refs_6_), channel_id=1, source_target_pairs={{0,4},{1,5},{2,6},{3,7},{4,0},{5,1},{6,2},{7,3},{8,12},{9,13},{10,... | collective-permute-start | bytes 589832 | tf_op jit(solution)/shard_map/ppermute | solution.py:278
  216.2 10.2 %collective-permute-start.25 = (bf16[192,512]{1,0:T(8,128)(2,1)S(1)}, bf16[192,512]{1,0:T(8,128)(2,1)S(1)}, u32[]{:S(2)}, u32[]{:S(2)}) collective-permute-start(bf16[192,512]{1,0:T(8,128)(2,1)S(1)} %get-tuple-element.75), channel_id=1, source_target_pairs={{0,1},{1,0},{2,3},{3,2},{4,5},{5,4},{6,7},{7,6},{8,9},{9,8},{10,11... | collective-permute-start | bytes 589832 | tf_op jit(solution)/shard_map/ppermute | solution.py:278
  218.2 9.9 %collective-permute-start.26 = (bf16[192,512]{1,0:T(8,128)(2,1)S(1)}, bf16[192,512]{1,0:T(8,128)(2,1)S(1)}, u32[]{:S(2)}, u32[]{:S(2)}) collective-permute-start(bf16[192,512]{1,0:T(8,128)(2,1)S(1)} %get-tuple-element.76), channel_id=1, source_target_pairs={{0,6},{1,7},{2,0},{3,1},{4,2},{5,3},{6,4},{7,5},{8,14},{9,15},{10,... | collective-permute-start | bytes 589832 | tf_op jit(solution)/shard_map/ppermute | solution.py:278
  219.9 8.7 %collective-permute-start.27 = (bf16[192,512]{1,0:T(8,128)(2,1)S(1)}, bf16[192,512]{1,0:T(8,128)(2,1)S(1)}, u32[]{:S(2)}, u32[]{:S(2)}) collective-permute-start(bf16[192,512]{1,0:T(8,128)(2,1)S(1)} %get-tuple-element.77), channel_id=1, source_target_pairs={{0,2},{1,3},{2,4},{3,5},{4,6},{5,7},{6,0},{7,1},{8,10},{9,11},{10,... | collective-permute-start | bytes 589832 | tf_op jit(solution)/shard_map/ppermute | solution.py:278
  230.0 10.4 %collective-permute-start.32 = (bf16[512,128]{1,0:T(8,128)(2,1)S(1)}, bf16[512,128]{1,0:T(8,128)(2,1)S(1)}, u32[]{:S(2)}, u32[]{:S(2)}) collective-permute-start(bf16[512,128]{1,0:T(8,128)(2,1)S(1)} %get-tuple-element.82), channel_id=1, source_target_pairs={{0,64},{8,72},{16,80},{24,88},{32,96},{40,104},{48,112},{56,120},{... | collective-permute-start | bytes 393224 | tf_op jit(solution)/shard_map/ppermute | solution.py:284
  232.5 7.9 %collective-permute-start.33 = (bf16[512,128]{1,0:T(8,128)(2,1)S(1)}, bf16[512,128]{1,0:T(8,128)(2,1)S(1)}, u32[]{:S(2)}, u32[]{:S(2)}) collective-permute-start(bf16[512,128]{1,0:T(8,128)(2,1)S(1)} %get-tuple-element.83), channel_id=1, source_target_pairs={{0,32},{8,40},{16,48},{24,56},{32,64},{40,72},{48,80},{56,88},{64,... | collective-permute-start | bytes 393224 | tf_op jit(solution)/shard_map/ppermute | solution.py:284
  (16 other events, 147.8 us)
where the time goes:
time: 246 us; the launch traced here: 241 us
  waiting for transfers between devices  130 us (53%)
  starting transfers between devices  64.3 us (26%)
  Pallas kernels  34 us (14%)
  local copies, waits for them, and re-layouts  11.2 us (5%)
    ppermute x20, waiting for transfers between devices, shift_fs(): lax.ppermute(a, 'fs', [(4 * z + y, 4 * ((z + dz) % 4) + (y + dy) % 4) for...  62 us
    all_to_all x1, waiting for transfers between devices, local(): lax.all_to_all(to_z, ('gr', 'fs'), 0, 0, axis_index_groups=[[4 * z + y fo...  50.4 us
    ppermute x20, starting transfers between devices, shift_fs(): lax.ppermute(a, 'fs', [(4 * z + y, 4 * ((z + dz) % 4) + (y + dy) % 4) for...  36.6 us
    pallas_call x15, Pallas kernels, call(): pl.pallas_call(run, out_shape=outs, in_specs=[pl.BlockSpec(memory_space=p...  23.8 us
    ppermute x15, starting transfers between devices, shift_tp(): lax.ppermute(a, 'tp', [(2 * x + c, 2 * ((x + dx) % 4) + (c + dc) % 2) for...  22.3 us
    ppermute x15, waiting for transfers between devices, shift_tp(): lax.ppermute(a, 'tp', [(2 * x + c, 2 * ((x + dx) % 4) + (c + dc) % 2) for...  17.5 us
    unnamed x29, local copies, waits for them, and re-layouts  10.4 us
    pallas_call x2, Pallas kernels, by_rows(): pl.pallas_call(run, grid=(2,), in_specs=[pl.BlockSpec(memory_space=pltpu....  10.2 us
  transfers between devices with their start and end apart: 36, of which 18 were waited for; matrix products, arithmetic and copies ran while one was open for 2% of the time, Pallas kernels for 10%

commit v1 on v0

--- a/solution.py
+++ b/solution.py
@@ -13,16 +13,15 @@
 MAIN, REM = 128, 48
 PACK_GU, PACK_D = 176, 96
 PACK = PACK_GU + PACK_D
-TRIPS = ((4, 5, 3, 7), (0, 1, 2, 6))
+TRIPS = ((4, 5), (3, 7, 2, 6, 1, 0))
 ROWS = CAP * 8
-HALF = CAP * 4
 
 
 def spec_vmem():
     return pl.BlockSpec(memory_space=pltpu.VMEM)
 
 
-def call(body, outs, args, scratch=(), after=(), in_hbm=0):
+def call(body, outs, args, scratch=(), after=()):
     n, m = len(args), len(after)
 
     def run(*refs):
@@ -32,8 +31,7 @@
         run,
         out_shape=outs,
         in_specs=[pl.BlockSpec(memory_space=pltpu.SMEM)]
-        + [spec_vmem()] * (n - 1 - in_hbm)
-        + [pl.BlockSpec(memory_space=pltpu.HBM)] * in_hbm
+        + [spec_vmem()] * (n - 1)
         + [pl.BlockSpec(memory_space=pl.ANY)] * m,
         out_specs=jax.tree.map(lambda _: spec_vmem(), outs),
         scratch_shapes=list(scratch),
@@ -49,17 +47,8 @@
     return ((where[0] + r // 2) % 4) * 2 + (where[1] + r % 2) % 2
 
 
-def pack_body(where, gain, gate_hbm, up_hbm, down_hbm, *refs):
-    outs, (gate, up, down, sems) = refs[:4], refs[4:]
-    copies = [
-        pltpu.make_async_copy(src, dst, sems.at[i])
-        for i, (src, dst) in enumerate(((gate_hbm, gate), (up_hbm, up), (down_hbm, down)))
-    ]
-    for copy in copies:
-        copy.start()
+def pack_body(where, gain, gate, up, down, *outs):
     g = gain[...]
-    for copy in copies:
-        copy.wait()
     for r in range(8):
         e = peer(where, r)
         for top, mats in ((0, (gate[e] * g, up[e] * g)), (PACK_GU, (down[e],))):
@@ -112,7 +101,6 @@
     def _(z8):
         for j in range(4):
             block = z8 * 4 + (y + 4 - j) % 4
-            at = pl.multiple_of(block * 64, 64)
             part = block // 2
             near = ((part // 4 + 4 - z) % 4) * 128 + (block % 2) * 64
             near = pl.multiple_of(near, 64)
@@ -131,23 +119,21 @@
                     rest = jnp.concatenate(
                         [row[:, REM * p : REM * p + REM] for p in range(4 * i, 4 * i + 4)], axis=0
                     ).astype(BF)
-                    outs[m][0, pl.ds(at, 64), 0:MAIN] = main
-                    outs[m][0, pl.ds(at, 64), MAIN:F] = rest
-                    outs[3 + m][q, pl.ds(near, 64), 0:MAIN] = main
-                    outs[3 + m][q, pl.ds(near, 64), MAIN:F] = rest
-
-
-def dispatch_body(where, routes, *refs):
-    toks, outs, table, made = refs[:4], refs[4:8], refs[8], refs[9]
-    r0, r1 = routes[0:1, :], routes[1:2, :]
-    expert = lax.broadcasted_iota(jnp.int32, (8, TOK), 0)
-    named = (r0 == expert) | (r1 == expert)
-    before = (
-        lax.broadcasted_iota(jnp.int32, (TOK, TOK), 0)
-        < lax.broadcasted_iota(jnp.int32, (TOK, TOK), 1)
-    ).astype(F32).astype(BF)
-    count = jnp.dot(named.astype(F32).astype(BF), before, preferred_element_type=F32)
-    table[...] = jnp.where(named, count, -1.0)
+                    outs[m][q, pl.ds(near, 64), 0:MAIN] = main
+                    outs[m][q, pl.ds(near, 64), MAIN:F] = rest
+
+
+def serve_body(where, *refs):
+    z, y = where[2], where[3]
+    for m in range(3):
+        for q in range(4):
+            for k in range(4):
+                at = pl.multiple_of((((z + k) % 4) * 4 + (y + q) % 4) * 128, 128)
+                refs[3 + m][0, pl.ds(at, 128), :] = refs[m][q, 128 * k : 128 * k + 128, :]
+
+
+def dispatch_body(where, table, *refs):
+    toks, outs, made = refs[:4], refs[4:8], refs[8]
     x = jnp.concatenate([t[...] for t in toks], axis=1)
     slot = lax.broadcasted_iota(jnp.int32, (CAP, TOK), 0).astype(F32)
 
@@ -198,8 +184,8 @@
     own[:, 256:512] = out(0, 1)
 
 
-def by_rows(body, where, tiled, whole, widths, n, block, after=()):
-    tile = n // 2
+def by_rows(body, where, tiled, whole, widths, n, first_tile, after=()):
+    tile = 2 * CAP
     rows = lambda w, first=0: pl.BlockSpec((tile, w), lambda i: (i + first, 0))
     m = len(tiled) + len(whole) + 1
 
@@ -208,9 +194,9 @@
 
     return pl.pallas_call(
         run,
-        grid=(2,),
+        grid=(n // tile,),
         in_specs=[pl.BlockSpec(memory_space=pltpu.SMEM)]
-        + [rows(a.shape[1], 2 * block) for a in tiled]
+        + [rows(a.shape[1], first_tile) for a in tiled]
         + [pl.BlockSpec(a.shape, lambda i: (0, 0, 0)) for a in whole]
         + [pl.BlockSpec(memory_space=pl.ANY)] * len(after),
         out_specs=[rows(w) for w in widths],
@@ -233,7 +219,7 @@
         out[:, 256:512] = (b + from_left[at, 256:512].astype(F32)).astype(BF)
 
 
-def plan_body(where, routes, weight, out):
+def plan_body(where, routes, weight, routes_t, out, table_t):
     r0, r1 = routes[:, 0:1], routes[:, 1:2]
     w0, w1 = weight[:, 0:1], weight[:, 1:2]
     expert = lax.broadcasted_iota(jnp.int32, (TOK, 128), 1)
@@ -252,6 +238,14 @@
         w = jnp.where(r0 == e, w0, jnp.where(r1 == e, w1, 0.0))
         table = jnp.where(expert == r, at, jnp.where(expert == 8 + r, w, table))
     out[...] = table
+    expert = lax.broadcasted_iota(jnp.int32, (8, TOK), 0)
+    named = (routes_t[0:1, :] == expert) | (routes_t[1:2, :] == expert)
+    before = (
+        lax.broadcasted_iota(jnp.int32, (TOK, TOK), 0)
+        < lax.broadcasted_iota(jnp.int32, (TOK, TOK), 1)
+    ).astype(F32).astype(BF)
+    count = jnp.dot(named.astype(F32).astype(BF), before, preferred_element_type=F32)
+    table_t[...] = jnp.where(named, count, -1.0)
 
 
 def combine_body(relative, plan, *refs):
@@ -292,12 +286,16 @@
     by_k = [tokens] * 4
     for k in (2, 1, 3):
         by_k[k] = shift_fs(tokens, -k, 0)
+    plan, table = call(
+        plan_body,
+        [sds(TOK, 128, dtype=F32), sds(8, TOK, dtype=F32)],
+        (where, routes, route_weight, routes.T),
+    )
     packed = call(
         pack_body,
         [sds(2, 2, PACK, 128)] * 4,
         (where, norm_gain[:, None], gate_master, up_master, down_master),
-        scratch=[pltpu.VMEM(gate_master.shape, F32)] * 3 + [pltpu.SemaphoreType.DMA((3,))],
-        in_hbm=3,
+        after=(plan,),
     )
 
     def over_x(parts):
@@ -315,8 +313,8 @@
     slots = call(
         dispatch_body,
         [sds(2, CAP, 512)] * 4,
-        (where, routes.T, *by_k),
-        scratch=[pltpu.VMEM((8, TOK), F32), pltpu.VMEM((8, CAP, 512), BF)],
+        (where, table, *by_k),
+        scratch=[pltpu.VMEM((8, CAP, 512), BF)],
         after=(packed[0],),
     )
     t_x = over_x(slots)
@@ -331,10 +329,7 @@
     w_y = list(to_y)
     for dy in (2, 1, 3):
         w_y[dy] = shift_fs(to_y[dy], 0, dy)
-    plan = call(
-        plan_body, [sds(TOK, 128, dtype=F32)], (where, routes, route_weight), after=(to_y[0],)
-    )[0]
-    _, t_core = swap(t_x, (plan,))
+    _, t_core = swap(t_x, (to_y[0],))
     own = call(rows_body, [sds(ROWS, 512)], (where, *t_x, t_core))[0]
     two, plus, minus = shift_fs(own, 0, 2), shift_fs(own, 0, 1), shift_fs(own, 0, -1)
     rows = (own, minus, two, plus)
@@ -347,19 +342,19 @@
         axis_index_groups=[[4 * z + y for z in range(8)] for y in range(4)],
         tiled=True,
     )
-    gate_w, up_w, down_w, *ordered = call(
-        unpack_body, [sds(1, D, F)] * 3 + [sds(4, 512, F)] * 3, (where, w_z)
-    )
+    ordered = call(unpack_body, [sds(4, 512, F)] * 3, (where, w_z))
     made = []
     for t in range(2):
         last = [m[0] for m in made[-1:]]
-        made.append(by_rows(ffn_body, where, rows, ordered, (512,) * 4, HALF, t, after=last))
+        n = CAP * len(TRIPS[t])
+        made.append(by_rows(ffn_body, where, rows, ordered, (512,) * 4, n, t, after=last))
 
     def out_y(t):
         return shift_fs(made[t][1], 0, 1), shift_fs(made[t][2], 0, -1)
 
     def sum_y(t, got, after):
-        sums = call(add_body, [sds(HALF, 256)] * 2, (where, made[t][3], *got), after=after)
+        n = CAP * len(TRIPS[t])
+        sums = call(add_body, [sds(n, 256)] * 2, (where, made[t][3], *got), after=after)
         return sums[0], (shift_fs(sums[0], 0, 1), shift_fs(sums[1], 0, -1))
 
     def home(t, got, ends, after):
@@ -379,7 +374,8 @@
 
     got = [out_y(t) for t in range(2)]
     add0, ends0 = sum_y(0, got[0], (made[1][0],))
-    add1, ends1 = sum_y(1, got[1], (add0,))
+    gate_w, up_w, down_w = call(serve_body, [sds(1, D, F)] * 3, (where, *ordered), after=(add0,))
+    add1, ends1 = sum_y(1, got[1], (gate_w,))
     sums0, home0 = home(0, got[0], ends0, (add1,))
     sums1, home1 = home(1, got[1], ends1, (sums0,))
     part = combine(0, home0, [sds(TOK, 512, dtype=F32)], (sums1,))

time: 246 us -> 271 us (1.10)
  waiting for transfers between devices: 130 us -> 157 us
    ppermute x20, waiting for transfers between devices: 62 us -> 80 us  [shift_fs(): lax.ppermute(a, 'fs', [(4 * z + y, 4 * ((z + dz) % 4) + (y + dy) % 4) for...]
    ppermute x15, waiting for transfers between devices: 17.5 us -> 26.7 us  [shift_tp(): lax.ppermute(a, 'tp', [(2 * x + c, 2 * ((x + dx) % 4) + (c + dc) % 2) for...]
    pallas_call x15 -> x16, Pallas kernels: 23.8 us -> 22.1 us  [call(): pl.pallas_call(run, out_shape=outs, in_specs=[pl.BlockSpec(memory_space=p...]
  transfers between devices with their start and end apart: 36 -> 36, of which waited for: 18 -> 16; matrix products, arithmetic and copies ran while one was open for 2% -> 1% of each run, Pallas kernels for 10% -> 5%
where the time goes in v1:
time: 271 us; the launch traced here: 267 us
  waiting for transfers between devices  157 us (58%)
  starting transfers between devices  64.1 us (24%)
  Pallas kernels  32 us (12%)
  local copies, waits for them, and re-layouts  11.3 us (4%)
    ppermute x20, waiting for transfers between devices, shift_fs(): lax.ppermute(a, 'fs', [(4 * z + y, 4 * ((z + dz) % 4) + (y + dy) % 4) for...  80 us
    all_to_all x1, waiting for transfers between devices, local(): lax.all_to_all(to_z, ('gr', 'fs'), 0, 0, axis_index_groups=[[4 * z + y fo...  50.4 us
    ppermute x20, starting transfers between devices, shift_fs(): lax.ppermute(a, 'fs', [(4 * z + y, 4 * ((z + dz) % 4) + (y + dy) % 4) for...  37.1 us
    ppermute x15, waiting for transfers between devices, shift_tp(): lax.ppermute(a, 'tp', [(2 * x + c, 2 * ((x + dx) % 4) + (c + dc) % 2) for...  26.7 us
    pallas_call x16, Pallas kernels, call(): pl.pallas_call(run, out_shape=outs, in_specs=[pl.BlockSpec(memory_space=p...  22.1 us
    ppermute x15, starting transfers between devices, shift_tp(): lax.ppermute(a, 'tp', [(2 * x + c, 2 * ((x + dx) % 4) + (c + dc) % 2) for...  21.5 us
    unnamed x29, local copies, waits for them, and re-layouts  10.4 us
    pallas_call x2, Pallas kernels, by_rows(): pl.pallas_call(run, grid=(n // tile,), in_specs=[pl.BlockSpec(memory_spac...  9.85 us
  transfers between devices with their start and end apart: 36, of which 16 were waited for; matrix products, arithmetic and copies ran while one was open for 1% of the time, Pallas kernels for 5%

profile of v1, /device:TPU:1, one launch (start us, length us, event | category | flops | bytes accessed | tf_op | source)
XLA Modules:
  0.0 267.2 jit_solution(6208789534848167222)
XLA Ops:
  4.0 3.6 %shard_map.102 = (f32[512,128]{1,0:T(8,128)S(1)}, f32[8,512]{1,0:T(8,128)S(1)}) custom-call(s32[5]{0:T(128)S(1)} %stack.23.refs_0_, s32[512,2]{1,0:T(8,128)S(1)} %copy.11.refs_1_, f32[512,2]{1,0:T(8,128)S(1)} %copy.12.refs_2_, s32[2,512]{1,0:T(2,128)S(1)} %bitcast.7), custom_call_target="tpu_custom_call" | custom-call | tf_op jit(solution)/shard_map/pallas_call | solution.py:30
  10.9 2.1 collective-permute-start.6
  13.0 2.5 collective-permute-start.7
  16.6 3.0 %collective-permute-start.1 = (bf16[512,128]{1,0:T(8,128)(2,1)S(1)}, bf16[512,128]{1,0:T(8,128)(2,1)S(1)}, u32[]{:S(2)}, u32[]{:S(2)}) collective-permute-start(bf16[512,128]{1,0:T(8,128)(2,1)S(1)} %copy-done.9), channel_id=1, source_target_pairs={{0,64},{8,72},{16,80},{24,88},{32,96},{40,104},{48,112},{56,120},{... | collective-permute-start | bytes 393224 | tf_op jit(solution)/shard_map/ppermute | solution.py:278
  22.0 7.7 %collective-permute-start.2 = (bf16[512,128]{1,0:T(8,128)(2,1)S(1)}, bf16[512,128]{1,0:T(8,128)(2,1)S(1)}, u32[]{:S(2)}, u32[]{:S(2)}) collective-permute-start(bf16[512,128]{1,0:T(8,128)(2,1)S(1)} %copy-done.9), channel_id=1, source_target_pairs={{0,32},{8,40},{16,48},{24,56},{32,64},{40,72},{48,80},{56,88},{64,... | collective-permute-start | bytes 393224 | tf_op jit(solution)/shard_map/ppermute | solution.py:278
  29.6 6.2 %collective-permute-done.2.refs_5_ = bf16[512,128]{1,0:T(8,128)(2,1)S(1)} collective-permute-done((bf16[512,128]{1,0:T(8,128)(2,1)S(1)}, bf16[512,128]{1,0:T(8,128)(2,1)S(1)}, u32[]{:S(2)}, u32[]{:S(2)}) %collective-permute-start.2) | collective-permute-done | bytes 131104 | tf_op jit(solution)/shard_map/ppermute | solution.py:278
  35.8 2.8 %shard_map.104 = (bf16[2,192,512]{2,1,0:T(8,128)(2,1)S(1)}, bf16[2,192,512]{2,1,0:T(8,128)(2,1)S(1)}, bf16[2,192,512]{2,1,0:T(8,128)(2,1)S(1)}, bf16[2,192,512]{2,1,0:T(8,128)(2,1)S(1)}) custom-call(s32[5]{0:T(128)S(1)} %stack.23.refs_0_, f32[8,512]{1,0:T(8,128)S(1)} %get-tuple-element.49.refs_1_, bf16[512,128]{1,0:T(8,128)(2,1)S(1)} %copy-done.9, ...), custom_call_target="tpu_custom_call" | custom-call | tf_op jit(solution)/shard_map/pallas_call | solution.py:30
  43.9 16.8 %collective-permute-done.3.refs_2_ = bf16[2,192,512]{2,1,0:T(8,128)(2,1)S(1)} collective-permute-done((bf16[2,192,512]{2,1,0:T(8,128)(2,1)S(1)}, bf16[2,192,512]{2,1,0:T(8,128)(2,1)S(1)}, u32[]{:S(2)}, u32[]{:S(2)}) %collective-permute-start.3) | collective-permute-done | bytes 393248 | tf_op jit(solution)/shard_map/ppermute | solution.py:272
  64.2 2.6 collective-permute-start.15
  68.6 3.6 %collective-permute-done.14.refs_2_ = bf16[4,272,128]{2,1,0:T(8,128)(2,1)S(1)} collective-permute-done((bf16[4,272,128]{2,1,0:T(8,128)(2,1)S(1)}, bf16[4,272,128]{2,1,0:T(8,128)(2,1)S(1)}, u32[]{:S(2)}, u32[]{:S(2)}) %collective-permute-start.14) | collective-permute-done | bytes 278560 | tf_op jit(solution)/shard_map/ppermute | solution.py:278
  72.2 7.1 %collective-permute-done.15.refs_3_ = bf16[4,272,128]{2,1,0:T(8,128)(2,1)S(1)} collective-permute-done((bf16[4,272,128]{2,1,0:T(8,128)(2,1)S(1)}, bf16[4,272,128]{2,1,0:T(8,128)(2,1)S(1)}, u32[]{:S(2)}, u32[]{:S(2)}) %collective-permute-start.15) | collective-permute-done | bytes 278560 | tf_op jit(solution)/shard_map/ppermute | solution.py:278
  81.4 5.5 %all-to-all-start = ((bf16[8,4,272,128]{3,2,1,0:T(8,128)(2,1)}), bf16[8,4,272,128]{3,2,1,0:T(8,128)(2,1)}, u32[]{:S(2)}, u32[]{:S(2)}) async-start(bf16[8,4,272,128]{3,2,1,0:T(8,128)(2,1)} %copy-done.2), calls=%async_computation | async-start | bytes 4456448 | tf_op jit(solution)/shard_map/all_to_all | solution.py:337
  87.6 2.9 %collective-permute-start.12 = (bf16[1536,512]{1,0:T(8,128)(2,1)S(1)}, bf16[1536,512]{1,0:T(8,128)(2,1)}, u32[]{:S(2)}, u32[]{:S(2)}) collective-permute-start(bf16[1536,512]{1,0:T(8,128)(2,1)S(1)} %shard_map.108.refs_5_.refs_1_), channel_id=1, source_target_pairs={{0,16},{8,24},{16,0},{24,8},{32,48},{40,56},{48,32},{56,40},{64,80... | collective-permute-start | bytes 4718600 | tf_op jit(solution)/shard_map/ppermute | solution.py:278
  91.0 50.4 %all-to-all-done.refs_1_ = bf16[8,4,272,128]{3,2,1,0:T(8,128)(2,1)} async-done(((bf16[8,4,272,128]{3,2,1,0:T(8,128)(2,1)}), bf16[8,4,272,128]{3,2,1,0:T(8,128)(2,1)}, u32[]{:S(2)}, u32[]{:S(2)}) %all-to-all-start) | async-done | bytes 2228256 | tf_op jit(solution)/shard_map/all_to_all | solution.py:337
  141.5 3.4 %shard_map.110 = (bf16[4,512,176]{2,1,0:T(8,128)(2,1)S(1)}, bf16[4,512,176]{2,1,0:T(8,128)(2,1)S(1)}, bf16[4,512,176]{2,1,0:T(8,128)(2,1)S(1)}) custom-call(s32[5]{0:T(128)S(1)} %stack.23.refs_0_, bf16[8,4,272,128]{3,2,1,0:T(8,128)(2,1)} %all-to-all-done.refs_1_), custom_call_target="tpu_custom_call" | custom-call | tf_op jit(solution)/shard_map/pallas_call | solution.py:30
  144.9 13.1 %collective-permute-done.12.refs_3_ = bf16[1536,512]{1,0:T(8,128)(2,1)} collective-permute-done((bf16[1536,512]{1,0:T(8,128)(2,1)S(1)}, bf16[1536,512]{1,0:T(8,128)(2,1)}, u32[]{:S(2)}, u32[]{:S(2)}) %collective-permute-start.12) | collective-permute-done | bytes 1572896 | tf_op jit(solution)/shard_map/ppermute | solution.py:278
  158.0 2.9 %shard_map.111 = (bf16[384,512]{1,0:T(8,128)(2,1)S(1)}, bf16[384,512]{1,0:T(8,128)(2,1)S(1)}, bf16[384,512]{1,0:T(8,128)(2,1)S(1)}, bf16[384,512]{1,0:T(8,128)(2,1)S(1)}) custom-call(s32[5]{0:T(128)S(1)} %stack.23.refs_0_, bf16[1536,512]{1,0:T(8,128)(2,1)} %copy-done, bf16[1536,512]{1,0:T(8,128)(2,1)} %collective-permute-done.11.refs_2_, ...), custom_call_target="tpu_custom_call" | custom-call | tf_op jit(solution)/shard_map/pallas_call | solution.py:195
  161.0 6.9 %shard_map.112 = (bf16[1152,512]{1,0:T(8,128)(2,1)S(1)}, bf16[1152,512]{1,0:T(8,128)(2,1)S(1)}, bf16[1152,512]{1,0:T(8,128)(2,1)}, bf16[1152,512]{1,0:T(8,128)(2,1)}) custom-call(s32[5]{0:T(128)S(1)} %stack.23.refs_0_, bf16[1536,512]{1,0:T(8,128)(2,1)} %copy-done, bf16[1536,512]{1,0:T(8,128)(2,1)} %collective-permute-done.11.refs_2_, ...), custom_call_target="tpu_custom_call" | custom-call | tf_op jit(solution)/shard_map/pallas_call | solution.py:195
  167.9 2.2 collective-permute-start.17
  171.6 2.2 collective-permute-start.20
  173.8 30.6 %collective-permute-done.19.refs_2_ = bf16[384,512]{1,0:T(8,128)(2,1)S(1)} collective-permute-done((bf16[384,512]{1,0:T(8,128)(2,1)S(1)}, bf16[384,512]{1,0:T(8,128)(2,1)S(1)}, u32[]{:S(2)}, u32[]{:S(2)}) %collective-permute-start.19) | collective-permute-done | bytes 393248 | tf_op jit(solution)/shard_map/ppermute | solution.py:278
  210.3 2.7 %collective-permute-start.24 = (bf16[384,256]{1,0:T(8,128)(2,1)S(1)}, bf16[384,256]{1,0:T(8,128)(2,1)S(1)}, u32[]{:S(2)}, u32[]{:S(2)}) collective-permute-start(bf16[384,256]{1,0:T(8,128)(2,1)S(1)} %get-tuple-element.77), channel_id=1, source_target_pairs={{0,24},{8,0},{16,8},{24,16},{32,56},{40,32},{48,40},{56,48},{64,88... | collective-permute-start | bytes 589832 | tf_op jit(solution)/shard_map/ppermute | solution.py:278
  213.0 13.1 %collective-permute-done.24.refs_5_ = bf16[384,256]{1,0:T(8,128)(2,1)S(1)} collective-permute-done((bf16[384,256]{1,0:T(8,128)(2,1)S(1)}, bf16[384,256]{1,0:T(8,128)(2,1)S(1)}, u32[]{:S(2)}, u32[]{:S(2)}) %collective-permute-start.24) | collective-permute-done | bytes 196640 | tf_op jit(solution)/shard_map/ppermute | solution.py:278
  226.1 2.1 collective-permute-done.23.refs_4_
  228.9 3.9 %collective-permute-start.31 = (bf16[192,512]{1,0:T(8,128)(2,1)S(1)}, bf16[192,512]{1,0:T(8,128)(2,1)S(1)}, u32[]{:S(2)}, u32[]{:S(2)}) collective-permute-start(bf16[192,512]{1,0:T(8,128)(2,1)S(1)} %get-tuple-element.85), channel_id=1, source_target_pairs={{0,5},{1,4},{2,7},{3,6},{4,1},{5,0},{6,3},{7,2},{8,13},{9,12},{10,... | collective-permute-start | bytes 589832 | tf_op jit(solution)/shard_map/ppermute | solution.py:272
  232.8 2.3 collective-permute-start.30
  236.3 2.1 collective-permute-start.27
  238.4 2.1 collective-permute-start.29
  240.5 3.5 %collective-permute-done.30.refs_2_ = bf16[192,512]{1,0:T(8,128)(2,1)S(1)} collective-permute-done((bf16[192,512]{1,0:T(8,128)(2,1)S(1)}, bf16[192,512]{1,0:T(8,128)(2,1)S(1)}, u32[]{:S(2)}, u32[]{:S(2)}) %collective-permute-start.30) | collective-permute-done | bytes 196640 | tf_op jit(solution)/shard_map/ppermute | solution.py:272
  246.9 4.2 %collective-permute-done.28.refs_5_ = bf16[192,512]{1,0:T(8,128)(2,1)S(1)} collective-permute-done((bf16[192,512]{1,0:T(8,128)(2,1)S(1)}, bf16[192,512]{1,0:T(8,128)(2,1)S(1)}, u32[]{:S(2)}, u32[]{:S(2)}) %collective-permute-start.28) | collective-permute-done | bytes 196640 | tf_op jit(solution)/shard_map/ppermute | solution.py:272
  251.1 2.3 shard_map.119
  254.2 2.4 collective-permute-start.32
  (90 shorter events, 47.3 us)
Async XLA Ops:
  10.9 27.8 %collective-permute-start.6 = (bf16[2,2,272,128]{3,2,1,0:T(8,128)(2,1)S(1)}, bf16[2,2,272,128]{3,2,1,0:T(8,128)(2,1)S(1)}, u32[]{:S(2)}, u32[]{:S(2)}) collective-permute-start(bf16[2,2,272,128]{3,2,1,0:T(8,128)(2,1)S(1)} %get-tuple-element.55), channel_id=1, source_target_pairs={{0,2},{1,3},{2,4},{3,5},{4,6},{5,7},{6,0},{7,1},{8,10},{9,11},{10,... | collective-permute-start | bytes 835592 | tf_op jit(solution)/shard_map/ppermute | solution.py:272
  13.0 25.7 %collective-permute-start.7 = (bf16[2,2,272,128]{3,2,1,0:T(8,128)(2,1)S(1)}, bf16[2,2,272,128]{3,2,1,0:T(8,128)(2,1)S(1)}, u32[]{:S(2)}, u32[]{:S(2)}) collective-permute-start(bf16[2,2,272,128]{3,2,1,0:T(8,128)(2,1)S(1)} %get-tuple-element.56), channel_id=1, source_target_pairs={{0,4},{1,5},{2,6},{3,7},{4,0},{5,1},{6,2},{7,3},{8,12},{9,13},{10,... | collective-permute-start | bytes 835592 | tf_op jit(solution)/shard_map/ppermute | solution.py:272
  15.5 23.2 %collective-permute-start.8 = (bf16[2,2,272,128]{3,2,1,0:T(8,128)(2,1)S(1)}, bf16[2,2,272,128]{3,2,1,0:T(8,128)(2,1)S(1)}, u32[]{:S(2)}, u32[]{:S(2)}) collective-permute-start(bf16[2,2,272,128]{3,2,1,0:T(8,128)(2,1)S(1)} %get-tuple-element.57), channel_id=1, source_target_pairs={{0,6},{1,7},{2,0},{3,1},{4,2},{5,3},{6,4},{7,5},{8,14},{9,15},{10,... | collective-permute-start | bytes 835592 | tf_op jit(solution)/shard_map/ppermute | solution.py:272
  19.6 10.0 %collective-permute-start = (bf16[512,128]{1,0:T(8,128)(2,1)S(1)}, bf16[512,128]{1,0:T(8,128)(2,1)S(1)}, u32[]{:S(2)}, u32[]{:S(2)}) collective-permute-start(bf16[512,128]{1,0:T(8,128)(2,1)S(1)} %copy-done.9), channel_id=1, source_target_pairs={{0,96},{8,104},{16,112},{24,120},{32,0},{40,8},{48,16},{56,24},{64... | collective-permute-start | bytes 393224 | tf_op jit(solution)/shard_map/ppermute | solution.py:278
  22.0 13.8 %collective-permute-start.2 = (bf16[512,128]{1,0:T(8,128)(2,1)S(1)}, bf16[512,128]{1,0:T(8,128)(2,1)S(1)}, u32[]{:S(2)}, u32[]{:S(2)}) collective-permute-start(bf16[512,128]{1,0:T(8,128)(2,1)S(1)} %copy-done.9), channel_id=1, source_target_pairs={{0,32},{8,40},{16,48},{24,56},{32,64},{40,72},{48,80},{56,88},{64,... | collective-permute-start | bytes 393224 | tf_op jit(solution)/shard_map/ppermute | solution.py:278
  40.5 20.2 %collective-permute-start.3 = (bf16[2,192,512]{2,1,0:T(8,128)(2,1)S(1)}, bf16[2,192,512]{2,1,0:T(8,128)(2,1)S(1)}, u32[]{:S(2)}, u32[]{:S(2)}) collective-permute-start(bf16[2,192,512]{2,1,0:T(8,128)(2,1)S(1)} %get-tuple-element.52), channel_id=1, source_target_pairs={{0,2},{1,3},{2,4},{3,5},{4,6},{5,7},{6,0},{7,1},{8,10},{9,11},{10,... | collective-permute-start | bytes 1179656 | tf_op jit(solution)/shard_map/ppermute | solution.py:272
  40.8 19.9 %collective-permute-start.4 = (bf16[2,192,512]{2,1,0:T(8,128)(2,1)S(1)}, bf16[2,192,512]{2,1,0:T(8,128)(2,1)S(1)}, u32[]{:S(2)}, u32[]{:S(2)}) collective-permute-start(bf16[2,192,512]{2,1,0:T(8,128)(2,1)S(1)} %get-tuple-element.53), channel_id=1, source_target_pairs={{0,4},{1,5},{2,6},{3,7},{4,0},{5,1},{6,2},{7,3},{8,12},{9,13},{10,... | collective-permute-start | bytes 1179656 | tf_op jit(solution)/shard_map/ppermute | solution.py:272
  41.6 19.4 %collective-permute-start.5 = (bf16[2,192,512]{2,1,0:T(8,128)(2,1)S(1)}, bf16[2,192,512]{2,1,0:T(8,128)(2,1)S(1)}, u32[]{:S(2)}, u32[]{:S(2)}) collective-permute-start(bf16[2,192,512]{2,1,0:T(8,128)(2,1)S(1)} %get-tuple-element.54), channel_id=1, source_target_pairs={{0,6},{1,7},{2,0},{3,1},{4,2},{5,3},{6,4},{7,5},{8,14},{9,15},{10,... | collective-permute-start | bytes 1179656 | tf_op jit(solution)/shard_map/ppermute | solution.py:272
  62.9 9.3 %collective-permute-start.14 = (bf16[4,272,128]{2,1,0:T(8,128)(2,1)S(1)}, bf16[4,272,128]{2,1,0:T(8,128)(2,1)S(1)}, u32[]{:S(2)}, u32[]{:S(2)}) collective-permute-start(bf16[4,272,128]{2,1,0:T(8,128)(2,1)S(1)} %get-tuple-element.59), channel_id=1, source_target_pairs={{0,8},{8,16},{16,24},{24,0},{32,40},{40,48},{48,56},{56,32},{64,72... | collective-permute-start | bytes 835592 | tf_op jit(solution)/shard_map/ppermute | solution.py:278
  64.2 15.1 %collective-permute-start.15 = (bf16[4,272,128]{2,1,0:T(8,128)(2,1)S(1)}, bf16[4,272,128]{2,1,0:T(8,128)(2,1)S(1)}, u32[]{:S(2)}, u32[]{:S(2)}) collective-permute-start(bf16[4,272,128]{2,1,0:T(8,128)(2,1)S(1)} %get-tuple-element.60), channel_id=1, source_target_pairs={{0,16},{8,24},{16,0},{24,8},{32,48},{40,56},{48,32},{56,40},{64,80... | collective-permute-start | bytes 835592 | tf_op jit(solution)/shard_map/ppermute | solution.py:278
  66.9 12.4 %collective-permute-start.16 = (bf16[4,272,128]{2,1,0:T(8,128)(2,1)S(1)}, bf16[4,272,128]{2,1,0:T(8,128)(2,1)S(1)}, u32[]{:S(2)}, u32[]{:S(2)}) collective-permute-start(bf16[4,272,128]{2,1,0:T(8,128)(2,1)S(1)} %get-tuple-element.61), channel_id=1, source_target_pairs={{0,24},{8,0},{16,8},{24,16},{32,56},{40,32},{48,40},{56,48},{64,88... | collective-permute-start | bytes 835592 | tf_op jit(solution)/shard_map/ppermute | solution.py:278
  81.4 60.0 %all-to-all-start = ((bf16[8,4,272,128]{3,2,1,0:T(8,128)(2,1)}), bf16[8,4,272,128]{3,2,1,0:T(8,128)(2,1)}, u32[]{:S(2)}, u32[]{:S(2)}) async-start(bf16[8,4,272,128]{3,2,1,0:T(8,128)(2,1)} %copy-done.2), calls=%async_computation | async-start | bytes 4456448 | tf_op jit(solution)/shard_map/all_to_all | solution.py:337
  86.9 58.0 %collective-permute-start.13 = (bf16[1536,512]{1,0:T(8,128)(2,1)S(1)}, bf16[1536,512]{1,0:T(8,128)(2,1)S(1)}, u32[]{:S(2)}, u32[]{:S(2)}) collective-permute-start(bf16[1536,512]{1,0:T(8,128)(2,1)S(1)} %shard_map.108.refs_5_.refs_1_), channel_id=1, source_target_pairs={{0,8},{8,16},{16,24},{24,0},{32,40},{40,48},{48,56},{56,32},{64,72... | collective-permute-start | bytes 4718600 | tf_op jit(solution)/shard_map/ppermute | solution.py:278
  87.6 70.4 %collective-permute-start.12 = (bf16[1536,512]{1,0:T(8,128)(2,1)S(1)}, bf16[1536,512]{1,0:T(8,128)(2,1)}, u32[]{:S(2)}, u32[]{:S(2)}) collective-permute-start(bf16[1536,512]{1,0:T(8,128)(2,1)S(1)} %shard_map.108.refs_5_.refs_1_), channel_id=1, source_target_pairs={{0,16},{8,24},{16,0},{24,8},{32,48},{40,56},{48,32},{56,40},{64,80... | collective-permute-start | bytes 4718600 | tf_op jit(solution)/shard_map/ppermute | solution.py:278
  90.5 67.5 %collective-permute-start.11 = (bf16[1536,512]{1,0:T(8,128)(2,1)S(1)}, bf16[1536,512]{1,0:T(8,128)(2,1)}, u32[]{:S(2)}, u32[]{:S(2)}) collective-permute-start(bf16[1536,512]{1,0:T(8,128)(2,1)S(1)} %shard_map.108.refs_5_.refs_1_), channel_id=1, source_target_pairs={{0,24},{8,0},{16,8},{24,16},{32,56},{40,32},{48,40},{56,48},{64,88... | collective-permute-start | bytes 4718600 | tf_op jit(solution)/shard_map/ppermute | solution.py:278
  167.9 39.8 %collective-permute-start.17 = (bf16[1152,512]{1,0:T(8,128)(2,1)S(1)}, bf16[1152,512]{1,0:T(8,128)(2,1)S(1)}, u32[]{:S(2)}, u32[]{:S(2)}) collective-permute-start(bf16[1152,512]{1,0:T(8,128)(2,1)S(1)} %get-tuple-element.67), channel_id=1, source_target_pairs={{0,8},{8,16},{16,24},{24,0},{32,40},{40,48},{48,56},{56,32},{64,72... | collective-permute-start | bytes 3538952 | tf_op jit(solution)/shard_map/ppermute | solution.py:278
  170.1 37.6 %collective-permute-start.18 = (bf16[1152,512]{1,0:T(8,128)(2,1)}, bf16[1152,512]{1,0:T(8,128)(2,1)S(1)}, u32[]{:S(2)}, u32[]{:S(2)}) collective-permute-start(bf16[1152,512]{1,0:T(8,128)(2,1)} %get-tuple-element.68), channel_id=1, source_target_pairs={{0,24},{8,0},{16,8},{24,16},{32,56},{40,32},{48,40},{56,48},{64,88... | collective-permute-start | bytes 3538952 | tf_op jit(solution)/shard_map/ppermute | solution.py:278
  171.1 33.3 %collective-permute-start.19 = (bf16[384,512]{1,0:T(8,128)(2,1)S(1)}, bf16[384,512]{1,0:T(8,128)(2,1)S(1)}, u32[]{:S(2)}, u32[]{:S(2)}) collective-permute-start(bf16[384,512]{1,0:T(8,128)(2,1)S(1)} %get-tuple-element.71), channel_id=1, source_target_pairs={{0,8},{8,16},{16,24},{24,0},{32,40},{40,48},{48,56},{56,32},{64,72... | collective-permute-start | bytes 1179656 | tf_op jit(solution)/shard_map/ppermute | solution.py:278
  171.6 33.9 %collective-permute-start.20 = (bf16[384,512]{1,0:T(8,128)(2,1)S(1)}, bf16[384,512]{1,0:T(8,128)(2,1)S(1)}, u32[]{:S(2)}, u32[]{:S(2)}) collective-permute-start(bf16[384,512]{1,0:T(8,128)(2,1)S(1)} %get-tuple-element.72), channel_id=1, source_target_pairs={{0,24},{8,0},{16,8},{24,16},{32,56},{40,32},{48,40},{56,48},{64,88... | collective-permute-start | bytes 1179656 | tf_op jit(solution)/shard_map/ppermute | solution.py:278
  208.6 26.6 %collective-permute-start.22 = (bf16[1152,256]{1,0:T(8,128)(2,1)S(1)}, bf16[1152,256]{1,0:T(8,128)(2,1)S(1)}, u32[]{:S(2)}, u32[]{:S(2)}) collective-permute-start(bf16[1152,256]{1,0:T(8,128)(2,1)S(1)} %get-tuple-element.76), channel_id=1, source_target_pairs={{0,24},{8,0},{16,8},{24,16},{32,56},{40,32},{48,40},{56,48},{64,88... | collective-permute-start | bytes 1769480 | tf_op jit(solution)/shard_map/ppermute | solution.py:278
  210.3 24.8 %collective-permute-start.21 = (bf16[1152,256]{1,0:T(8,128)(2,1)S(1)}, bf16[1152,256]{1,0:T(8,128)(2,1)S(1)}, u32[]{:S(2)}, u32[]{:S(2)}) collective-permute-start(bf16[1152,256]{1,0:T(8,128)(2,1)S(1)} %get-tuple-element.75.refs_6_), channel_id=1, source_target_pairs={{0,8},{8,16},{16,24},{24,0},{32,40},{40,48},{48,56},{56,32},{64,72... | collective-permute-start | bytes 1769480 | tf_op jit(solution)/shard_map/ppermute | solution.py:278
  210.3 15.8 %collective-permute-start.24 = (bf16[384,256]{1,0:T(8,128)(2,1)S(1)}, bf16[384,256]{1,0:T(8,128)(2,1)S(1)}, u32[]{:S(2)}, u32[]{:S(2)}) collective-permute-start(bf16[384,256]{1,0:T(8,128)(2,1)S(1)} %get-tuple-element.77), channel_id=1, source_target_pairs={{0,24},{8,0},{16,8},{24,16},{32,56},{40,32},{48,40},{56,48},{64,88... | collective-permute-start | bytes 589832 | tf_op jit(solution)/shard_map/ppermute | solution.py:278
  213.0 15.2 %collective-permute-start.23 = (bf16[384,256]{1,0:T(8,128)(2,1)S(1)}, bf16[384,256]{1,0:T(8,128)(2,1)S(1)}, u32[]{:S(2)}, u32[]{:S(2)}) collective-permute-start(bf16[384,256]{1,0:T(8,128)(2,1)S(1)} %get-tuple-element.73.refs_4_), channel_id=1, source_target_pairs={{0,8},{8,16},{16,24},{24,0},{32,40},{40,48},{48,56},{56,32},{64,72... | collective-permute-start | bytes 589832 | tf_op jit(solution)/shard_map/ppermute | solution.py:278
  228.9 9.5 %collective-permute-start.31 = (bf16[192,512]{1,0:T(8,128)(2,1)S(1)}, bf16[192,512]{1,0:T(8,128)(2,1)S(1)}, u32[]{:S(2)}, u32[]{:S(2)}) collective-permute-start(bf16[192,512]{1,0:T(8,128)(2,1)S(1)} %get-tuple-element.85), channel_id=1, source_target_pairs={{0,5},{1,4},{2,7},{3,6},{4,1},{5,0},{6,3},{7,2},{8,13},{9,12},{10,... | collective-permute-start | bytes 589832 | tf_op jit(solution)/shard_map/ppermute | solution.py:272
  232.8 11.2 %collective-permute-start.30 = (bf16[192,512]{1,0:T(8,128)(2,1)S(1)}, bf16[192,512]{1,0:T(8,128)(2,1)S(1)}, u32[]{:S(2)}, u32[]{:S(2)}) collective-permute-start(bf16[192,512]{1,0:T(8,128)(2,1)S(1)} %get-tuple-element.78.refs_6_), channel_id=1, source_target_pairs={{0,4},{1,5},{2,6},{3,7},{4,0},{5,1},{6,2},{7,3},{8,12},{9,13},{10,... | collective-permute-start | bytes 589832 | tf_op jit(solution)/shard_map/ppermute | solution.py:272
  236.1 10.8 %collective-permute-start.26 = (bf16[192,512]{1,0:T(8,128)(2,1)S(1)}, bf16[192,512]{1,0:T(8,128)(2,1)S(1)}, u32[]{:S(2)}, u32[]{:S(2)}) collective-permute-start(bf16[192,512]{1,0:T(8,128)(2,1)S(1)} %get-tuple-element.80), channel_id=1, source_target_pairs={{0,3},{1,2},{2,5},{3,4},{4,7},{5,6},{6,1},{7,0},{8,11},{9,10},{10,... | collective-permute-start | bytes 589832 | tf_op jit(solution)/shard_map/ppermute | solution.py:272
  236.3 10.6 %collective-permute-start.27 = (bf16[192,512]{1,0:T(8,128)(2,1)S(1)}, bf16[192,512]{1,0:T(8,128)(2,1)S(1)}, u32[]{:S(2)}, u32[]{:S(2)}) collective-permute-start(bf16[192,512]{1,0:T(8,128)(2,1)S(1)} %get-tuple-element.81), channel_id=1, source_target_pairs={{0,6},{1,7},{2,0},{3,1},{4,2},{5,3},{6,4},{7,5},{8,14},{9,15},{10,... | collective-permute-start | bytes 589832 | tf_op jit(solution)/shard_map/ppermute | solution.py:272
  238.4 12.7 %collective-permute-start.28 = (bf16[192,512]{1,0:T(8,128)(2,1)S(1)}, bf16[192,512]{1,0:T(8,128)(2,1)S(1)}, u32[]{:S(2)}, u32[]{:S(2)}) collective-permute-start(bf16[192,512]{1,0:T(8,128)(2,1)S(1)} %get-tuple-element.82), channel_id=1, source_target_pairs={{0,2},{1,3},{2,4},{3,5},{4,6},{5,7},{6,0},{7,1},{8,10},{9,11},{10,... | collective-permute-start | bytes 589832 | tf_op jit(solution)/shard_map/ppermute | solution.py:272
  238.4 12.7 %collective-permute-start.29 = (bf16[192,512]{1,0:T(8,128)(2,1)S(1)}, bf16[192,512]{1,0:T(8,128)(2,1)S(1)}, u32[]{:S(2)}, u32[]{:S(2)}) collective-permute-start(bf16[192,512]{1,0:T(8,128)(2,1)S(1)} %get-tuple-element.83), channel_id=1, source_target_pairs={{0,1},{1,0},{2,3},{3,2},{4,5},{5,4},{6,7},{7,6},{8,9},{9,8},{10,11... | collective-permute-start | bytes 589832 | tf_op jit(solution)/shard_map/ppermute | solution.py:272
  254.2 11.3 %collective-permute-start.32 = (bf16[512,128]{1,0:T(8,128)(2,1)}, bf16[512,128]{1,0:T(8,128)(2,1)}, u32[]{:S(2)}, u32[]{:S(2)}) collective-permute-start(bf16[512,128]{1,0:T(8,128)(2,1)} %get-tuple-element.87), channel_id=1, source_target_pairs={{0,64},{8,72},{16,80},{24,88},{32,96},{40,104},{48,112},{56,120},{... | collective-permute-start | bytes 393224 | tf_op jit(solution)/shard_map/ppermute | solution.py:278
  256.5 9.0 %collective-permute-start.33 = (bf16[512,128]{1,0:T(8,128)(2,1)}, bf16[512,128]{1,0:T(8,128)(2,1)}, u32[]{:S(2)}, u32[]{:S(2)}) collective-permute-start(bf16[512,128]{1,0:T(8,128)(2,1)} %get-tuple-element.88), channel_id=1, source_target_pairs={{0,32},{8,40},{16,48},{24,56},{32,64},{40,72},{48,80},{56,88},{64,... | collective-permute-start | bytes 393224 | tf_op jit(solution)/shard_map/ppermute | solution.py:278
  257.7 7.8 %collective-permute-start.34 = (bf16[512,128]{1,0:T(8,128)(2,1)S(1)}, bf16[512,128]{1,0:T(8,128)(2,1)}, u32[]{:S(2)}, u32[]{:S(2)}) collective-permute-start(bf16[512,128]{1,0:T(8,128)(2,1)S(1)} %get-tuple-element.89), channel_id=1, source_target_pairs={{0,96},{8,104},{16,112},{24,120},{32,0},{40,8},{48,16},{56,24},{64... | collective-permute-start | bytes 393224 | tf_op jit(solution)/shard_map/ppermute | solution.py:278
  (16 other events, 104.6 us)

commit v2 on v1

--- a/solution.py
+++ b/solution.py
@@ -11,7 +11,7 @@
 F32 = jnp.float32
 CAP, TOK, D, F = 192, 512, 2048, 176
 MAIN, REM = 128, 48
-PACK_GU, PACK_D = 176, 96
+PACK_GU, PACK_D = 176, 88
 PACK = PACK_GU + PACK_D
 TRIPS = ((4, 5), (3, 7, 2, 6, 1, 0))
 ROWS = CAP * 8
@@ -58,13 +58,13 @@
                     at = top + 64 * m
                     outs[r // 2][r % 2, h, at : at + 64, :] = mat[:, h * F : h * F + MAIN].astype(BF)
                     rest = mat[:, h * F + MAIN : (h + 1) * F]
-                    pieces += [rest[16 * i : 16 * i + 16] for i in range(4)]
-                if len(mats) == 1:
-                    pieces.append(jnp.zeros((16, 64), F32))
-                row = jnp.concatenate(pieces, axis=1).astype(BF)
-                for i in range(row.shape[1] // 128):
-                    at = top + 64 * len(mats) + 16 * i
-                    outs[r // 2][r % 2, h, at : at + 16, :] = row[:, 128 * i : 128 * i + 128]
+                    pieces += [rest[8 * i : 8 * i + 8] for i in range(8)]
+                row = jnp.concatenate(pieces, axis=1)
+                at = top + 64 * len(mats)
+                rest = [row[:, 128 * i : 128 * i + 128] for i in range(row.shape[1] // 128)]
+                outs[r // 2][r % 2, h, at : at + 8 * len(rest), :] = jnp.concatenate(
+                    rest, axis=0
+                ).astype(BF)
 
 
 def swap_body(where, *refs):
@@ -106,18 +106,13 @@
             near = pl.multiple_of(near, 64)
             q = (part % 4 + 4 - y) % 4
             for top, mats in ((0, (0, 1)), (PACK_GU, (2,))):
-                first = top + 64 * len(mats)
-                row = jnp.concatenate(
-                    [
-                        got[z8, j, first + 16 * i : first + 16 * i + 16, :].astype(F32)
-                        for i in range(3 if len(mats) == 2 else 2)
-                    ],
-                    axis=1,
-                )
+                first, tiles = top + 64 * len(mats), 3 * len(mats)
+                flat = got[z8, j, first : first + 8 * tiles, :].astype(F32)
+                row = jnp.concatenate([flat[8 * i : 8 * i + 8] for i in range(tiles)], axis=1)
                 for i, m in enumerate(mats):
                     main = got[z8, j, top + 64 * i : top + 64 * i + 64, :]
                     rest = jnp.concatenate(
-                        [row[:, REM * p : REM * p + REM] for p in range(4 * i, 4 * i + 4)], axis=0
+                        [row[:, REM * p : REM * p + REM] for p in range(8 * i, 8 * i + 8)], axis=0
                     ).astype(BF)
                     outs[m][q, pl.ds(near, 64), 0:MAIN] = main
                     outs[m][q, pl.ds(near, 64), MAIN:F] = rest
@@ -132,8 +127,16 @@
                 refs[3 + m][0, pl.ds(at, 128), :] = refs[m][q, 128 * k : 128 * k + 128, :]
 
 
-def dispatch_body(where, table, *refs):
-    toks, outs, made = refs[:4], refs[4:8], refs[8]
+def dispatch_body(where, routes, *refs):
+    toks, outs, table, made = refs[:4], refs[4:8], refs[8], refs[9]
+    expert = lax.broadcasted_iota(jnp.int32, (8, TOK), 0)
+    named = (routes[0:1, :] == expert) | (routes[1:2, :] == expert)
+    before = (
+        lax.broadcasted_iota(jnp.int32, (TOK, TOK), 0)
+        < lax.broadcasted_iota(jnp.int32, (TOK, TOK), 1)
+    ).astype(F32).astype(BF)
+    count = jnp.dot(named.astype(F32).astype(BF), before, preferred_element_type=F32)
+    table[...] = jnp.where(named, count, -1.0)
     x = jnp.concatenate([t[...] for t in toks], axis=1)
     slot = lax.broadcasted_iota(jnp.int32, (CAP, TOK), 0).astype(F32)
 
@@ -219,7 +222,7 @@
         out[:, 256:512] = (b + from_left[at, 256:512].astype(F32)).astype(BF)
 
 
-def plan_body(where, routes, weight, routes_t, out, table_t):
+def plan_body(where, routes, weight, out):
     r0, r1 = routes[:, 0:1], routes[:, 1:2]
     w0, w1 = weight[:, 0:1], weight[:, 1:2]
     expert = lax.broadcasted_iota(jnp.int32, (TOK, 128), 1)
@@ -238,14 +241,6 @@
         w = jnp.where(r0 == e, w0, jnp.where(r1 == e, w1, 0.0))
         table = jnp.where(expert == r, at, jnp.where(expert == 8 + r, w, table))
     out[...] = table
-    expert = lax.broadcasted_iota(jnp.int32, (8, TOK), 0)
-    named = (routes_t[0:1, :] == expert) | (routes_t[1:2, :] == expert)
-    before = (
-        lax.broadcasted_iota(jnp.int32, (TOK, TOK), 0)
-        < lax.broadcasted_iota(jnp.int32, (TOK, TOK), 1)
-    ).astype(F32).astype(BF)
-    count = jnp.dot(named.astype(F32).astype(BF), before, preferred_element_type=F32)
-    table_t[...] = jnp.where(named, count, -1.0)
 
 
 def combine_body(relative, plan, *refs):
@@ -286,16 +281,10 @@
     by_k = [tokens] * 4
     for k in (2, 1, 3):
         by_k[k] = shift_fs(tokens, -k, 0)
-    plan, table = call(
-        plan_body,
-        [sds(TOK, 128, dtype=F32), sds(8, TOK, dtype=F32)],
-        (where, routes, route_weight, routes.T),
-    )
     packed = call(
         pack_body,
         [sds(2, 2, PACK, 128)] * 4,
         (where, norm_gain[:, None], gate_master, up_master, down_master),
-        after=(plan,),
     )
 
     def over_x(parts):
@@ -313,8 +302,8 @@
     slots = call(
         dispatch_body,
         [sds(2, CAP, 512)] * 4,
-        (where, table, *by_k),
-        scratch=[pltpu.VMEM((8, CAP, 512), BF)],
+        (where, routes.T, *by_k),
+        scratch=[pltpu.VMEM((8, TOK), F32), pltpu.VMEM((8, CAP, 512), BF)],
         after=(packed[0],),
     )
     t_x = over_x(slots)
@@ -329,7 +318,10 @@
     w_y = list(to_y)
     for dy in (2, 1, 3):
         w_y[dy] = shift_fs(to_y[dy], 0, dy)
-    _, t_core = swap(t_x, (to_y[0],))
+    plan = call(
+        plan_body, [sds(TOK, 128, dtype=F32)], (where, routes, route_weight), after=(to_y[0],)
+    )[0]
+    _, t_core = swap(t_x, (plan,))
     own = call(rows_body, [sds(ROWS, 512)], (where, *t_x, t_core))[0]
     two, plus, minus = shift_fs(own, 0, 2), shift_fs(own, 0, 1), shift_fs(own, 0, -1)
     rows = (own, minus, two, plus)

time: 271 us -> 265 us (0.978)
  waiting for transfers between devices: 157 us -> 152 us
    ppermute x15, waiting for transfers between devices: 26.7 us -> 21.8 us  [shift_tp(): lax.ppermute(a, 'tp', [(2 * x + c, 2 * ((x + dx) % 4) + (c + dc) % 2) for...]
    unnamed x29 -> x31, local copies, waits for them, and re-layouts: 10.4 us -> 10.4 us
  transfers between devices with their start and end apart: 36 -> 36, of which waited for: 16 -> 17; matrix products, arithmetic and copies ran while one was open for 1% -> 2% of each run, Pallas kernels for 5% -> 6%
where the time goes in v2:
time: 265 us; the launch traced here: 262 us
  waiting for transfers between devices  152 us (57%)
  starting transfers between devices  64 us (24%)
  Pallas kernels  33 us (12%)
  local copies, waits for them, and re-layouts  11.3 us (4%)
    ppermute x20, waiting for transfers between devices, shift_fs(): lax.ppermute(a, 'fs', [(4 * z + y, 4 * ((z + dz) % 4) + (y + dy) % 4) for...  81 us
    all_to_all x1, waiting for transfers between devices, local(): lax.all_to_all(to_z, ('gr', 'fs'), 0, 0, axis_index_groups=[[4 * z + y fo...  49 us
    ppermute x20, starting transfers between devices, shift_fs(): lax.ppermute(a, 'fs', [(4 * z + y, 4 * ((z + dz) % 4) + (y + dy) % 4) for...  37.2 us
    pallas_call x16, Pallas kernels, call(): pl.pallas_call(run, out_shape=outs, in_specs=[pl.BlockSpec(memory_space=p...  23.2 us
    ppermute x15, waiting for transfers between devices, shift_tp(): lax.ppermute(a, 'tp', [(2 * x + c, 2 * ((x + dx) % 4) + (c + dc) % 2) for...  21.8 us
    ppermute x15, starting transfers between devices, shift_tp(): lax.ppermute(a, 'tp', [(2 * x + c, 2 * ((x + dx) % 4) + (c + dc) % 2) for...  21.4 us
    unnamed x31, local copies, waits for them, and re-layouts  10.4 us
    pallas_call x2, Pallas kernels, by_rows(): pl.pallas_call(run, grid=(n // tile,), in_specs=[pl.BlockSpec(memory_spac...  9.84 us
  transfers between devices with their start and end apart: 36, of which 17 were waited for; matrix products, arithmetic and copies ran while one was open for 2% of the time, Pallas kernels for 6%

profile of v2, /device:TPU:1, one launch (start us, length us, event | category | flops | bytes accessed | tf_op | source)
XLA Modules:
  0.0 261.8 jit_solution(13874532384615036407)
XLA Ops:
  6.0 2.1 collective-permute-start
  8.1 2.5 collective-permute-start.1
  11.7 3.0 %collective-permute-start.4 = (bf16[512,128]{1,0:T(8,128)(2,1)S(1)}, bf16[512,128]{1,0:T(8,128)(2,1)S(1)}, u32[]{:S(2)}, u32[]{:S(2)}) collective-permute-start(bf16[512,128]{1,0:T(8,128)(2,1)S(1)} %copy-done.9), channel_id=1, source_target_pairs={{0,64},{8,72},{16,80},{24,88},{32,96},{40,104},{48,112},{56,120},{... | collective-permute-start | bytes 393224 | tf_op jit(solution)/shard_map/ppermute | solution.py:273
  17.1 7.7 %collective-permute-start.5 = (bf16[512,128]{1,0:T(8,128)(2,1)S(1)}, bf16[512,128]{1,0:T(8,128)(2,1)S(1)}, u32[]{:S(2)}, u32[]{:S(2)}) collective-permute-start(bf16[512,128]{1,0:T(8,128)(2,1)S(1)} %copy-done.9), channel_id=1, source_target_pairs={{0,32},{8,40},{16,48},{24,56},{32,64},{40,72},{48,80},{56,88},{64,... | collective-permute-start | bytes 393224 | tf_op jit(solution)/shard_map/ppermute | solution.py:273
  24.7 6.2 %collective-permute-done.5.refs_5_ = bf16[512,128]{1,0:T(8,128)(2,1)S(1)} collective-permute-done((bf16[512,128]{1,0:T(8,128)(2,1)S(1)}, bf16[512,128]{1,0:T(8,128)(2,1)S(1)}, u32[]{:S(2)}, u32[]{:S(2)}) %collective-permute-start.5) | collective-permute-done | bytes 131104 | tf_op jit(solution)/shard_map/ppermute | solution.py:273
  30.9 3.9 %shard_map.103 = (bf16[2,192,512]{2,1,0:T(8,128)(2,1)S(1)}, bf16[2,192,512]{2,1,0:T(8,128)(2,1)}, bf16[2,192,512]{2,1,0:T(8,128)(2,1)}, bf16[2,192,512]{2,1,0:T(8,128)(2,1)}) custom-call(s32[5]{0:T(128)S(1)} %stack.23.refs_0_, s32[2,512]{1,0:T(2,128)S(1)} %bitcast.7, bf16[512,128]{1,0:T(8,128)(2,1)S(1)} %copy-done.9, ...), custom_call_target="tpu_custom_call" | custom-call | tf_op jit(solution)/shard_map/pallas_call | solution.py:30
  42.3 3.6 %shard_map.106.refs_5_.refs_1_ = f32[512,128]{1,0:T(8,128)S(1)} custom-call(s32[5]{0:T(128)S(1)} %stack.23.refs_0_, s32[512,2]{1,0:T(8,128)S(1)} %copy.12.refs_1_, f32[512,2]{1,0:T(8,128)S(1)} %copy-done.5, bf16[4,264,128]{2,1,0:T(8,128)(2,1)S(1)} %get-tuple-element.51.refs_3_.refs_1_), custom_call_target="tpu_custom_call" | custom-call | tf_op jit(solution)/shard_map/pallas_call | solution.py:30
  46.0 11.9 %collective-permute-done.7.refs_2_ = bf16[2,192,512]{2,1,0:T(8,128)(2,1)S(1)} collective-permute-done((bf16[2,192,512]{2,1,0:T(8,128)(2,1)}, bf16[2,192,512]{2,1,0:T(8,128)(2,1)S(1)}, u32[]{:S(2)}, u32[]{:S(2)}) %collective-permute-start.7) | collective-permute-done | bytes 393248 | tf_op jit(solution)/shard_map/ppermute | solution.py:267
  61.3 2.6 %collective-permute-start.15 = (bf16[4,264,128]{2,1,0:T(8,128)(2,1)S(1)}, bf16[4,264,128]{2,1,0:T(8,128)(2,1)S(1)}, u32[]{:S(2)}, u32[]{:S(2)}) collective-permute-start(bf16[4,264,128]{2,1,0:T(8,128)(2,1)S(1)} %get-tuple-element.56), channel_id=1, source_target_pairs={{0,16},{8,24},{16,0},{24,8},{32,48},{40,56},{48,32},{56,40},{64,80... | collective-permute-start | bytes 811016 | tf_op jit(solution)/shard_map/ppermute | solution.py:273
  65.6 3.4 %collective-permute-done.14.refs_2_ = bf16[4,264,128]{2,1,0:T(8,128)(2,1)S(1)} collective-permute-done((bf16[4,264,128]{2,1,0:T(8,128)(2,1)S(1)}, bf16[4,264,128]{2,1,0:T(8,128)(2,1)S(1)}, u32[]{:S(2)}, u32[]{:S(2)}) %collective-permute-start.14) | collective-permute-done | bytes 270368 | tf_op jit(solution)/shard_map/ppermute | solution.py:273
  69.1 6.9 %collective-permute-done.15.refs_3_ = bf16[4,264,128]{2,1,0:T(8,128)(2,1)S(1)} collective-permute-done((bf16[4,264,128]{2,1,0:T(8,128)(2,1)S(1)}, bf16[4,264,128]{2,1,0:T(8,128)(2,1)S(1)}, u32[]{:S(2)}, u32[]{:S(2)}) %collective-permute-start.15) | collective-permute-done | bytes 270368 | tf_op jit(solution)/shard_map/ppermute | solution.py:273
  78.1 5.5 %all-to-all-start = ((bf16[8,4,264,128]{3,2,1,0:T(8,128)(2,1)}), bf16[8,4,264,128]{3,2,1,0:T(8,128)(2,1)}, u32[]{:S(2)}, u32[]{:S(2)}) async-start(bf16[8,4,264,128]{3,2,1,0:T(8,128)(2,1)} %copy-done.2), calls=%async_computation | async-start | bytes 4325376 | tf_op jit(solution)/shard_map/all_to_all | solution.py:329
  84.3 2.9 %collective-permute-start.12 = (bf16[1536,512]{1,0:T(8,128)(2,1)S(1)}, bf16[1536,512]{1,0:T(8,128)(2,1)}, u32[]{:S(2)}, u32[]{:S(2)}) collective-permute-start(bf16[1536,512]{1,0:T(8,128)(2,1)S(1)} %shard_map.108.refs_5_.refs_1_), channel_id=1, source_target_pairs={{0,16},{8,24},{16,0},{24,8},{32,48},{40,56},{48,32},{56,40},{64,80... | collective-permute-start | bytes 4718600 | tf_op jit(solution)/shard_map/ppermute | solution.py:273
  87.7 49.0 %all-to-all-done.refs_1_ = bf16[8,4,264,128]{3,2,1,0:T(8,128)(2,1)} async-done(((bf16[8,4,264,128]{3,2,1,0:T(8,128)(2,1)}), bf16[8,4,264,128]{3,2,1,0:T(8,128)(2,1)}, u32[]{:S(2)}, u32[]{:S(2)}) %all-to-all-start) | async-done | bytes 2162720 | tf_op jit(solution)/shard_map/all_to_all | solution.py:329
  136.8 2.7 %shard_map.110 = (bf16[4,512,176]{2,1,0:T(8,128)(2,1)S(1)}, bf16[4,512,176]{2,1,0:T(8,128)(2,1)S(1)}, bf16[4,512,176]{2,1,0:T(8,128)(2,1)S(1)}) custom-call(s32[5]{0:T(128)S(1)} %stack.23.refs_0_, bf16[8,4,264,128]{3,2,1,0:T(8,128)(2,1)} %all-to-all-done.refs_1_), custom_call_target="tpu_custom_call" | custom-call | tf_op jit(solution)/shard_map/pallas_call | solution.py:30
  139.5 15.3 %collective-permute-done.12.refs_3_ = bf16[1536,512]{1,0:T(8,128)(2,1)} collective-permute-done((bf16[1536,512]{1,0:T(8,128)(2,1)S(1)}, bf16[1536,512]{1,0:T(8,128)(2,1)}, u32[]{:S(2)}, u32[]{:S(2)}) %collective-permute-start.12) | collective-permute-done | bytes 1572896 | tf_op jit(solution)/shard_map/ppermute | solution.py:273
  154.7 2.9 %shard_map.111 = (bf16[384,512]{1,0:T(8,128)(2,1)S(1)}, bf16[384,512]{1,0:T(8,128)(2,1)S(1)}, bf16[384,512]{1,0:T(8,128)(2,1)S(1)}, bf16[384,512]{1,0:T(8,128)(2,1)S(1)}) custom-call(s32[5]{0:T(128)S(1)} %stack.23.refs_0_, bf16[1536,512]{1,0:T(8,128)(2,1)} %copy-done, bf16[1536,512]{1,0:T(8,128)(2,1)} %collective-permute-done.11.refs_2_, ...), custom_call_target="tpu_custom_call" | custom-call | tf_op jit(solution)/shard_map/pallas_call | solution.py:198
  157.7 6.9 %shard_map.112 = (bf16[1152,512]{1,0:T(8,128)(2,1)S(1)}, bf16[1152,512]{1,0:T(8,128)(2,1)S(1)}, bf16[1152,512]{1,0:T(8,128)(2,1)}, bf16[1152,512]{1,0:T(8,128)(2,1)}) custom-call(s32[5]{0:T(128)S(1)} %stack.23.refs_0_, bf16[1536,512]{1,0:T(8,128)(2,1)} %copy-done, bf16[1536,512]{1,0:T(8,128)(2,1)} %collective-permute-done.11.refs_2_, ...), custom_call_target="tpu_custom_call" | custom-call | tf_op jit(solution)/shard_map/pallas_call | solution.py:198
  164.6 2.2 collective-permute-start.17
  168.3 2.2 collective-permute-start.20
  170.5 30.6 %collective-permute-done.19.refs_2_ = bf16[384,512]{1,0:T(8,128)(2,1)S(1)} collective-permute-done((bf16[384,512]{1,0:T(8,128)(2,1)S(1)}, bf16[384,512]{1,0:T(8,128)(2,1)S(1)}, u32[]{:S(2)}, u32[]{:S(2)}) %collective-permute-start.19) | collective-permute-done | bytes 393248 | tf_op jit(solution)/shard_map/ppermute | solution.py:273
  207.1 2.7 %collective-permute-start.24 = (bf16[384,256]{1,0:T(8,128)(2,1)S(1)}, bf16[384,256]{1,0:T(8,128)(2,1)S(1)}, u32[]{:S(2)}, u32[]{:S(2)}) collective-permute-start(bf16[384,256]{1,0:T(8,128)(2,1)S(1)} %get-tuple-element.73), channel_id=1, source_target_pairs={{0,24},{8,0},{16,8},{24,16},{32,56},{40,32},{48,40},{56,48},{64,88... | collective-permute-start | bytes 589832 | tf_op jit(solution)/shard_map/ppermute | solution.py:273
  209.7 13.1 %collective-permute-done.24.refs_5_ = bf16[384,256]{1,0:T(8,128)(2,1)S(1)} collective-permute-done((bf16[384,256]{1,0:T(8,128)(2,1)S(1)}, bf16[384,256]{1,0:T(8,128)(2,1)S(1)}, u32[]{:S(2)}, u32[]{:S(2)}) %collective-permute-start.24) | collective-permute-done | bytes 196640 | tf_op jit(solution)/shard_map/ppermute | solution.py:273
  225.6 3.9 %collective-permute-start.31 = (bf16[192,512]{1,0:T(8,128)(2,1)S(1)}, bf16[192,512]{1,0:T(8,128)(2,1)S(1)}, u32[]{:S(2)}, u32[]{:S(2)}) collective-permute-start(bf16[192,512]{1,0:T(8,128)(2,1)S(1)} %get-tuple-element.81), channel_id=1, source_target_pairs={{0,5},{1,4},{2,7},{3,6},{4,1},{5,0},{6,3},{7,2},{8,13},{9,12},{10,... | collective-permute-start | bytes 589832 | tf_op jit(solution)/shard_map/ppermute | solution.py:267
  229.5 2.3 collective-permute-start.30
  233.0 2.1 collective-permute-start.27
  235.1 2.2 collective-permute-start.29
  237.3 3.5 %collective-permute-done.30.refs_2_ = bf16[192,512]{1,0:T(8,128)(2,1)S(1)} collective-permute-done((bf16[192,512]{1,0:T(8,128)(2,1)S(1)}, bf16[192,512]{1,0:T(8,128)(2,1)S(1)}, u32[]{:S(2)}, u32[]{:S(2)}) %collective-permute-start.30) | collective-permute-done | bytes 196640 | tf_op jit(solution)/shard_map/ppermute | solution.py:267
  243.6 4.2 %collective-permute-done.28.refs_5_ = bf16[192,512]{1,0:T(8,128)(2,1)S(1)} collective-permute-done((bf16[192,512]{1,0:T(8,128)(2,1)S(1)}, bf16[192,512]{1,0:T(8,128)(2,1)S(1)}, u32[]{:S(2)}, u32[]{:S(2)}) %collective-permute-start.28) | collective-permute-done | bytes 196640 | tf_op jit(solution)/shard_map/ppermute | solution.py:267
  249.5 2.4 collective-permute-start.32
  253.1 2.1 collective-permute-start.34
  256.4 2.2 copy.15
  (92 shorter events, 46.1 us)
Async XLA Ops:
  6.0 28.8 %collective-permute-start = (bf16[2,2,264,128]{3,2,1,0:T(8,128)(2,1)S(1)}, bf16[2,2,264,128]{3,2,1,0:T(8,128)(2,1)S(1)}, u32[]{:S(2)}, u32[]{:S(2)}) collective-permute-start(bf16[2,2,264,128]{3,2,1,0:T(8,128)(2,1)S(1)} %get-tuple-element.47), channel_id=1, source_target_pairs={{0,2},{1,3},{2,4},{3,5},{4,6},{5,7},{6,0},{7,1},{8,10},{9,11},{10,... | collective-permute-start | bytes 811016 | tf_op jit(solution)/shard_map/ppermute | solution.py:267
  8.1 26.7 %collective-permute-start.1 = (bf16[2,2,264,128]{3,2,1,0:T(8,128)(2,1)S(1)}, bf16[2,2,264,128]{3,2,1,0:T(8,128)(2,1)S(1)}, u32[]{:S(2)}, u32[]{:S(2)}) collective-permute-start(bf16[2,2,264,128]{3,2,1,0:T(8,128)(2,1)S(1)} %get-tuple-element.48), channel_id=1, source_target_pairs={{0,4},{1,5},{2,6},{3,7},{4,0},{5,1},{6,2},{7,3},{8,12},{9,13},{10,... | collective-permute-start | bytes 811016 | tf_op jit(solution)/shard_map/ppermute | solution.py:267
  10.6 24.3 %collective-permute-start.2 = (bf16[2,2,264,128]{3,2,1,0:T(8,128)(2,1)S(1)}, bf16[2,2,264,128]{3,2,1,0:T(8,128)(2,1)S(1)}, u32[]{:S(2)}, u32[]{:S(2)}) collective-permute-start(bf16[2,2,264,128]{3,2,1,0:T(8,128)(2,1)S(1)} %get-tuple-element.49), channel_id=1, source_target_pairs={{0,6},{1,7},{2,0},{3,1},{4,2},{5,3},{6,4},{7,5},{8,14},{9,15},{10,... | collective-permute-start | bytes 811016 | tf_op jit(solution)/shard_map/ppermute | solution.py:267
  14.7 10.0 %collective-permute-start.3 = (bf16[512,128]{1,0:T(8,128)(2,1)S(1)}, bf16[512,128]{1,0:T(8,128)(2,1)S(1)}, u32[]{:S(2)}, u32[]{:S(2)}) collective-permute-start(bf16[512,128]{1,0:T(8,128)(2,1)S(1)} %copy-done.9), channel_id=1, source_target_pairs={{0,96},{8,104},{16,112},{24,120},{32,0},{40,8},{48,16},{56,24},{64... | collective-permute-start | bytes 393224 | tf_op jit(solution)/shard_map/ppermute | solution.py:273
  17.1 13.8 %collective-permute-start.5 = (bf16[512,128]{1,0:T(8,128)(2,1)S(1)}, bf16[512,128]{1,0:T(8,128)(2,1)S(1)}, u32[]{:S(2)}, u32[]{:S(2)}) collective-permute-start(bf16[512,128]{1,0:T(8,128)(2,1)S(1)} %copy-done.9), channel_id=1, source_target_pairs={{0,32},{8,40},{16,48},{24,56},{32,64},{40,72},{48,80},{56,88},{64,... | collective-permute-start | bytes 393224 | tf_op jit(solution)/shard_map/ppermute | solution.py:273
  37.3 20.5 %collective-permute-start.7 = (bf16[2,192,512]{2,1,0:T(8,128)(2,1)}, bf16[2,192,512]{2,1,0:T(8,128)(2,1)S(1)}, u32[]{:S(2)}, u32[]{:S(2)}) collective-permute-start(bf16[2,192,512]{2,1,0:T(8,128)(2,1)} %get-tuple-element.52), channel_id=1, source_target_pairs={{0,2},{1,3},{2,4},{3,5},{4,6},{5,7},{6,0},{7,1},{8,10},{9,11},{10,... | collective-permute-start | bytes 1179656 | tf_op jit(solution)/shard_map/ppermute | solution.py:267
  37.6 20.2 %collective-permute-start.8 = (bf16[2,192,512]{2,1,0:T(8,128)(2,1)}, bf16[2,192,512]{2,1,0:T(8,128)(2,1)S(1)}, u32[]{:S(2)}, u32[]{:S(2)}) collective-permute-start(bf16[2,192,512]{2,1,0:T(8,128)(2,1)} %get-tuple-element.53), channel_id=1, source_target_pairs={{0,4},{1,5},{2,6},{3,7},{4,0},{5,1},{6,2},{7,3},{8,12},{9,13},{10,... | collective-permute-start | bytes 1179656 | tf_op jit(solution)/shard_map/ppermute | solution.py:267
  38.5 19.7 %collective-permute-start.9 = (bf16[2,192,512]{2,1,0:T(8,128)(2,1)}, bf16[2,192,512]{2,1,0:T(8,128)(2,1)S(1)}, u32[]{:S(2)}, u32[]{:S(2)}) collective-permute-start(bf16[2,192,512]{2,1,0:T(8,128)(2,1)} %get-tuple-element.54), channel_id=1, source_target_pairs={{0,6},{1,7},{2,0},{3,1},{4,2},{5,3},{6,4},{7,5},{8,14},{9,15},{10,... | collective-permute-start | bytes 1179656 | tf_op jit(solution)/shard_map/ppermute | solution.py:267
  60.0 9.1 %collective-permute-start.14 = (bf16[4,264,128]{2,1,0:T(8,128)(2,1)S(1)}, bf16[4,264,128]{2,1,0:T(8,128)(2,1)S(1)}, u32[]{:S(2)}, u32[]{:S(2)}) collective-permute-start(bf16[4,264,128]{2,1,0:T(8,128)(2,1)S(1)} %get-tuple-element.55), channel_id=1, source_target_pairs={{0,8},{8,16},{16,24},{24,0},{32,40},{40,48},{48,56},{56,32},{64,72... | collective-permute-start | bytes 811016 | tf_op jit(solution)/shard_map/ppermute | solution.py:273
  61.3 14.7 %collective-permute-start.15 = (bf16[4,264,128]{2,1,0:T(8,128)(2,1)S(1)}, bf16[4,264,128]{2,1,0:T(8,128)(2,1)S(1)}, u32[]{:S(2)}, u32[]{:S(2)}) collective-permute-start(bf16[4,264,128]{2,1,0:T(8,128)(2,1)S(1)} %get-tuple-element.56), channel_id=1, source_target_pairs={{0,16},{8,24},{16,0},{24,8},{32,48},{40,56},{48,32},{56,40},{64,80... | collective-permute-start | bytes 811016 | tf_op jit(solution)/shard_map/ppermute | solution.py:273
  63.9 12.1 %collective-permute-start.16 = (bf16[4,264,128]{2,1,0:T(8,128)(2,1)S(1)}, bf16[4,264,128]{2,1,0:T(8,128)(2,1)S(1)}, u32[]{:S(2)}, u32[]{:S(2)}) collective-permute-start(bf16[4,264,128]{2,1,0:T(8,128)(2,1)S(1)} %get-tuple-element.57), channel_id=1, source_target_pairs={{0,24},{8,0},{16,8},{24,16},{32,56},{40,32},{48,40},{56,48},{64,88... | collective-permute-start | bytes 811016 | tf_op jit(solution)/shard_map/ppermute | solution.py:273
  78.1 58.6 %all-to-all-start = ((bf16[8,4,264,128]{3,2,1,0:T(8,128)(2,1)}), bf16[8,4,264,128]{3,2,1,0:T(8,128)(2,1)}, u32[]{:S(2)}, u32[]{:S(2)}) async-start(bf16[8,4,264,128]{3,2,1,0:T(8,128)(2,1)} %copy-done.2), calls=%async_computation | async-start | bytes 4325376 | tf_op jit(solution)/shard_map/all_to_all | solution.py:329
  83.6 55.8 %collective-permute-start.13 = (bf16[1536,512]{1,0:T(8,128)(2,1)S(1)}, bf16[1536,512]{1,0:T(8,128)(2,1)S(1)}, u32[]{:S(2)}, u32[]{:S(2)}) collective-permute-start(bf16[1536,512]{1,0:T(8,128)(2,1)S(1)} %shard_map.108.refs_5_.refs_1_), channel_id=1, source_target_pairs={{0,8},{8,16},{16,24},{24,0},{32,40},{40,48},{48,56},{56,32},{64,72... | collective-permute-start | bytes 4718600 | tf_op jit(solution)/shard_map/ppermute | solution.py:273
  84.3 70.4 %collective-permute-start.12 = (bf16[1536,512]{1,0:T(8,128)(2,1)S(1)}, bf16[1536,512]{1,0:T(8,128)(2,1)}, u32[]{:S(2)}, u32[]{:S(2)}) collective-permute-start(bf16[1536,512]{1,0:T(8,128)(2,1)S(1)} %shard_map.108.refs_5_.refs_1_), channel_id=1, source_target_pairs={{0,16},{8,24},{16,0},{24,8},{32,48},{40,56},{48,32},{56,40},{64,80... | collective-permute-start | bytes 4718600 | tf_op jit(solution)/shard_map/ppermute | solution.py:273
  87.2 67.5 %collective-permute-start.11 = (bf16[1536,512]{1,0:T(8,128)(2,1)S(1)}, bf16[1536,512]{1,0:T(8,128)(2,1)}, u32[]{:S(2)}, u32[]{:S(2)}) collective-permute-start(bf16[1536,512]{1,0:T(8,128)(2,1)S(1)} %shard_map.108.refs_5_.refs_1_), channel_id=1, source_target_pairs={{0,24},{8,0},{16,8},{24,16},{32,56},{40,32},{48,40},{56,48},{64,88... | collective-permute-start | bytes 4718600 | tf_op jit(solution)/shard_map/ppermute | solution.py:273
  164.6 39.9 %collective-permute-start.17 = (bf16[1152,512]{1,0:T(8,128)(2,1)S(1)}, bf16[1152,512]{1,0:T(8,128)(2,1)S(1)}, u32[]{:S(2)}, u32[]{:S(2)}) collective-permute-start(bf16[1152,512]{1,0:T(8,128)(2,1)S(1)} %get-tuple-element.63), channel_id=1, source_target_pairs={{0,8},{8,16},{16,24},{24,0},{32,40},{40,48},{48,56},{56,32},{64,72... | collective-permute-start | bytes 3538952 | tf_op jit(solution)/shard_map/ppermute | solution.py:273
  166.8 37.6 %collective-permute-start.18 = (bf16[1152,512]{1,0:T(8,128)(2,1)}, bf16[1152,512]{1,0:T(8,128)(2,1)S(1)}, u32[]{:S(2)}, u32[]{:S(2)}) collective-permute-start(bf16[1152,512]{1,0:T(8,128)(2,1)} %get-tuple-element.64), channel_id=1, source_target_pairs={{0,24},{8,0},{16,8},{24,16},{32,56},{40,32},{48,40},{56,48},{64,88... | collective-permute-start | bytes 3538952 | tf_op jit(solution)/shard_map/ppermute | solution.py:273
  167.8 33.3 %collective-permute-start.19 = (bf16[384,512]{1,0:T(8,128)(2,1)S(1)}, bf16[384,512]{1,0:T(8,128)(2,1)S(1)}, u32[]{:S(2)}, u32[]{:S(2)}) collective-permute-start(bf16[384,512]{1,0:T(8,128)(2,1)S(1)} %get-tuple-element.67), channel_id=1, source_target_pairs={{0,8},{8,16},{16,24},{24,0},{32,40},{40,48},{48,56},{56,32},{64,72... | collective-permute-start | bytes 1179656 | tf_op jit(solution)/shard_map/ppermute | solution.py:273
  168.3 33.9 %collective-permute-start.20 = (bf16[384,512]{1,0:T(8,128)(2,1)S(1)}, bf16[384,512]{1,0:T(8,128)(2,1)S(1)}, u32[]{:S(2)}, u32[]{:S(2)}) collective-permute-start(bf16[384,512]{1,0:T(8,128)(2,1)S(1)} %get-tuple-element.68), channel_id=1, source_target_pairs={{0,24},{8,0},{16,8},{24,16},{32,56},{40,32},{48,40},{56,48},{64,88... | collective-permute-start | bytes 1179656 | tf_op jit(solution)/shard_map/ppermute | solution.py:273
  205.3 26.6 %collective-permute-start.22 = (bf16[1152,256]{1,0:T(8,128)(2,1)S(1)}, bf16[1152,256]{1,0:T(8,128)(2,1)S(1)}, u32[]{:S(2)}, u32[]{:S(2)}) collective-permute-start(bf16[1152,256]{1,0:T(8,128)(2,1)S(1)} %get-tuple-element.72), channel_id=1, source_target_pairs={{0,24},{8,0},{16,8},{24,16},{32,56},{40,32},{48,40},{56,48},{64,88... | collective-permute-start | bytes 1769480 | tf_op jit(solution)/shard_map/ppermute | solution.py:273
  207.1 24.8 %collective-permute-start.21 = (bf16[1152,256]{1,0:T(8,128)(2,1)S(1)}, bf16[1152,256]{1,0:T(8,128)(2,1)S(1)}, u32[]{:S(2)}, u32[]{:S(2)}) collective-permute-start(bf16[1152,256]{1,0:T(8,128)(2,1)S(1)} %get-tuple-element.71.refs_6_), channel_id=1, source_target_pairs={{0,8},{8,16},{16,24},{24,0},{32,40},{40,48},{48,56},{56,32},{64,72... | collective-permute-start | bytes 1769480 | tf_op jit(solution)/shard_map/ppermute | solution.py:273
  207.1 15.8 %collective-permute-start.24 = (bf16[384,256]{1,0:T(8,128)(2,1)S(1)}, bf16[384,256]{1,0:T(8,128)(2,1)S(1)}, u32[]{:S(2)}, u32[]{:S(2)}) collective-permute-start(bf16[384,256]{1,0:T(8,128)(2,1)S(1)} %get-tuple-element.73), channel_id=1, source_target_pairs={{0,24},{8,0},{16,8},{24,16},{32,56},{40,32},{48,40},{56,48},{64,88... | collective-permute-start | bytes 589832 | tf_op jit(solution)/shard_map/ppermute | solution.py:273
  209.7 15.2 %collective-permute-start.23 = (bf16[384,256]{1,0:T(8,128)(2,1)S(1)}, bf16[384,256]{1,0:T(8,128)(2,1)S(1)}, u32[]{:S(2)}, u32[]{:S(2)}) collective-permute-start(bf16[384,256]{1,0:T(8,128)(2,1)S(1)} %get-tuple-element.69.refs_4_), channel_id=1, source_target_pairs={{0,8},{8,16},{16,24},{24,0},{32,40},{40,48},{48,56},{56,32},{64,72... | collective-permute-start | bytes 589832 | tf_op jit(solution)/shard_map/ppermute | solution.py:273
  225.6 9.5 %collective-permute-start.31 = (bf16[192,512]{1,0:T(8,128)(2,1)S(1)}, bf16[192,512]{1,0:T(8,128)(2,1)S(1)}, u32[]{:S(2)}, u32[]{:S(2)}) collective-permute-start(bf16[192,512]{1,0:T(8,128)(2,1)S(1)} %get-tuple-element.81), channel_id=1, source_target_pairs={{0,5},{1,4},{2,7},{3,6},{4,1},{5,0},{6,3},{7,2},{8,13},{9,12},{10,... | collective-permute-start | bytes 589832 | tf_op jit(solution)/shard_map/ppermute | solution.py:267
  229.5 11.2 %collective-permute-start.30 = (bf16[192,512]{1,0:T(8,128)(2,1)S(1)}, bf16[192,512]{1,0:T(8,128)(2,1)S(1)}, u32[]{:S(2)}, u32[]{:S(2)}) collective-permute-start(bf16[192,512]{1,0:T(8,128)(2,1)S(1)} %get-tuple-element.74.refs_6_), channel_id=1, source_target_pairs={{0,4},{1,5},{2,6},{3,7},{4,0},{5,1},{6,2},{7,3},{8,12},{9,13},{10,... | collective-permute-start | bytes 589832 | tf_op jit(solution)/shard_map/ppermute | solution.py:267
  232.8 10.8 %collective-permute-start.26 = (bf16[192,512]{1,0:T(8,128)(2,1)S(1)}, bf16[192,512]{1,0:T(8,128)(2,1)S(1)}, u32[]{:S(2)}, u32[]{:S(2)}) collective-permute-start(bf16[192,512]{1,0:T(8,128)(2,1)S(1)} %get-tuple-element.76), channel_id=1, source_target_pairs={{0,3},{1,2},{2,5},{3,4},{4,7},{5,6},{6,1},{7,0},{8,11},{9,10},{10,... | collective-permute-start | bytes 589832 | tf_op jit(solution)/shard_map/ppermute | solution.py:267
  233.0 10.6 %collective-permute-start.27 = (bf16[192,512]{1,0:T(8,128)(2,1)S(1)}, bf16[192,512]{1,0:T(8,128)(2,1)S(1)}, u32[]{:S(2)}, u32[]{:S(2)}) collective-permute-start(bf16[192,512]{1,0:T(8,128)(2,1)S(1)} %get-tuple-element.77), channel_id=1, source_target_pairs={{0,6},{1,7},{2,0},{3,1},{4,2},{5,3},{6,4},{7,5},{8,14},{9,15},{10,... | collective-permute-start | bytes 589832 | tf_op jit(solution)/shard_map/ppermute | solution.py:267
  235.1 12.8 %collective-permute-start.28 = (bf16[192,512]{1,0:T(8,128)(2,1)S(1)}, bf16[192,512]{1,0:T(8,128)(2,1)S(1)}, u32[]{:S(2)}, u32[]{:S(2)}) collective-permute-start(bf16[192,512]{1,0:T(8,128)(2,1)S(1)} %get-tuple-element.78), channel_id=1, source_target_pairs={{0,2},{1,3},{2,4},{3,5},{4,6},{5,7},{6,0},{7,1},{8,10},{9,11},{10,... | collective-permute-start | bytes 589832 | tf_op jit(solution)/shard_map/ppermute | solution.py:267
  235.1 12.7 %collective-permute-start.29 = (bf16[192,512]{1,0:T(8,128)(2,1)S(1)}, bf16[192,512]{1,0:T(8,128)(2,1)S(1)}, u32[]{:S(2)}, u32[]{:S(2)}) collective-permute-start(bf16[192,512]{1,0:T(8,128)(2,1)S(1)} %get-tuple-element.79), channel_id=1, source_target_pairs={{0,1},{1,0},{2,3},{3,2},{4,5},{5,4},{6,7},{7,6},{8,9},{9,8},{10,11... | collective-permute-start | bytes 589832 | tf_op jit(solution)/shard_map/ppermute | solution.py:267
  249.5 11.1 %collective-permute-start.32 = (bf16[512,128]{1,0:T(8,128)(2,1)S(1)}, bf16[512,128]{1,0:T(8,128)(2,1)S(1)}, u32[]{:S(2)}, u32[]{:S(2)}) collective-permute-start(bf16[512,128]{1,0:T(8,128)(2,1)S(1)} %get-tuple-element.83), channel_id=1, source_target_pairs={{0,64},{8,72},{16,80},{24,88},{32,96},{40,104},{48,112},{56,120},{... | collective-permute-start | bytes 393224 | tf_op jit(solution)/shard_map/ppermute | solution.py:273
  251.9 8.7 %collective-permute-start.33 = (bf16[512,128]{1,0:T(8,128)(2,1)S(1)}, bf16[512,128]{1,0:T(8,128)(2,1)S(1)}, u32[]{:S(2)}, u32[]{:S(2)}) collective-permute-start(bf16[512,128]{1,0:T(8,128)(2,1)S(1)} %get-tuple-element.84), channel_id=1, source_target_pairs={{0,32},{8,40},{16,48},{24,56},{32,64},{40,72},{48,80},{56,88},{64,... | collective-permute-start | bytes 393224 | tf_op jit(solution)/shard_map/ppermute | solution.py:273
  253.1 8.0 %collective-permute-start.34 = (bf16[512,128]{1,0:T(8,128)(2,1)S(1)}, bf16[512,128]{1,0:T(8,128)(2,1)S(1)}, u32[]{:S(2)}, u32[]{:S(2)}) collective-permute-start(bf16[512,128]{1,0:T(8,128)(2,1)S(1)} %get-tuple-element.85), channel_id=1, source_target_pairs={{0,96},{8,104},{16,112},{24,120},{32,0},{40,8},{48,16},{56,24},{64... | collective-permute-start | bytes 393224 | tf_op jit(solution)/shard_map/ppermute | solution.py:273
  (17 other events, 190.2 us)

commit v3 on v2

--- a/solution.py
+++ b/solution.py
@@ -14,7 +14,7 @@
 PACK_GU, PACK_D = 176, 88
 PACK = PACK_GU + PACK_D
 TRIPS = ((4, 5), (3, 7, 2, 6, 1, 0))
-ROWS = CAP * 8
+FAR = TRIPS[0] + TRIPS[1][:5]
 
 
 def spec_vmem():
@@ -128,7 +128,7 @@
 
 
 def dispatch_body(where, routes, *refs):
-    toks, outs, table, made = refs[:4], refs[4:8], refs[8], refs[9]
+    toks, outs, near, table, made = refs[:4], refs[4:8], refs[8], refs[9], refs[10]
     expert = lax.broadcasted_iota(jnp.int32, (8, TOK), 0)
     named = (routes[0:1, :] == expert) | (routes[1:2, :] == expert)
     before = (
@@ -145,22 +145,44 @@
         pick = (slot == table[pl.ds(peer(where, r), 1), :]).astype(F32).astype(BF)
         made[r] = jnp.dot(pick, x, preferred_element_type=F32).astype(BF)
 
+    near[...] = made[0]
     for r in range(8):
         outs[r // 2][r % 2] = made[r]
 
 
 def rows_body(where, *refs):
     got, swapped, out = refs[:4], refs[4], refs[5]
-    for i, r in enumerate(TRIPS[0] + TRIPS[1]):
+    for i, r in enumerate(FAR):
         part = swapped[r // 2] if r % 2 else got[r // 2][0]
         out[CAP * i : CAP * i + CAP, :] = part
 
 
-def ffn_body(where, *refs):
-    xs, (wg, wu, wd), (own, plus, minus, keep) = refs[:4], refs[4:7], refs[7:]
+def first_ffn_body(where, *refs):
+    ffn_of([x[...] for x in refs[:4]], *refs[4:])
+
+
+def second_ffn_body(where, *refs):
+    tiles, last, near, held = refs[:4], refs[4:8], refs[8:12], refs[-1]
+    at_end = pl.program_id(0) == 2
+
+    @pl.when(at_end)
+    def _():
+        for q in range(4):
+            held[q, 0:CAP, :] = last[q][...]
+            held[q, CAP : 2 * CAP, :] = near[q][...]
+
+    @pl.when(jnp.logical_not(at_end))
+    def _():
+        for q in range(4):
+            held[q] = tiles[q][...]
+
+    ffn_of([held[q] for q in range(4)], *refs[12:-1])
+
+
+def ffn_of(xs, wg, wu, wd, own, plus, minus, keep):
     g = u = total = None
     for q in range(4):
-        x = xs[q][...]
+        x = xs[q]
         xf = x.astype(F32)
         dg = jnp.dot(x, wg[q], preferred_element_type=F32)
         du = jnp.dot(x, wu[q], preferred_element_type=F32)
@@ -187,10 +209,18 @@
     own[:, 256:512] = out(0, 1)
 
 
-def by_rows(body, where, tiled, whole, widths, n, first_tile, after=()):
-    tile = 2 * CAP
-    rows = lambda w, first=0: pl.BlockSpec((tile, w), lambda i: (i + first, 0))
-    m = len(tiled) + len(whole) + 1
+def ffn(t, where, rows, near, weights, after=()):
+    tile, n = 2 * CAP, CAP * len(TRIPS[t])
+    out = pl.BlockSpec((tile, 512), lambda i: (i, 0))
+    if t == 0:
+        body, tiled = first_ffn_body, rows
+        specs = [out] * 4
+    else:
+        body, tiled = second_ffn_body, (*rows, *rows, *near)
+        specs = [pl.BlockSpec((tile, 512), lambda i: (jnp.minimum(i, 1) + 1, 0))] * 4
+        specs += [pl.BlockSpec((CAP, 512), lambda i: (6, 0))] * 4
+        specs += [pl.BlockSpec((CAP, 512), lambda i: (0, 0))] * 4
+    m = 1 + len(tiled) + len(weights)
 
     def run(*refs):
         body(*refs[:m], *refs[m + len(after) :])
@@ -199,13 +229,14 @@
         run,
         grid=(n // tile,),
         in_specs=[pl.BlockSpec(memory_space=pltpu.SMEM)]
-        + [rows(a.shape[1], first_tile) for a in tiled]
-        + [pl.BlockSpec(a.shape, lambda i: (0, 0, 0)) for a in whole]
+        + specs
+        + [pl.BlockSpec(a.shape, lambda i: (0, 0, 0)) for a in weights]
         + [pl.BlockSpec(memory_space=pl.ANY)] * len(after),
-        out_specs=[rows(w) for w in widths],
-        out_shape=[sds(n, w) for w in widths],
+        out_specs=[out] * 4,
+        out_shape=[sds(n, 512)] * 4,
+        scratch_shapes=[pltpu.VMEM((4, tile, 512), BF)] if t else [],
         compiler_params=pltpu.CompilerParams(vmem_limit_bytes=48 * 2**20),
-    )(where, *tiled, *whole, *after)
+    )(where, *tiled, *weights, *after)
 
 
 def add_body(where, keep, from_left, from_right, out0, out1):
@@ -223,24 +254,30 @@
 
 
 def plan_body(where, routes, weight, out):
-    r0, r1 = routes[:, 0:1], routes[:, 1:2]
-    w0, w1 = weight[:, 0:1], weight[:, 1:2]
     expert = lax.broadcasted_iota(jnp.int32, (TOK, 128), 1)
-    one0, one1 = (r0 == expert).astype(F32), (r1 == expert).astype(F32)
-    before = (
-        lax.broadcasted_iota(jnp.int32, (TOK, TOK), 1)
-        < lax.broadcasted_iota(jnp.int32, (TOK, TOK), 0)
-    ).astype(F32).astype(BF)
-    count = jnp.dot(before, (one0 + one1).astype(BF), preferred_element_type=F32)
-    slot0 = jnp.sum(one0 * count, axis=1, keepdims=True)
-    slot1 = jnp.sum(one1 * count, axis=1, keepdims=True)
-    table = jnp.zeros((TOK, 128), F32)
-    for r in range(8):
-        e = peer(where, r)
-        at = jnp.where(r0 == e, slot0, jnp.where(r1 == e, slot1, -1.0))
-        w = jnp.where(r0 == e, w0, jnp.where(r1 == e, w1, 0.0))
-        table = jnp.where(expert == r, at, jnp.where(expert == 8 + r, w, table))
-    out[...] = table
+    named = (routes[:, 0:1] == expert) | (routes[:, 1:2] == expert)
+    named = named.astype(F32).astype(BF)
+    lane = lax.broadcasted_iota(jnp.int32, (128, 128), 1)
+
+    @pl.loop(0, 4)
+    def _(t):
+        at = pl.ds(pl.multiple_of(t * 128, 128), 128)
+        r0, r1 = routes[at, 0:1], routes[at, 1:2]
+        w0, w1 = weight[at, 0:1], weight[at, 1:2]
+        before = (
+            lax.broadcasted_iota(jnp.int32, (128, TOK), 1)
+            < lax.broadcasted_iota(jnp.int32, (128, TOK), 0) + t * 128
+        ).astype(F32).astype(BF)
+        count = jnp.dot(before, named, preferred_element_type=F32)
+        slot0 = jnp.sum(jnp.where(r0 == lane, count, 0.0), axis=1, keepdims=True)
+        slot1 = jnp.sum(jnp.where(r1 == lane, count, 0.0), axis=1, keepdims=True)
+        table = jnp.zeros((128, 128), F32)
+        for r in range(8):
+            e = peer(where, r)
+            slot = jnp.where(r0 == e, slot0, jnp.where(r1 == e, slot1, -1.0))
+            w = jnp.where(r0 == e, w0, jnp.where(r1 == e, w1, 0.0))
+            table = jnp.where(lane == r, slot, jnp.where(lane == 8 + r, w, table))
+        out[at, :] = table
 
 
 def combine_body(relative, plan, *refs):
@@ -299,14 +336,20 @@
         return mine, shift_tp(mine, 1)
 
     w_x = over_x(packed)
-    slots = call(
+    *slots, near = call(
         dispatch_body,
-        [sds(2, CAP, 512)] * 4,
+        [sds(2, CAP, 512)] * 4 + [sds(CAP, 512)],
         (where, routes.T, *by_k),
         scratch=[pltpu.VMEM((8, TOK), F32), pltpu.VMEM((8, CAP, 512), BF)],
         after=(packed[0],),
     )
     t_x = over_x(slots)
+
+    def over_y(own):
+        two, plus, minus = shift_fs(own, 0, 2), shift_fs(own, 0, 1), shift_fs(own, 0, -1)
+        return own, minus, two, plus
+
+    near = over_y(near)
     _, w_core = swap(w_x, (slots[0],))
 
     to_y = call(
@@ -322,9 +365,8 @@
         plan_body, [sds(TOK, 128, dtype=F32)], (where, routes, route_weight), after=(to_y[0],)
     )[0]
     _, t_core = swap(t_x, (plan,))
-    own = call(rows_body, [sds(ROWS, 512)], (where, *t_x, t_core))[0]
-    two, plus, minus = shift_fs(own, 0, 2), shift_fs(own, 0, 1), shift_fs(own, 0, -1)
-    rows = (own, minus, two, plus)
+    own = call(rows_body, [sds(CAP * len(FAR), 512)], (where, *t_x, t_core))[0]
+    rows = over_y(own)
     to_z = call(by_z_body, [sds(8, 4, PACK, 128)], (where, *w_y), after=(own,))[0]
     w_z = lax.all_to_all(
         to_z,
@@ -335,11 +377,8 @@
         tiled=True,
     )
     ordered = call(unpack_body, [sds(4, 512, F)] * 3, (where, w_z))
-    made = []
-    for t in range(2):
-        last = [m[0] for m in made[-1:]]
-        n = CAP * len(TRIPS[t])
-        made.append(by_rows(ffn_body, where, rows, ordered, (512,) * 4, n, t, after=last))
+    made = [ffn(0, where, rows, near, ordered)]
+    made.append(ffn(1, where, rows, near, ordered, (made[0][0],)))
 
     def out_y(t):
         return shift_fs(made[t][1], 0, 1), shift_fs(made[t][2], 0, -1)

time: 265 us -> 263 us (level)
  waiting for transfers between devices: 152 us -> 146 us
  Pallas kernels: 33 us -> 36.7 us
    all_to_all x1, waiting for transfers between devices: 49 us -> 18.6 us  [local(): lax.all_to_all(to_z, ('gr', 'fs'), 0, 0, axis_index_groups=[[4 * z + y fo...]
    ppermute x20 -> x23, waiting for transfers between devices: 81 us -> 106 us  [shift_fs(): lax.ppermute(a, 'fs', [(4 * z + y, 4 * ((z + dz) % 4) + (y + dy) % 4) for...]
    pallas_call x16, Pallas kernels: 23.2 us -> 25.9 us  [call(): pl.pallas_call(run, out_shape=outs, in_specs=[pl.BlockSpec(memory_space=p...]
    unnamed x31 -> x33, local copies, waits for them, and re-layouts: 10.4 us -> 8.48 us
    ppermute x20 -> x23, starting transfers between devices: 37.2 us -> 38.8 us  [shift_fs(): lax.ppermute(a, 'fs', [(4 * z + y, 4 * ((z + dz) % 4) + (y + dy) % 4) for...]
  transfers between devices with their start and end apart: 36 -> 39, of which waited for: 17 -> 19; matrix products, arithmetic and copies ran while one was open for 2% -> 1% of each run, Pallas kernels for 6% -> 8%
where the time goes in v3:
time: 263 us; the launch traced here: 261 us
  waiting for transfers between devices  146 us (56%)
  starting transfers between devices  66.2 us (25%)
  Pallas kernels  36.7 us (14%)
  local copies, waits for them, and re-layouts  9.34 us (4%)
    ppermute x23, waiting for transfers between devices, shift_fs(): lax.ppermute(a, 'fs', [(4 * z + y, 4 * ((z + dz) % 4) + (y + dy) % 4) for...  106 us
    ppermute x23, starting transfers between devices, shift_fs(): lax.ppermute(a, 'fs', [(4 * z + y, 4 * ((z + dz) % 4) + (y + dy) % 4) for...  38.8 us
    pallas_call x16, Pallas kernels, call(): pl.pallas_call(run, out_shape=outs, in_specs=[pl.BlockSpec(memory_space=p...  25.9 us
    ppermute x15, starting transfers between devices, shift_tp(): lax.ppermute(a, 'tp', [(2 * x + c, 2 * ((x + dx) % 4) + (c + dc) % 2) for...  21.9 us
    ppermute x15, waiting for transfers between devices, shift_tp(): lax.ppermute(a, 'tp', [(2 * x + c, 2 * ((x + dx) % 4) + (c + dc) % 2) for...  20.9 us
    all_to_all x1, waiting for transfers between devices, local(): lax.all_to_all(to_z, ('gr', 'fs'), 0, 0, axis_index_groups=[[4 * z + y fo...  18.6 us
    pallas_call x2, Pallas kernels, ffn(): pl.pallas_call(run, grid=(n // tile,), in_specs=[pl.BlockSpec(memory_spac...  10.8 us
    unnamed x33, local copies, waits for them, and re-layouts  8.48 us
  transfers between devices with their start and end apart: 39, of which 19 were waited for; matrix products, arithmetic and copies ran while one was open for 1% of the time, Pallas kernels for 8%

profile of v3, /device:TPU:1, one launch (start us, length us, event | category | flops | bytes accessed | tf_op | source)
XLA Modules:
  0.0 260.7 jit_solution(17565895670124397683)
XLA Ops:
  6.0 2.1 collective-permute-start
  8.1 2.5 collective-permute-start.1
  11.7 3.0 %collective-permute-start.4 = (bf16[512,128]{1,0:T(8,128)(2,1)S(1)}, bf16[512,128]{1,0:T(8,128)(2,1)S(1)}, u32[]{:S(2)}, u32[]{:S(2)}) collective-permute-start(bf16[512,128]{1,0:T(8,128)(2,1)S(1)} %copy-done.10), channel_id=1, source_target_pairs={{0,64},{8,72},{16,80},{24,88},{32,96},{40,104},{48,112},{56,120},{... | collective-permute-start | bytes 393224 | tf_op jit(solution)/shard_map/ppermute | solution.py:310
  17.1 7.7 %collective-permute-start.5 = (bf16[512,128]{1,0:T(8,128)(2,1)S(1)}, bf16[512,128]{1,0:T(8,128)(2,1)S(1)}, u32[]{:S(2)}, u32[]{:S(2)}) collective-permute-start(bf16[512,128]{1,0:T(8,128)(2,1)S(1)} %copy-done.10), channel_id=1, source_target_pairs={{0,32},{8,40},{16,48},{24,56},{32,64},{40,72},{48,80},{56,88},{64,... | collective-permute-start | bytes 393224 | tf_op jit(solution)/shard_map/ppermute | solution.py:310
  24.7 6.2 %collective-permute-done.5.refs_5_ = bf16[512,128]{1,0:T(8,128)(2,1)S(1)} collective-permute-done((bf16[512,128]{1,0:T(8,128)(2,1)S(1)}, bf16[512,128]{1,0:T(8,128)(2,1)S(1)}, u32[]{:S(2)}, u32[]{:S(2)}) %collective-permute-start.5) | collective-permute-done | bytes 131104 | tf_op jit(solution)/shard_map/ppermute | solution.py:310
  30.9 3.9 %shard_map.103 = (bf16[2,192,512]{2,1,0:T(8,128)(2,1)S(1)}, bf16[2,192,512]{2,1,0:T(8,128)(2,1)}, bf16[2,192,512]{2,1,0:T(8,128)(2,1)}, bf16[2,192,512]{2,1,0:T(8,128)(2,1)}, bf16[192,512]{1,0:T(8,128)(2,1)S(1)}) custom-call(s32[5]{0:T(128)S(1)} %stack.23.refs_0_, s32[2,512]{1,0:T(2,128)S(1)} %bitcast.7, bf16[512,128]{1,0:T(8,128)(2,1)S(1)} %copy-done.10, ...), custom_call_target="tpu_custom_call" | custom-call | tf_op jit(solution)/shard_map/pallas_call | solution.py:30
  41.6 5.3 %shard_map.106.refs_5_.refs_1_ = f32[512,128]{1,0:T(8,128)S(1)} custom-call(s32[5]{0:T(128)S(1)} %stack.23.refs_0_, s32[512,2]{1,0:T(8,128)S(1)} %copy.12.refs_1_, f32[512,2]{1,0:T(8,128)S(1)} %copy.13.refs_2_, bf16[4,264,128]{2,1,0:T(8,128)(2,1)S(1)} %get-tuple-element.52.refs_3_.refs_1_), custom_call_target="tpu_custom_call" | custom-call | tf_op jit(solution)/shard_map/pallas_call | solution.py:30
  46.9 10.9 %collective-permute-done.7.refs_2_ = bf16[2,192,512]{2,1,0:T(8,128)(2,1)S(1)} collective-permute-done((bf16[2,192,512]{2,1,0:T(8,128)(2,1)}, bf16[2,192,512]{2,1,0:T(8,128)(2,1)S(1)}, u32[]{:S(2)}, u32[]{:S(2)}) %collective-permute-start.7) | collective-permute-done | bytes 393248 | tf_op jit(solution)/shard_map/ppermute | solution.py:304
  61.3 2.6 %collective-permute-start.18 = (bf16[4,264,128]{2,1,0:T(8,128)(2,1)S(1)}, bf16[4,264,128]{2,1,0:T(8,128)(2,1)S(1)}, u32[]{:S(2)}, u32[]{:S(2)}) collective-permute-start(bf16[4,264,128]{2,1,0:T(8,128)(2,1)S(1)} %get-tuple-element.58), channel_id=1, source_target_pairs={{0,16},{8,24},{16,0},{24,8},{32,48},{40,56},{48,32},{56,40},{64,80... | collective-permute-start | bytes 811016 | tf_op jit(solution)/shard_map/ppermute | solution.py:310
  65.7 3.6 %collective-permute-done.17.refs_2_ = bf16[4,264,128]{2,1,0:T(8,128)(2,1)S(1)} collective-permute-done((bf16[4,264,128]{2,1,0:T(8,128)(2,1)S(1)}, bf16[4,264,128]{2,1,0:T(8,128)(2,1)S(1)}, u32[]{:S(2)}, u32[]{:S(2)}) %collective-permute-start.17) | collective-permute-done | bytes 270368 | tf_op jit(solution)/shard_map/ppermute | solution.py:310
  69.3 6.9 %collective-permute-done.18.refs_3_ = bf16[4,264,128]{2,1,0:T(8,128)(2,1)S(1)} collective-permute-done((bf16[4,264,128]{2,1,0:T(8,128)(2,1)S(1)}, bf16[4,264,128]{2,1,0:T(8,128)(2,1)S(1)}, u32[]{:S(2)}, u32[]{:S(2)}) %collective-permute-start.18) | collective-permute-done | bytes 270368 | tf_op jit(solution)/shard_map/ppermute | solution.py:310
  78.3 5.5 %all-to-all-start = ((bf16[8,4,264,128]{3,2,1,0:T(8,128)(2,1)}), bf16[8,4,264,128]{3,2,1,0:T(8,128)(2,1)S(1)}, u32[]{:S(2)}, u32[]{:S(2)}) async-start(bf16[8,4,264,128]{3,2,1,0:T(8,128)(2,1)} %shard_map.109), calls=%async_computation | async-start | bytes 4325376 | tf_op jit(solution)/shard_map/all_to_all | solution.py:371
  84.3 2.9 %collective-permute-start.12 = (bf16[1344,512]{1,0:T(8,128)(2,1)S(1)}, bf16[1344,512]{1,0:T(8,128)(2,1)}, u32[]{:S(2)}, u32[]{:S(2)}) collective-permute-start(bf16[1344,512]{1,0:T(8,128)(2,1)S(1)} %shard_map.108.refs_5_.refs_1_), channel_id=1, source_target_pairs={{0,16},{8,24},{16,0},{24,8},{32,48},{40,56},{48,32},{56,40},{64,80... | collective-permute-start | bytes 4128776 | tf_op jit(solution)/shard_map/ppermute | solution.py:310
  89.0 26.4 %collective-permute-done.13.refs_4_.refs_8_ = bf16[1344,512]{1,0:T(8,128)(2,1)S(1)} collective-permute-done((bf16[1344,512]{1,0:T(8,128)(2,1)S(1)}, bf16[1344,512]{1,0:T(8,128)(2,1)S(1)}, u32[]{:S(2)}, u32[]{:S(2)}) %collective-permute-start.13) | collective-permute-done | bytes 1376288 | tf_op jit(solution)/shard_map/ppermute | solution.py:310
  118.2 18.6 %all-to-all-done.refs_1_ = bf16[8,4,264,128]{3,2,1,0:T(8,128)(2,1)S(1)} async-done(((bf16[8,4,264,128]{3,2,1,0:T(8,128)(2,1)}), bf16[8,4,264,128]{3,2,1,0:T(8,128)(2,1)S(1)}, u32[]{:S(2)}, u32[]{:S(2)}) %all-to-all-start) | async-done | bytes 2162720 | tf_op jit(solution)/shard_map/all_to_all | solution.py:371
  138.4 7.9 %collective-permute-done.12.refs_3_.refs_7_ = bf16[1344,512]{1,0:T(8,128)(2,1)} collective-permute-done((bf16[1344,512]{1,0:T(8,128)(2,1)S(1)}, bf16[1344,512]{1,0:T(8,128)(2,1)}, u32[]{:S(2)}, u32[]{:S(2)}) %collective-permute-start.12) | collective-permute-done | bytes 1376288 | tf_op jit(solution)/shard_map/ppermute | solution.py:310
  147.5 2.9 %shard_map.111 = (bf16[384,512]{1,0:T(8,128)(2,1)S(1)}, bf16[384,512]{1,0:T(8,128)(2,1)S(1)}, bf16[384,512]{1,0:T(8,128)(2,1)S(1)}, bf16[384,512]{1,0:T(8,128)(2,1)S(1)}) custom-call(s32[5]{0:T(128)S(1)} %stack.23.refs_0_, bf16[1344,512]{1,0:T(8,128)(2,1)S(1)} %shard_map.108.refs_5_.refs_1_, bf16[1344,512]{1,0:T(8,128)(2,1)} %collective-permute-done.11.refs_2_.refs_6_, ...), custom_call_target="tpu_custom_call" | custom-call | tf_op jit(solution)/shard_map/pallas_call | solution.py:228
  150.4 4.4 %collective-permute-done.15.refs_11_ = bf16[192,512]{1,0:T(8,128)(2,1)} collective-permute-done((bf16[192,512]{1,0:T(8,128)(2,1)}, bf16[192,512]{1,0:T(8,128)(2,1)}, u32[]{:S(2)}, u32[]{:S(2)}) %collective-permute-start.15) | collective-permute-done | bytes 196640 | tf_op jit(solution)/shard_map/ppermute | solution.py:310
  154.8 7.9 %shard_map.112 = (bf16[1152,512]{1,0:T(8,128)(2,1)S(1)}, bf16[1152,512]{1,0:T(8,128)(2,1)}, bf16[1152,512]{1,0:T(8,128)(2,1)}, bf16[1152,512]{1,0:T(8,128)(2,1)}) custom-call(s32[5]{0:T(128)S(1)} %stack.23.refs_0_, bf16[1344,512]{1,0:T(8,128)(2,1)} %copy-done, bf16[1344,512]{1,0:T(8,128)(2,1)} %collective-permute-done.11.refs_2_.refs_6_, ...), custom_call_target="tpu_custom_call" | custom-call | tf_op jit(solution)/shard_map/pallas_call | solution.py:228
  165.9 2.3 collective-permute-start.23
  168.1 30.4 %collective-permute-done.22.refs_2_ = bf16[384,512]{1,0:T(8,128)(2,1)S(1)} collective-permute-done((bf16[384,512]{1,0:T(8,128)(2,1)S(1)}, bf16[384,512]{1,0:T(8,128)(2,1)S(1)}, u32[]{:S(2)}, u32[]{:S(2)}) %collective-permute-start.22) | collective-permute-done | bytes 393248 | tf_op jit(solution)/shard_map/ppermute | solution.py:310
  204.1 2.7 %collective-permute-start.27 = (bf16[384,256]{1,0:T(8,128)(2,1)S(1)}, bf16[384,256]{1,0:T(8,128)(2,1)S(1)}, u32[]{:S(2)}, u32[]{:S(2)}) collective-permute-start(bf16[384,256]{1,0:T(8,128)(2,1)S(1)} %get-tuple-element.75), channel_id=1, source_target_pairs={{0,24},{8,0},{16,8},{24,16},{32,56},{40,32},{48,40},{56,48},{64,88... | collective-permute-start | bytes 589832 | tf_op jit(solution)/shard_map/ppermute | solution.py:310
  206.7 12.3 %collective-permute-done.27.refs_5_ = bf16[384,256]{1,0:T(8,128)(2,1)S(1)} collective-permute-done((bf16[384,256]{1,0:T(8,128)(2,1)S(1)}, bf16[384,256]{1,0:T(8,128)(2,1)S(1)}, u32[]{:S(2)}, u32[]{:S(2)}) %collective-permute-start.27) | collective-permute-done | bytes 196640 | tf_op jit(solution)/shard_map/ppermute | solution.py:310
  219.1 2.3 collective-permute-done.26.refs_4_
  222.0 4.5 %collective-permute-start.34 = (bf16[192,512]{1,0:T(8,128)(2,1)S(1)}, bf16[192,512]{1,0:T(8,128)(2,1)S(1)}, u32[]{:S(2)}, u32[]{:S(2)}) collective-permute-start(bf16[192,512]{1,0:T(8,128)(2,1)S(1)} %get-tuple-element.83), channel_id=1, source_target_pairs={{0,5},{1,4},{2,7},{3,6},{4,1},{5,0},{6,3},{7,2},{8,13},{9,12},{10,... | collective-permute-start | bytes 589832 | tf_op jit(solution)/shard_map/ppermute | solution.py:304
  226.5 2.3 collective-permute-start.33
  230.0 2.1 collective-permute-start.30
  232.1 2.1 collective-permute-start.32
  234.2 3.5 %collective-permute-done.33.refs_2_ = bf16[192,512]{1,0:T(8,128)(2,1)S(1)} collective-permute-done((bf16[192,512]{1,0:T(8,128)(2,1)S(1)}, bf16[192,512]{1,0:T(8,128)(2,1)S(1)}, u32[]{:S(2)}, u32[]{:S(2)}) %collective-permute-start.33) | collective-permute-done | bytes 196640 | tf_op jit(solution)/shard_map/ppermute | solution.py:304
  240.6 4.2 %collective-permute-done.31.refs_5_ = bf16[192,512]{1,0:T(8,128)(2,1)S(1)} collective-permute-done((bf16[192,512]{1,0:T(8,128)(2,1)S(1)}, bf16[192,512]{1,0:T(8,128)(2,1)S(1)}, u32[]{:S(2)}, u32[]{:S(2)}) %collective-permute-start.31) | collective-permute-done | bytes 196640 | tf_op jit(solution)/shard_map/ppermute | solution.py:304
  244.8 2.5 shard_map.119
  256.0 3.0 %collective-permute-done.35 = bf16[512,128]{1,0:T(8,128)(2,1)} collective-permute-done((bf16[512,128]{1,0:T(8,128)(2,1)}, bf16[512,128]{1,0:T(8,128)(2,1)}, u32[]{:S(2)}, u32[]{:S(2)}) %collective-permute-start.35) | collective-permute-done | bytes 131104 | tf_op jit(solution)/shard_map/ppermute | solution.py:310
  (100 shorter events, 54.4 us)
Async XLA Ops:
  6.0 28.9 %collective-permute-start = (bf16[2,2,264,128]{3,2,1,0:T(8,128)(2,1)S(1)}, bf16[2,2,264,128]{3,2,1,0:T(8,128)(2,1)S(1)}, u32[]{:S(2)}, u32[]{:S(2)}) collective-permute-start(bf16[2,2,264,128]{3,2,1,0:T(8,128)(2,1)S(1)} %get-tuple-element.48), channel_id=1, source_target_pairs={{0,2},{1,3},{2,4},{3,5},{4,6},{5,7},{6,0},{7,1},{8,10},{9,11},{10,... | collective-permute-start | bytes 811016 | tf_op jit(solution)/shard_map/ppermute | solution.py:304
  8.1 26.8 %collective-permute-start.1 = (bf16[2,2,264,128]{3,2,1,0:T(8,128)(2,1)S(1)}, bf16[2,2,264,128]{3,2,1,0:T(8,128)(2,1)S(1)}, u32[]{:S(2)}, u32[]{:S(2)}) collective-permute-start(bf16[2,2,264,128]{3,2,1,0:T(8,128)(2,1)S(1)} %get-tuple-element.49), channel_id=1, source_target_pairs={{0,4},{1,5},{2,6},{3,7},{4,0},{5,1},{6,2},{7,3},{8,12},{9,13},{10,... | collective-permute-start | bytes 811016 | tf_op jit(solution)/shard_map/ppermute | solution.py:304
  10.6 24.3 %collective-permute-start.2 = (bf16[2,2,264,128]{3,2,1,0:T(8,128)(2,1)S(1)}, bf16[2,2,264,128]{3,2,1,0:T(8,128)(2,1)S(1)}, u32[]{:S(2)}, u32[]{:S(2)}) collective-permute-start(bf16[2,2,264,128]{3,2,1,0:T(8,128)(2,1)S(1)} %get-tuple-element.50), channel_id=1, source_target_pairs={{0,6},{1,7},{2,0},{3,1},{4,2},{5,3},{6,4},{7,5},{8,14},{9,15},{10,... | collective-permute-start | bytes 811016 | tf_op jit(solution)/shard_map/ppermute | solution.py:304
  14.7 10.0 %collective-permute-start.3 = (bf16[512,128]{1,0:T(8,128)(2,1)S(1)}, bf16[512,128]{1,0:T(8,128)(2,1)S(1)}, u32[]{:S(2)}, u32[]{:S(2)}) collective-permute-start(bf16[512,128]{1,0:T(8,128)(2,1)S(1)} %copy-done.10), channel_id=1, source_target_pairs={{0,96},{8,104},{16,112},{24,120},{32,0},{40,8},{48,16},{56,24},{64... | collective-permute-start | bytes 393224 | tf_op jit(solution)/shard_map/ppermute | solution.py:310
  17.1 13.8 %collective-permute-start.5 = (bf16[512,128]{1,0:T(8,128)(2,1)S(1)}, bf16[512,128]{1,0:T(8,128)(2,1)S(1)}, u32[]{:S(2)}, u32[]{:S(2)}) collective-permute-start(bf16[512,128]{1,0:T(8,128)(2,1)S(1)} %copy-done.10), channel_id=1, source_target_pairs={{0,32},{8,40},{16,48},{24,56},{32,64},{40,72},{48,80},{56,88},{64,... | collective-permute-start | bytes 393224 | tf_op jit(solution)/shard_map/ppermute | solution.py:310
  37.3 20.5 %collective-permute-start.7 = (bf16[2,192,512]{2,1,0:T(8,128)(2,1)}, bf16[2,192,512]{2,1,0:T(8,128)(2,1)S(1)}, u32[]{:S(2)}, u32[]{:S(2)}) collective-permute-start(bf16[2,192,512]{2,1,0:T(8,128)(2,1)} %get-tuple-element.53), channel_id=1, source_target_pairs={{0,2},{1,3},{2,4},{3,5},{4,6},{5,7},{6,0},{7,1},{8,10},{9,11},{10,... | collective-permute-start | bytes 1179656 | tf_op jit(solution)/shard_map/ppermute | solution.py:304
  37.6 20.2 %collective-permute-start.8 = (bf16[2,192,512]{2,1,0:T(8,128)(2,1)}, bf16[2,192,512]{2,1,0:T(8,128)(2,1)S(1)}, u32[]{:S(2)}, u32[]{:S(2)}) collective-permute-start(bf16[2,192,512]{2,1,0:T(8,128)(2,1)} %get-tuple-element.54), channel_id=1, source_target_pairs={{0,4},{1,5},{2,6},{3,7},{4,0},{5,1},{6,2},{7,3},{8,12},{9,13},{10,... | collective-permute-start | bytes 1179656 | tf_op jit(solution)/shard_map/ppermute | solution.py:304
  38.5 19.7 %collective-permute-start.9 = (bf16[2,192,512]{2,1,0:T(8,128)(2,1)}, bf16[2,192,512]{2,1,0:T(8,128)(2,1)S(1)}, u32[]{:S(2)}, u32[]{:S(2)}) collective-permute-start(bf16[2,192,512]{2,1,0:T(8,128)(2,1)} %get-tuple-element.55), channel_id=1, source_target_pairs={{0,6},{1,7},{2,0},{3,1},{4,2},{5,3},{6,4},{7,5},{8,14},{9,15},{10,... | collective-permute-start | bytes 1179656 | tf_op jit(solution)/shard_map/ppermute | solution.py:304
  61.3 14.9 %collective-permute-start.18 = (bf16[4,264,128]{2,1,0:T(8,128)(2,1)S(1)}, bf16[4,264,128]{2,1,0:T(8,128)(2,1)S(1)}, u32[]{:S(2)}, u32[]{:S(2)}) collective-permute-start(bf16[4,264,128]{2,1,0:T(8,128)(2,1)S(1)} %get-tuple-element.58), channel_id=1, source_target_pairs={{0,16},{8,24},{16,0},{24,8},{32,48},{40,56},{48,32},{56,40},{64,80... | collective-permute-start | bytes 811016 | tf_op jit(solution)/shard_map/ppermute | solution.py:310
  63.9 12.3 %collective-permute-start.19 = (bf16[4,264,128]{2,1,0:T(8,128)(2,1)S(1)}, bf16[4,264,128]{2,1,0:T(8,128)(2,1)S(1)}, u32[]{:S(2)}, u32[]{:S(2)}) collective-permute-start(bf16[4,264,128]{2,1,0:T(8,128)(2,1)S(1)} %get-tuple-element.59), channel_id=1, source_target_pairs={{0,24},{8,0},{16,8},{24,16},{32,56},{40,32},{48,40},{56,48},{64,88... | collective-permute-start | bytes 811016 | tf_op jit(solution)/shard_map/ppermute | solution.py:310
  78.3 58.5 %all-to-all-start = ((bf16[8,4,264,128]{3,2,1,0:T(8,128)(2,1)}), bf16[8,4,264,128]{3,2,1,0:T(8,128)(2,1)S(1)}, u32[]{:S(2)}, u32[]{:S(2)}) async-start(bf16[8,4,264,128]{3,2,1,0:T(8,128)(2,1)} %shard_map.109), calls=%async_computation | async-start | bytes 4325376 | tf_op jit(solution)/shard_map/all_to_all | solution.py:371
  83.8 31.7 %collective-permute-start.13 = (bf16[1344,512]{1,0:T(8,128)(2,1)S(1)}, bf16[1344,512]{1,0:T(8,128)(2,1)S(1)}, u32[]{:S(2)}, u32[]{:S(2)}) collective-permute-start(bf16[1344,512]{1,0:T(8,128)(2,1)S(1)} %shard_map.108.refs_5_.refs_1_), channel_id=1, source_target_pairs={{0,8},{8,16},{16,24},{24,0},{32,40},{40,48},{48,56},{56,32},{64,72... | collective-permute-start | bytes 4128776 | tf_op jit(solution)/shard_map/ppermute | solution.py:310
  84.3 62.0 %collective-permute-start.12 = (bf16[1344,512]{1,0:T(8,128)(2,1)S(1)}, bf16[1344,512]{1,0:T(8,128)(2,1)}, u32[]{:S(2)}, u32[]{:S(2)}) collective-permute-start(bf16[1344,512]{1,0:T(8,128)(2,1)S(1)} %shard_map.108.refs_5_.refs_1_), channel_id=1, source_target_pairs={{0,16},{8,24},{16,0},{24,8},{32,48},{40,56},{48,32},{56,40},{64,80... | collective-permute-start | bytes 4128776 | tf_op jit(solution)/shard_map/ppermute | solution.py:310
  87.2 60.3 %collective-permute-start.11 = (bf16[1344,512]{1,0:T(8,128)(2,1)S(1)}, bf16[1344,512]{1,0:T(8,128)(2,1)}, u32[]{:S(2)}, u32[]{:S(2)}) collective-permute-start(bf16[1344,512]{1,0:T(8,128)(2,1)S(1)} %shard_map.108.refs_5_.refs_1_), channel_id=1, source_target_pairs={{0,24},{8,0},{16,8},{24,16},{32,56},{40,32},{48,40},{56,48},{64,88... | collective-permute-start | bytes 4128776 | tf_op jit(solution)/shard_map/ppermute | solution.py:310
  87.9 62.5 %collective-permute-start.16 = (bf16[192,512]{1,0:T(8,128)(2,1)}, bf16[192,512]{1,0:T(8,128)(2,1)}, u32[]{:S(2)}, u32[]{:S(2)}) collective-permute-start(bf16[192,512]{1,0:T(8,128)(2,1)} %copy-done.8), channel_id=1, source_target_pairs={{0,8},{8,16},{16,24},{24,0},{32,40},{40,48},{48,56},{56,32},{64,72... | collective-permute-start | bytes 589832 | tf_op jit(solution)/shard_map/ppermute | solution.py:310
  88.7 66.1 %collective-permute-start.15 = (bf16[192,512]{1,0:T(8,128)(2,1)}, bf16[192,512]{1,0:T(8,128)(2,1)}, u32[]{:S(2)}, u32[]{:S(2)}) collective-permute-start(bf16[192,512]{1,0:T(8,128)(2,1)} %copy-done.8), channel_id=1, source_target_pairs={{0,16},{8,24},{16,0},{24,8},{32,48},{40,56},{48,32},{56,40},{64,80... | collective-permute-start | bytes 589832 | tf_op jit(solution)/shard_map/ppermute | solution.py:310
  116.6 38.1 %collective-permute-start.14 = (bf16[192,512]{1,0:T(8,128)(2,1)}, bf16[192,512]{1,0:T(8,128)(2,1)}, u32[]{:S(2)}, u32[]{:S(2)}) collective-permute-start(bf16[192,512]{1,0:T(8,128)(2,1)} %copy-done.8), channel_id=1, source_target_pairs={{0,24},{8,0},{16,8},{24,16},{32,56},{40,32},{48,40},{56,48},{64,88... | collective-permute-start | bytes 589832 | tf_op jit(solution)/shard_map/ppermute | solution.py:310
  162.7 38.6 %collective-permute-start.20 = (bf16[1152,512]{1,0:T(8,128)(2,1)}, bf16[1152,512]{1,0:T(8,128)(2,1)S(1)}, u32[]{:S(2)}, u32[]{:S(2)}) collective-permute-start(bf16[1152,512]{1,0:T(8,128)(2,1)} %get-tuple-element.65), channel_id=1, source_target_pairs={{0,8},{8,16},{16,24},{24,0},{32,40},{40,48},{48,56},{56,32},{64,72... | collective-permute-start | bytes 3538952 | tf_op jit(solution)/shard_map/ppermute | solution.py:310
  164.4 37.0 %collective-permute-start.21 = (bf16[1152,512]{1,0:T(8,128)(2,1)}, bf16[1152,512]{1,0:T(8,128)(2,1)S(1)}, u32[]{:S(2)}, u32[]{:S(2)}) collective-permute-start(bf16[1152,512]{1,0:T(8,128)(2,1)} %get-tuple-element.66), channel_id=1, source_target_pairs={{0,24},{8,0},{16,8},{24,16},{32,56},{40,32},{48,40},{56,48},{64,88... | collective-permute-start | bytes 3538952 | tf_op jit(solution)/shard_map/ppermute | solution.py:310
  165.4 33.1 %collective-permute-start.22 = (bf16[384,512]{1,0:T(8,128)(2,1)S(1)}, bf16[384,512]{1,0:T(8,128)(2,1)S(1)}, u32[]{:S(2)}, u32[]{:S(2)}) collective-permute-start(bf16[384,512]{1,0:T(8,128)(2,1)S(1)} %get-tuple-element.69), channel_id=1, source_target_pairs={{0,8},{8,16},{16,24},{24,0},{32,40},{40,48},{48,56},{56,32},{64,72... | collective-permute-start | bytes 1179656 | tf_op jit(solution)/shard_map/ppermute | solution.py:310
  165.9 33.3 %collective-permute-start.23 = (bf16[384,512]{1,0:T(8,128)(2,1)S(1)}, bf16[384,512]{1,0:T(8,128)(2,1)S(1)}, u32[]{:S(2)}, u32[]{:S(2)}) collective-permute-start(bf16[384,512]{1,0:T(8,128)(2,1)S(1)} %get-tuple-element.70), channel_id=1, source_target_pairs={{0,24},{8,0},{16,8},{24,16},{32,56},{40,32},{48,40},{56,48},{64,88... | collective-permute-start | bytes 1179656 | tf_op jit(solution)/shard_map/ppermute | solution.py:310
  202.2 26.7 %collective-permute-start.25 = (bf16[1152,256]{1,0:T(8,128)(2,1)S(1)}, bf16[1152,256]{1,0:T(8,128)(2,1)S(1)}, u32[]{:S(2)}, u32[]{:S(2)}) collective-permute-start(bf16[1152,256]{1,0:T(8,128)(2,1)S(1)} %get-tuple-element.74), channel_id=1, source_target_pairs={{0,24},{8,0},{16,8},{24,16},{32,56},{40,32},{48,40},{56,48},{64,88... | collective-permute-start | bytes 1769480 | tf_op jit(solution)/shard_map/ppermute | solution.py:310
  204.1 24.8 %collective-permute-start.24 = (bf16[1152,256]{1,0:T(8,128)(2,1)S(1)}, bf16[1152,256]{1,0:T(8,128)(2,1)S(1)}, u32[]{:S(2)}, u32[]{:S(2)}) collective-permute-start(bf16[1152,256]{1,0:T(8,128)(2,1)S(1)} %get-tuple-element.73.refs_6_), channel_id=1, source_target_pairs={{0,8},{8,16},{16,24},{24,0},{32,40},{40,48},{48,56},{56,32},{64,72... | collective-permute-start | bytes 1769480 | tf_op jit(solution)/shard_map/ppermute | solution.py:310
  204.1 15.0 %collective-permute-start.27 = (bf16[384,256]{1,0:T(8,128)(2,1)S(1)}, bf16[384,256]{1,0:T(8,128)(2,1)S(1)}, u32[]{:S(2)}, u32[]{:S(2)}) collective-permute-start(bf16[384,256]{1,0:T(8,128)(2,1)S(1)} %get-tuple-element.75), channel_id=1, source_target_pairs={{0,24},{8,0},{16,8},{24,16},{32,56},{40,32},{48,40},{56,48},{64,88... | collective-permute-start | bytes 589832 | tf_op jit(solution)/shard_map/ppermute | solution.py:310
  206.7 14.6 %collective-permute-start.26 = (bf16[384,256]{1,0:T(8,128)(2,1)S(1)}, bf16[384,256]{1,0:T(8,128)(2,1)S(1)}, u32[]{:S(2)}, u32[]{:S(2)}) collective-permute-start(bf16[384,256]{1,0:T(8,128)(2,1)S(1)} %get-tuple-element.71.refs_4_), channel_id=1, source_target_pairs={{0,8},{8,16},{16,24},{24,0},{32,40},{40,48},{48,56},{56,32},{64,72... | collective-permute-start | bytes 589832 | tf_op jit(solution)/shard_map/ppermute | solution.py:310
  222.0 10.1 %collective-permute-start.34 = (bf16[192,512]{1,0:T(8,128)(2,1)S(1)}, bf16[192,512]{1,0:T(8,128)(2,1)S(1)}, u32[]{:S(2)}, u32[]{:S(2)}) collective-permute-start(bf16[192,512]{1,0:T(8,128)(2,1)S(1)} %get-tuple-element.83), channel_id=1, source_target_pairs={{0,5},{1,4},{2,7},{3,6},{4,1},{5,0},{6,3},{7,2},{8,13},{9,12},{10,... | collective-permute-start | bytes 589832 | tf_op jit(solution)/shard_map/ppermute | solution.py:304
  226.5 11.2 %collective-permute-start.33 = (bf16[192,512]{1,0:T(8,128)(2,1)S(1)}, bf16[192,512]{1,0:T(8,128)(2,1)S(1)}, u32[]{:S(2)}, u32[]{:S(2)}) collective-permute-start(bf16[192,512]{1,0:T(8,128)(2,1)S(1)} %get-tuple-element.76.refs_6_), channel_id=1, source_target_pairs={{0,4},{1,5},{2,6},{3,7},{4,0},{5,1},{6,2},{7,3},{8,12},{9,13},{10,... | collective-permute-start | bytes 589832 | tf_op jit(solution)/shard_map/ppermute | solution.py:304
  229.8 10.8 %collective-permute-start.29 = (bf16[192,512]{1,0:T(8,128)(2,1)S(1)}, bf16[192,512]{1,0:T(8,128)(2,1)S(1)}, u32[]{:S(2)}, u32[]{:S(2)}) collective-permute-start(bf16[192,512]{1,0:T(8,128)(2,1)S(1)} %get-tuple-element.78), channel_id=1, source_target_pairs={{0,3},{1,2},{2,5},{3,4},{4,7},{5,6},{6,1},{7,0},{8,11},{9,10},{10,... | collective-permute-start | bytes 589832 | tf_op jit(solution)/shard_map/ppermute | solution.py:304
  230.0 10.6 %collective-permute-start.30 = (bf16[192,512]{1,0:T(8,128)(2,1)S(1)}, bf16[192,512]{1,0:T(8,128)(2,1)S(1)}, u32[]{:S(2)}, u32[]{:S(2)}) collective-permute-start(bf16[192,512]{1,0:T(8,128)(2,1)S(1)} %get-tuple-element.79), channel_id=1, source_target_pairs={{0,6},{1,7},{2,0},{3,1},{4,2},{5,3},{6,4},{7,5},{8,14},{9,15},{10,... | collective-permute-start | bytes 589832 | tf_op jit(solution)/shard_map/ppermute | solution.py:304
  232.1 12.7 %collective-permute-start.31 = (bf16[192,512]{1,0:T(8,128)(2,1)S(1)}, bf16[192,512]{1,0:T(8,128)(2,1)S(1)}, u32[]{:S(2)}, u32[]{:S(2)}) collective-permute-start(bf16[192,512]{1,0:T(8,128)(2,1)S(1)} %get-tuple-element.80), channel_id=1, source_target_pairs={{0,2},{1,3},{2,4},{3,5},{4,6},{5,7},{6,0},{7,1},{8,10},{9,11},{10,... | collective-permute-start | bytes 589832 | tf_op jit(solution)/shard_map/ppermute | solution.py:304
  232.1 12.7 %collective-permute-start.32 = (bf16[192,512]{1,0:T(8,128)(2,1)S(1)}, bf16[192,512]{1,0:T(8,128)(2,1)S(1)}, u32[]{:S(2)}, u32[]{:S(2)}) collective-permute-start(bf16[192,512]{1,0:T(8,128)(2,1)S(1)} %get-tuple-element.81), channel_id=1, source_target_pairs={{0,1},{1,0},{2,3},{3,2},{4,5},{5,4},{6,7},{7,6},{8,9},{9,8},{10,11... | collective-permute-start | bytes 589832 | tf_op jit(solution)/shard_map/ppermute | solution.py:304
  247.3 11.7 %collective-permute-start.35 = (bf16[512,128]{1,0:T(8,128)(2,1)}, bf16[512,128]{1,0:T(8,128)(2,1)}, u32[]{:S(2)}, u32[]{:S(2)}) collective-permute-start(bf16[512,128]{1,0:T(8,128)(2,1)} %get-tuple-element.85), channel_id=1, source_target_pairs={{0,64},{8,72},{16,80},{24,88},{32,96},{40,104},{48,112},{56,120},{... | collective-permute-start | bytes 393224 | tf_op jit(solution)/shard_map/ppermute | solution.py:310
  (21 other events, 246.5 us)

commit v4 on v3

--- a/solution.py
+++ b/solution.py
@@ -48,7 +48,9 @@
 
 
 def pack_body(where, gain, gate, up, down, *outs):
-    g = gain[...]
+    row = lax.broadcasted_iota(jnp.int32, (64, 64), 0)
+    col = lax.broadcasted_iota(jnp.int32, (64, 64), 1)
+    g = jnp.sum(jnp.where(row == col, gain[...], 0.0), axis=1, keepdims=True)
     for r in range(8):
         e = peer(where, r)
         for top, mats in ((0, (gate[e] * g, up[e] * g)), (PACK_GU, (down[e],))):
@@ -321,7 +323,7 @@
     packed = call(
         pack_body,
         [sds(2, 2, PACK, 128)] * 4,
-        (where, norm_gain[:, None], gate_master, up_master, down_master),
+        (where, norm_gain[None, :], gate_master, up_master, down_master),
     )
 
     def over_x(parts):

time: 263 us -> 263 us (level)
    unnamed x33 -> x35, local copies, waits for them, and re-layouts: 8.48 us -> 9.12 us
where the time goes in v4:
time: 263 us; the launch traced here: 261 us
  waiting for transfers between devices  146 us (56%)
  starting transfers between devices  66.4 us (25%)
  Pallas kernels  36.7 us (14%)
  local copies, waits for them, and re-layouts  9.21 us (4%)
    ppermute x23, waiting for transfers between devices, shift_fs(): lax.ppermute(a, 'fs', [(4 * z + y, 4 * ((z + dz) % 4) + (y + dy) % 4) for...  106 us
    ppermute x23, starting transfers between devices, shift_fs(): lax.ppermute(a, 'fs', [(4 * z + y, 4 * ((z + dz) % 4) + (y + dy) % 4) for...  38.8 us
    pallas_call x16, Pallas kernels, call(): pl.pallas_call(run, out_shape=outs, in_specs=[pl.BlockSpec(memory_space=p...  25.9 us
    ppermute x15, starting transfers between devices, shift_tp(): lax.ppermute(a, 'tp', [(2 * x + c, 2 * ((x + dx) % 4) + (c + dc) % 2) for...  21.9 us
    ppermute x15, waiting for transfers between devices, shift_tp(): lax.ppermute(a, 'tp', [(2 * x + c, 2 * ((x + dx) % 4) + (c + dc) % 2) for...  20.9 us
    all_to_all x1, waiting for transfers between devices, local(): lax.all_to_all(to_z, ('gr', 'fs'), 0, 0, axis_index_groups=[[4 * z + y fo...  18.6 us
    pallas_call x2, Pallas kernels, ffn(): pl.pallas_call(run, grid=(n // tile,), in_specs=[pl.BlockSpec(memory_spac...  10.8 us
    unnamed x35, local copies, waits for them, and re-layouts  9.12 us
  transfers between devices with their start and end apart: 39, of which 19 were waited for; matrix products, arithmetic and copies ran while one was open for 1% of the time, Pallas kernels for 8%

profile of v4, /device:TPU:1, one launch (start us, length us, event | category | flops | bytes accessed | tf_op | source)
XLA Modules:
  0.0 260.8 jit_solution(11897922388683915172)
XLA Ops:
  5.9 2.1 collective-permute-start
  8.0 2.5 collective-permute-start.1
  11.6 3.0 %collective-permute-start.4 = (bf16[512,128]{1,0:T(8,128)(2,1)S(1)}, bf16[512,128]{1,0:T(8,128)(2,1)S(1)}, u32[]{:S(2)}, u32[]{:S(2)}) collective-permute-start(bf16[512,128]{1,0:T(8,128)(2,1)S(1)} %copy-done.10), channel_id=1, source_target_pairs={{0,64},{8,72},{16,80},{24,88},{32,96},{40,104},{48,112},{56,120},{... | collective-permute-start | bytes 393224 | tf_op jit(solution)/shard_map/ppermute | solution.py:312
  17.0 7.7 %collective-permute-start.5 = (bf16[512,128]{1,0:T(8,128)(2,1)S(1)}, bf16[512,128]{1,0:T(8,128)(2,1)S(1)}, u32[]{:S(2)}, u32[]{:S(2)}) collective-permute-start(bf16[512,128]{1,0:T(8,128)(2,1)S(1)} %copy-done.10), channel_id=1, source_target_pairs={{0,32},{8,40},{16,48},{24,56},{32,64},{40,72},{48,80},{56,88},{64,... | collective-permute-start | bytes 393224 | tf_op jit(solution)/shard_map/ppermute | solution.py:312
  24.6 6.2 %collective-permute-done.5.refs_5_ = bf16[512,128]{1,0:T(8,128)(2,1)S(1)} collective-permute-done((bf16[512,128]{1,0:T(8,128)(2,1)S(1)}, bf16[512,128]{1,0:T(8,128)(2,1)S(1)}, u32[]{:S(2)}, u32[]{:S(2)}) %collective-permute-start.5) | collective-permute-done | bytes 131104 | tf_op jit(solution)/shard_map/ppermute | solution.py:312
  30.8 3.9 %shard_map.103 = (bf16[2,192,512]{2,1,0:T(8,128)(2,1)S(1)}, bf16[2,192,512]{2,1,0:T(8,128)(2,1)}, bf16[2,192,512]{2,1,0:T(8,128)(2,1)}, bf16[2,192,512]{2,1,0:T(8,128)(2,1)}, bf16[192,512]{1,0:T(8,128)(2,1)S(1)}) custom-call(s32[5]{0:T(128)S(1)} %stack.23.refs_0_, s32[2,512]{1,0:T(2,128)S(1)} %bitcast.7, bf16[512,128]{1,0:T(8,128)(2,1)S(1)} %copy-done.10, ...), custom_call_target="tpu_custom_call" | custom-call | tf_op jit(solution)/shard_map/pallas_call | solution.py:30
  41.5 5.3 %shard_map.106.refs_5_.refs_1_ = f32[512,128]{1,0:T(8,128)S(1)} custom-call(s32[5]{0:T(128)S(1)} %stack.23.refs_0_, s32[512,2]{1,0:T(8,128)S(1)} %copy.11.refs_1_, f32[512,2]{1,0:T(8,128)S(1)} %copy.12.refs_2_, bf16[4,264,128]{2,1,0:T(8,128)(2,1)S(1)} %get-tuple-element.52.refs_3_.refs_1_), custom_call_target="tpu_custom_call" | custom-call | tf_op jit(solution)/shard_map/pallas_call | solution.py:30
  46.8 10.9 %collective-permute-done.7.refs_2_ = bf16[2,192,512]{2,1,0:T(8,128)(2,1)S(1)} collective-permute-done((bf16[2,192,512]{2,1,0:T(8,128)(2,1)}, bf16[2,192,512]{2,1,0:T(8,128)(2,1)S(1)}, u32[]{:S(2)}, u32[]{:S(2)}) %collective-permute-start.7) | collective-permute-done | bytes 393248 | tf_op jit(solution)/shard_map/ppermute | solution.py:306
  61.2 2.6 %collective-permute-start.18 = (bf16[4,264,128]{2,1,0:T(8,128)(2,1)S(1)}, bf16[4,264,128]{2,1,0:T(8,128)(2,1)S(1)}, u32[]{:S(2)}, u32[]{:S(2)}) collective-permute-start(bf16[4,264,128]{2,1,0:T(8,128)(2,1)S(1)} %get-tuple-element.58), channel_id=1, source_target_pairs={{0,16},{8,24},{16,0},{24,8},{32,48},{40,56},{48,32},{56,40},{64,80... | collective-permute-start | bytes 811016 | tf_op jit(solution)/shard_map/ppermute | solution.py:312
  65.5 3.6 %collective-permute-done.17.refs_2_ = bf16[4,264,128]{2,1,0:T(8,128)(2,1)S(1)} collective-permute-done((bf16[4,264,128]{2,1,0:T(8,128)(2,1)S(1)}, bf16[4,264,128]{2,1,0:T(8,128)(2,1)S(1)}, u32[]{:S(2)}, u32[]{:S(2)}) %collective-permute-start.17) | collective-permute-done | bytes 270368 | tf_op jit(solution)/shard_map/ppermute | solution.py:312
  69.2 6.9 %collective-permute-done.18.refs_3_ = bf16[4,264,128]{2,1,0:T(8,128)(2,1)S(1)} collective-permute-done((bf16[4,264,128]{2,1,0:T(8,128)(2,1)S(1)}, bf16[4,264,128]{2,1,0:T(8,128)(2,1)S(1)}, u32[]{:S(2)}, u32[]{:S(2)}) %collective-permute-start.18) | collective-permute-done | bytes 270368 | tf_op jit(solution)/shard_map/ppermute | solution.py:312
  76.1 2.1 shard_map.109
  78.2 5.7 %all-to-all-start = ((bf16[8,4,264,128]{3,2,1,0:T(8,128)(2,1)}), bf16[8,4,264,128]{3,2,1,0:T(8,128)(2,1)S(1)}, u32[]{:S(2)}, u32[]{:S(2)}) async-start(bf16[8,4,264,128]{3,2,1,0:T(8,128)(2,1)} %shard_map.109), calls=%async_computation | async-start | bytes 4325376 | tf_op jit(solution)/shard_map/all_to_all | solution.py:373
  84.4 2.9 %collective-permute-start.12 = (bf16[1344,512]{1,0:T(8,128)(2,1)S(1)}, bf16[1344,512]{1,0:T(8,128)(2,1)}, u32[]{:S(2)}, u32[]{:S(2)}) collective-permute-start(bf16[1344,512]{1,0:T(8,128)(2,1)S(1)} %shard_map.108.refs_5_.refs_1_), channel_id=1, source_target_pairs={{0,16},{8,24},{16,0},{24,8},{32,48},{40,56},{48,32},{56,40},{64,80... | collective-permute-start | bytes 4128776 | tf_op jit(solution)/shard_map/ppermute | solution.py:312
  89.1 26.5 %collective-permute-done.13.refs_4_.refs_8_ = bf16[1344,512]{1,0:T(8,128)(2,1)S(1)} collective-permute-done((bf16[1344,512]{1,0:T(8,128)(2,1)S(1)}, bf16[1344,512]{1,0:T(8,128)(2,1)S(1)}, u32[]{:S(2)}, u32[]{:S(2)}) %collective-permute-start.13) | collective-permute-done | bytes 1376288 | tf_op jit(solution)/shard_map/ppermute | solution.py:312
  118.3 18.6 %all-to-all-done.refs_1_ = bf16[8,4,264,128]{3,2,1,0:T(8,128)(2,1)S(1)} async-done(((bf16[8,4,264,128]{3,2,1,0:T(8,128)(2,1)}), bf16[8,4,264,128]{3,2,1,0:T(8,128)(2,1)S(1)}, u32[]{:S(2)}, u32[]{:S(2)}) %all-to-all-start) | async-done | bytes 2162720 | tf_op jit(solution)/shard_map/all_to_all | solution.py:373
  138.5 7.9 %collective-permute-done.12.refs_3_.refs_7_ = bf16[1344,512]{1,0:T(8,128)(2,1)} collective-permute-done((bf16[1344,512]{1,0:T(8,128)(2,1)S(1)}, bf16[1344,512]{1,0:T(8,128)(2,1)}, u32[]{:S(2)}, u32[]{:S(2)}) %collective-permute-start.12) | collective-permute-done | bytes 1376288 | tf_op jit(solution)/shard_map/ppermute | solution.py:312
  147.6 2.9 %shard_map.111 = (bf16[384,512]{1,0:T(8,128)(2,1)S(1)}, bf16[384,512]{1,0:T(8,128)(2,1)S(1)}, bf16[384,512]{1,0:T(8,128)(2,1)S(1)}, bf16[384,512]{1,0:T(8,128)(2,1)S(1)}) custom-call(s32[5]{0:T(128)S(1)} %stack.23.refs_0_, bf16[1344,512]{1,0:T(8,128)(2,1)S(1)} %shard_map.108.refs_5_.refs_1_, bf16[1344,512]{1,0:T(8,128)(2,1)} %collective-permute-done.11.refs_2_.refs_6_, ...), custom_call_target="tpu_custom_call" | custom-call | tf_op jit(solution)/shard_map/pallas_call | solution.py:230
  150.4 4.4 %collective-permute-done.15.refs_11_ = bf16[192,512]{1,0:T(8,128)(2,1)} collective-permute-done((bf16[192,512]{1,0:T(8,128)(2,1)}, bf16[192,512]{1,0:T(8,128)(2,1)}, u32[]{:S(2)}, u32[]{:S(2)}) %collective-permute-start.15) | collective-permute-done | bytes 196640 | tf_op jit(solution)/shard_map/ppermute | solution.py:312
  154.9 7.9 %shard_map.112 = (bf16[1152,512]{1,0:T(8,128)(2,1)S(1)}, bf16[1152,512]{1,0:T(8,128)(2,1)}, bf16[1152,512]{1,0:T(8,128)(2,1)}, bf16[1152,512]{1,0:T(8,128)(2,1)}) custom-call(s32[5]{0:T(128)S(1)} %stack.23.refs_0_, bf16[1344,512]{1,0:T(8,128)(2,1)} %copy-done, bf16[1344,512]{1,0:T(8,128)(2,1)} %collective-permute-done.11.refs_2_.refs_6_, ...), custom_call_target="tpu_custom_call" | custom-call | tf_op jit(solution)/shard_map/pallas_call | solution.py:230
  165.9 2.2 collective-permute-start.23
  168.2 30.4 %collective-permute-done.22.refs_2_ = bf16[384,512]{1,0:T(8,128)(2,1)S(1)} collective-permute-done((bf16[384,512]{1,0:T(8,128)(2,1)S(1)}, bf16[384,512]{1,0:T(8,128)(2,1)S(1)}, u32[]{:S(2)}, u32[]{:S(2)}) %collective-permute-start.22) | collective-permute-done | bytes 393248 | tf_op jit(solution)/shard_map/ppermute | solution.py:312
  204.1 2.7 %collective-permute-start.27 = (bf16[384,256]{1,0:T(8,128)(2,1)S(1)}, bf16[384,256]{1,0:T(8,128)(2,1)S(1)}, u32[]{:S(2)}, u32[]{:S(2)}) collective-permute-start(bf16[384,256]{1,0:T(8,128)(2,1)S(1)} %get-tuple-element.75), channel_id=1, source_target_pairs={{0,24},{8,0},{16,8},{24,16},{32,56},{40,32},{48,40},{56,48},{64,88... | collective-permute-start | bytes 589832 | tf_op jit(solution)/shard_map/ppermute | solution.py:312
  206.8 12.4 %collective-permute-done.27.refs_5_ = bf16[384,256]{1,0:T(8,128)(2,1)S(1)} collective-permute-done((bf16[384,256]{1,0:T(8,128)(2,1)S(1)}, bf16[384,256]{1,0:T(8,128)(2,1)S(1)}, u32[]{:S(2)}, u32[]{:S(2)}) %collective-permute-start.27) | collective-permute-done | bytes 196640 | tf_op jit(solution)/shard_map/ppermute | solution.py:312
  219.2 2.2 collective-permute-done.26.refs_4_
  222.1 4.5 %collective-permute-start.34 = (bf16[192,512]{1,0:T(8,128)(2,1)S(1)}, bf16[192,512]{1,0:T(8,128)(2,1)S(1)}, u32[]{:S(2)}, u32[]{:S(2)}) collective-permute-start(bf16[192,512]{1,0:T(8,128)(2,1)S(1)} %get-tuple-element.83), channel_id=1, source_target_pairs={{0,5},{1,4},{2,7},{3,6},{4,1},{5,0},{6,3},{7,2},{8,13},{9,12},{10,... | collective-permute-start | bytes 589832 | tf_op jit(solution)/shard_map/ppermute | solution.py:306
  226.6 2.3 collective-permute-start.33
  232.2 2.1 collective-permute-start.32
  234.3 3.5 %collective-permute-done.33.refs_2_ = bf16[192,512]{1,0:T(8,128)(2,1)S(1)} collective-permute-done((bf16[192,512]{1,0:T(8,128)(2,1)S(1)}, bf16[192,512]{1,0:T(8,128)(2,1)S(1)}, u32[]{:S(2)}, u32[]{:S(2)}) %collective-permute-start.33) | collective-permute-done | bytes 196640 | tf_op jit(solution)/shard_map/ppermute | solution.py:306
  240.7 4.2 %collective-permute-done.31.refs_5_ = bf16[192,512]{1,0:T(8,128)(2,1)S(1)} collective-permute-done((bf16[192,512]{1,0:T(8,128)(2,1)S(1)}, bf16[192,512]{1,0:T(8,128)(2,1)S(1)}, u32[]{:S(2)}, u32[]{:S(2)}) %collective-permute-start.31) | collective-permute-done | bytes 196640 | tf_op jit(solution)/shard_map/ppermute | solution.py:306
  244.9 2.5 shard_map.119
  256.1 3.0 %collective-permute-done.35 = bf16[512,128]{1,0:T(8,128)(2,1)} collective-permute-done((bf16[512,128]{1,0:T(8,128)(2,1)}, bf16[512,128]{1,0:T(8,128)(2,1)}, u32[]{:S(2)}, u32[]{:S(2)}) %collective-permute-start.35) | collective-permute-done | bytes 131104 | tf_op jit(solution)/shard_map/ppermute | solution.py:312
  (101 shorter events, 54.3 us)
Async XLA Ops:
  5.9 28.9 %collective-permute-start = (bf16[2,2,264,128]{3,2,1,0:T(8,128)(2,1)S(1)}, bf16[2,2,264,128]{3,2,1,0:T(8,128)(2,1)S(1)}, u32[]{:S(2)}, u32[]{:S(2)}) collective-permute-start(bf16[2,2,264,128]{3,2,1,0:T(8,128)(2,1)S(1)} %get-tuple-element.48), channel_id=1, source_target_pairs={{0,2},{1,3},{2,4},{3,5},{4,6},{5,7},{6,0},{7,1},{8,10},{9,11},{10,... | collective-permute-start | bytes 811016 | tf_op jit(solution)/shard_map/ppermute | solution.py:306
  8.0 26.8 %collective-permute-start.1 = (bf16[2,2,264,128]{3,2,1,0:T(8,128)(2,1)S(1)}, bf16[2,2,264,128]{3,2,1,0:T(8,128)(2,1)S(1)}, u32[]{:S(2)}, u32[]{:S(2)}) collective-permute-start(bf16[2,2,264,128]{3,2,1,0:T(8,128)(2,1)S(1)} %get-tuple-element.49), channel_id=1, source_target_pairs={{0,4},{1,5},{2,6},{3,7},{4,0},{5,1},{6,2},{7,3},{8,12},{9,13},{10,... | collective-permute-start | bytes 811016 | tf_op jit(solution)/shard_map/ppermute | solution.py:306
  10.5 24.3 %collective-permute-start.2 = (bf16[2,2,264,128]{3,2,1,0:T(8,128)(2,1)S(1)}, bf16[2,2,264,128]{3,2,1,0:T(8,128)(2,1)S(1)}, u32[]{:S(2)}, u32[]{:S(2)}) collective-permute-start(bf16[2,2,264,128]{3,2,1,0:T(8,128)(2,1)S(1)} %get-tuple-element.50), channel_id=1, source_target_pairs={{0,6},{1,7},{2,0},{3,1},{4,2},{5,3},{6,4},{7,5},{8,14},{9,15},{10,... | collective-permute-start | bytes 811016 | tf_op jit(solution)/shard_map/ppermute | solution.py:306
  14.6 10.0 %collective-permute-start.3 = (bf16[512,128]{1,0:T(8,128)(2,1)S(1)}, bf16[512,128]{1,0:T(8,128)(2,1)S(1)}, u32[]{:S(2)}, u32[]{:S(2)}) collective-permute-start(bf16[512,128]{1,0:T(8,128)(2,1)S(1)} %copy-done.10), channel_id=1, source_target_pairs={{0,96},{8,104},{16,112},{24,120},{32,0},{40,8},{48,16},{56,24},{64... | collective-permute-start | bytes 393224 | tf_op jit(solution)/shard_map/ppermute | solution.py:312
  17.0 13.8 %collective-permute-start.5 = (bf16[512,128]{1,0:T(8,128)(2,1)S(1)}, bf16[512,128]{1,0:T(8,128)(2,1)S(1)}, u32[]{:S(2)}, u32[]{:S(2)}) collective-permute-start(bf16[512,128]{1,0:T(8,128)(2,1)S(1)} %copy-done.10), channel_id=1, source_target_pairs={{0,32},{8,40},{16,48},{24,56},{32,64},{40,72},{48,80},{56,88},{64,... | collective-permute-start | bytes 393224 | tf_op jit(solution)/shard_map/ppermute | solution.py:312
  37.2 20.5 %collective-permute-start.7 = (bf16[2,192,512]{2,1,0:T(8,128)(2,1)}, bf16[2,192,512]{2,1,0:T(8,128)(2,1)S(1)}, u32[]{:S(2)}, u32[]{:S(2)}) collective-permute-start(bf16[2,192,512]{2,1,0:T(8,128)(2,1)} %get-tuple-element.53), channel_id=1, source_target_pairs={{0,2},{1,3},{2,4},{3,5},{4,6},{5,7},{6,0},{7,1},{8,10},{9,11},{10,... | collective-permute-start | bytes 1179656 | tf_op jit(solution)/shard_map/ppermute | solution.py:306
  37.5 20.2 %collective-permute-start.8 = (bf16[2,192,512]{2,1,0:T(8,128)(2,1)}, bf16[2,192,512]{2,1,0:T(8,128)(2,1)S(1)}, u32[]{:S(2)}, u32[]{:S(2)}) collective-permute-start(bf16[2,192,512]{2,1,0:T(8,128)(2,1)} %get-tuple-element.54), channel_id=1, source_target_pairs={{0,4},{1,5},{2,6},{3,7},{4,0},{5,1},{6,2},{7,3},{8,12},{9,13},{10,... | collective-permute-start | bytes 1179656 | tf_op jit(solution)/shard_map/ppermute | solution.py:306
  38.4 19.7 %collective-permute-start.9 = (bf16[2,192,512]{2,1,0:T(8,128)(2,1)}, bf16[2,192,512]{2,1,0:T(8,128)(2,1)S(1)}, u32[]{:S(2)}, u32[]{:S(2)}) collective-permute-start(bf16[2,192,512]{2,1,0:T(8,128)(2,1)} %get-tuple-element.55), channel_id=1, source_target_pairs={{0,6},{1,7},{2,0},{3,1},{4,2},{5,3},{6,4},{7,5},{8,14},{9,15},{10,... | collective-permute-start | bytes 1179656 | tf_op jit(solution)/shard_map/ppermute | solution.py:306
  61.2 14.9 %collective-permute-start.18 = (bf16[4,264,128]{2,1,0:T(8,128)(2,1)S(1)}, bf16[4,264,128]{2,1,0:T(8,128)(2,1)S(1)}, u32[]{:S(2)}, u32[]{:S(2)}) collective-permute-start(bf16[4,264,128]{2,1,0:T(8,128)(2,1)S(1)} %get-tuple-element.58), channel_id=1, source_target_pairs={{0,16},{8,24},{16,0},{24,8},{32,48},{40,56},{48,32},{56,40},{64,80... | collective-permute-start | bytes 811016 | tf_op jit(solution)/shard_map/ppermute | solution.py:312
  63.8 12.3 %collective-permute-start.19 = (bf16[4,264,128]{2,1,0:T(8,128)(2,1)S(1)}, bf16[4,264,128]{2,1,0:T(8,128)(2,1)S(1)}, u32[]{:S(2)}, u32[]{:S(2)}) collective-permute-start(bf16[4,264,128]{2,1,0:T(8,128)(2,1)S(1)} %get-tuple-element.59), channel_id=1, source_target_pairs={{0,24},{8,0},{16,8},{24,16},{32,56},{40,32},{48,40},{56,48},{64,88... | collective-permute-start | bytes 811016 | tf_op jit(solution)/shard_map/ppermute | solution.py:312
  78.2 58.7 %all-to-all-start = ((bf16[8,4,264,128]{3,2,1,0:T(8,128)(2,1)}), bf16[8,4,264,128]{3,2,1,0:T(8,128)(2,1)S(1)}, u32[]{:S(2)}, u32[]{:S(2)}) async-start(bf16[8,4,264,128]{3,2,1,0:T(8,128)(2,1)} %shard_map.109), calls=%async_computation | async-start | bytes 4325376 | tf_op jit(solution)/shard_map/all_to_all | solution.py:373
  83.9 31.7 %collective-permute-start.13 = (bf16[1344,512]{1,0:T(8,128)(2,1)S(1)}, bf16[1344,512]{1,0:T(8,128)(2,1)S(1)}, u32[]{:S(2)}, u32[]{:S(2)}) collective-permute-start(bf16[1344,512]{1,0:T(8,128)(2,1)S(1)} %shard_map.108.refs_5_.refs_1_), channel_id=1, source_target_pairs={{0,8},{8,16},{16,24},{24,0},{32,40},{40,48},{48,56},{56,32},{64,72... | collective-permute-start | bytes 4128776 | tf_op jit(solution)/shard_map/ppermute | solution.py:312
  84.4 62.0 %collective-permute-start.12 = (bf16[1344,512]{1,0:T(8,128)(2,1)S(1)}, bf16[1344,512]{1,0:T(8,128)(2,1)}, u32[]{:S(2)}, u32[]{:S(2)}) collective-permute-start(bf16[1344,512]{1,0:T(8,128)(2,1)S(1)} %shard_map.108.refs_5_.refs_1_), channel_id=1, source_target_pairs={{0,16},{8,24},{16,0},{24,8},{32,48},{40,56},{48,32},{56,40},{64,80... | collective-permute-start | bytes 4128776 | tf_op jit(solution)/shard_map/ppermute | solution.py:312
  87.3 60.3 %collective-permute-start.11 = (bf16[1344,512]{1,0:T(8,128)(2,1)S(1)}, bf16[1344,512]{1,0:T(8,128)(2,1)}, u32[]{:S(2)}, u32[]{:S(2)}) collective-permute-start(bf16[1344,512]{1,0:T(8,128)(2,1)S(1)} %shard_map.108.refs_5_.refs_1_), channel_id=1, source_target_pairs={{0,24},{8,0},{16,8},{24,16},{32,56},{40,32},{48,40},{56,48},{64,88... | collective-permute-start | bytes 4128776 | tf_op jit(solution)/shard_map/ppermute | solution.py:312
  87.9 62.5 %collective-permute-start.16 = (bf16[192,512]{1,0:T(8,128)(2,1)}, bf16[192,512]{1,0:T(8,128)(2,1)}, u32[]{:S(2)}, u32[]{:S(2)}) collective-permute-start(bf16[192,512]{1,0:T(8,128)(2,1)} %copy-done.8), channel_id=1, source_target_pairs={{0,8},{8,16},{16,24},{24,0},{32,40},{40,48},{48,56},{56,32},{64,72... | collective-permute-start | bytes 589832 | tf_op jit(solution)/shard_map/ppermute | solution.py:312
  88.7 66.1 %collective-permute-start.15 = (bf16[192,512]{1,0:T(8,128)(2,1)}, bf16[192,512]{1,0:T(8,128)(2,1)}, u32[]{:S(2)}, u32[]{:S(2)}) collective-permute-start(bf16[192,512]{1,0:T(8,128)(2,1)} %copy-done.8), channel_id=1, source_target_pairs={{0,16},{8,24},{16,0},{24,8},{32,48},{40,56},{48,32},{56,40},{64,80... | collective-permute-start | bytes 589832 | tf_op jit(solution)/shard_map/ppermute | solution.py:312
  116.7 38.2 %collective-permute-start.14 = (bf16[192,512]{1,0:T(8,128)(2,1)}, bf16[192,512]{1,0:T(8,128)(2,1)}, u32[]{:S(2)}, u32[]{:S(2)}) collective-permute-start(bf16[192,512]{1,0:T(8,128)(2,1)} %copy-done.8), channel_id=1, source_target_pairs={{0,24},{8,0},{16,8},{24,16},{32,56},{40,32},{48,40},{56,48},{64,88... | collective-permute-start | bytes 589832 | tf_op jit(solution)/shard_map/ppermute | solution.py:312
  162.8 38.7 %collective-permute-start.20 = (bf16[1152,512]{1,0:T(8,128)(2,1)}, bf16[1152,512]{1,0:T(8,128)(2,1)S(1)}, u32[]{:S(2)}, u32[]{:S(2)}) collective-permute-start(bf16[1152,512]{1,0:T(8,128)(2,1)} %get-tuple-element.65), channel_id=1, source_target_pairs={{0,8},{8,16},{16,24},{24,0},{32,40},{40,48},{48,56},{56,32},{64,72... | collective-permute-start | bytes 3538952 | tf_op jit(solution)/shard_map/ppermute | solution.py:312
  164.5 37.0 %collective-permute-start.21 = (bf16[1152,512]{1,0:T(8,128)(2,1)}, bf16[1152,512]{1,0:T(8,128)(2,1)S(1)}, u32[]{:S(2)}, u32[]{:S(2)}) collective-permute-start(bf16[1152,512]{1,0:T(8,128)(2,1)} %get-tuple-element.66), channel_id=1, source_target_pairs={{0,24},{8,0},{16,8},{24,16},{32,56},{40,32},{48,40},{56,48},{64,88... | collective-permute-start | bytes 3538952 | tf_op jit(solution)/shard_map/ppermute | solution.py:312
  165.5 33.1 %collective-permute-start.22 = (bf16[384,512]{1,0:T(8,128)(2,1)S(1)}, bf16[384,512]{1,0:T(8,128)(2,1)S(1)}, u32[]{:S(2)}, u32[]{:S(2)}) collective-permute-start(bf16[384,512]{1,0:T(8,128)(2,1)S(1)} %get-tuple-element.69), channel_id=1, source_target_pairs={{0,8},{8,16},{16,24},{24,0},{32,40},{40,48},{48,56},{56,32},{64,72... | collective-permute-start | bytes 1179656 | tf_op jit(solution)/shard_map/ppermute | solution.py:312
  165.9 33.3 %collective-permute-start.23 = (bf16[384,512]{1,0:T(8,128)(2,1)S(1)}, bf16[384,512]{1,0:T(8,128)(2,1)S(1)}, u32[]{:S(2)}, u32[]{:S(2)}) collective-permute-start(bf16[384,512]{1,0:T(8,128)(2,1)S(1)} %get-tuple-element.70), channel_id=1, source_target_pairs={{0,24},{8,0},{16,8},{24,16},{32,56},{40,32},{48,40},{56,48},{64,88... | collective-permute-start | bytes 1179656 | tf_op jit(solution)/shard_map/ppermute | solution.py:312
  202.3 26.7 %collective-permute-start.25 = (bf16[1152,256]{1,0:T(8,128)(2,1)S(1)}, bf16[1152,256]{1,0:T(8,128)(2,1)S(1)}, u32[]{:S(2)}, u32[]{:S(2)}) collective-permute-start(bf16[1152,256]{1,0:T(8,128)(2,1)S(1)} %get-tuple-element.74), channel_id=1, source_target_pairs={{0,24},{8,0},{16,8},{24,16},{32,56},{40,32},{48,40},{56,48},{64,88... | collective-permute-start | bytes 1769480 | tf_op jit(solution)/shard_map/ppermute | solution.py:312
  204.1 24.8 %collective-permute-start.24 = (bf16[1152,256]{1,0:T(8,128)(2,1)S(1)}, bf16[1152,256]{1,0:T(8,128)(2,1)S(1)}, u32[]{:S(2)}, u32[]{:S(2)}) collective-permute-start(bf16[1152,256]{1,0:T(8,128)(2,1)S(1)} %get-tuple-element.73.refs_6_), channel_id=1, source_target_pairs={{0,8},{8,16},{16,24},{24,0},{32,40},{40,48},{48,56},{56,32},{64,72... | collective-permute-start | bytes 1769480 | tf_op jit(solution)/shard_map/ppermute | solution.py:312
  204.1 15.0 %collective-permute-start.27 = (bf16[384,256]{1,0:T(8,128)(2,1)S(1)}, bf16[384,256]{1,0:T(8,128)(2,1)S(1)}, u32[]{:S(2)}, u32[]{:S(2)}) collective-permute-start(bf16[384,256]{1,0:T(8,128)(2,1)S(1)} %get-tuple-element.75), channel_id=1, source_target_pairs={{0,24},{8,0},{16,8},{24,16},{32,56},{40,32},{48,40},{56,48},{64,88... | collective-permute-start | bytes 589832 | tf_op jit(solution)/shard_map/ppermute | solution.py:312
  206.8 14.6 %collective-permute-start.26 = (bf16[384,256]{1,0:T(8,128)(2,1)S(1)}, bf16[384,256]{1,0:T(8,128)(2,1)S(1)}, u32[]{:S(2)}, u32[]{:S(2)}) collective-permute-start(bf16[384,256]{1,0:T(8,128)(2,1)S(1)} %get-tuple-element.71.refs_4_), channel_id=1, source_target_pairs={{0,8},{8,16},{16,24},{24,0},{32,40},{40,48},{48,56},{56,32},{64,72... | collective-permute-start | bytes 589832 | tf_op jit(solution)/shard_map/ppermute | solution.py:312
  222.1 10.1 %collective-permute-start.34 = (bf16[192,512]{1,0:T(8,128)(2,1)S(1)}, bf16[192,512]{1,0:T(8,128)(2,1)S(1)}, u32[]{:S(2)}, u32[]{:S(2)}) collective-permute-start(bf16[192,512]{1,0:T(8,128)(2,1)S(1)} %get-tuple-element.83), channel_id=1, source_target_pairs={{0,5},{1,4},{2,7},{3,6},{4,1},{5,0},{6,3},{7,2},{8,13},{9,12},{10,... | collective-permute-start | bytes 589832 | tf_op jit(solution)/shard_map/ppermute | solution.py:306
  226.6 11.2 %collective-permute-start.33 = (bf16[192,512]{1,0:T(8,128)(2,1)S(1)}, bf16[192,512]{1,0:T(8,128)(2,1)S(1)}, u32[]{:S(2)}, u32[]{:S(2)}) collective-permute-start(bf16[192,512]{1,0:T(8,128)(2,1)S(1)} %get-tuple-element.76.refs_6_), channel_id=1, source_target_pairs={{0,4},{1,5},{2,6},{3,7},{4,0},{5,1},{6,2},{7,3},{8,12},{9,13},{10,... | collective-permute-start | bytes 589832 | tf_op jit(solution)/shard_map/ppermute | solution.py:306
  229.9 10.8 %collective-permute-start.29 = (bf16[192,512]{1,0:T(8,128)(2,1)S(1)}, bf16[192,512]{1,0:T(8,128)(2,1)S(1)}, u32[]{:S(2)}, u32[]{:S(2)}) collective-permute-start(bf16[192,512]{1,0:T(8,128)(2,1)S(1)} %get-tuple-element.78), channel_id=1, source_target_pairs={{0,3},{1,2},{2,5},{3,4},{4,7},{5,6},{6,1},{7,0},{8,11},{9,10},{10,... | collective-permute-start | bytes 589832 | tf_op jit(solution)/shard_map/ppermute | solution.py:306
  230.1 10.6 %collective-permute-start.30 = (bf16[192,512]{1,0:T(8,128)(2,1)S(1)}, bf16[192,512]{1,0:T(8,128)(2,1)S(1)}, u32[]{:S(2)}, u32[]{:S(2)}) collective-permute-start(bf16[192,512]{1,0:T(8,128)(2,1)S(1)} %get-tuple-element.79), channel_id=1, source_target_pairs={{0,6},{1,7},{2,0},{3,1},{4,2},{5,3},{6,4},{7,5},{8,14},{9,15},{10,... | collective-permute-start | bytes 589832 | tf_op jit(solution)/shard_map/ppermute | solution.py:306
  232.2 12.7 %collective-permute-start.31 = (bf16[192,512]{1,0:T(8,128)(2,1)S(1)}, bf16[192,512]{1,0:T(8,128)(2,1)S(1)}, u32[]{:S(2)}, u32[]{:S(2)}) collective-permute-start(bf16[192,512]{1,0:T(8,128)(2,1)S(1)} %get-tuple-element.80), channel_id=1, source_target_pairs={{0,2},{1,3},{2,4},{3,5},{4,6},{5,7},{6,0},{7,1},{8,10},{9,11},{10,... | collective-permute-start | bytes 589832 | tf_op jit(solution)/shard_map/ppermute | solution.py:306
  232.2 12.7 %collective-permute-start.32 = (bf16[192,512]{1,0:T(8,128)(2,1)S(1)}, bf16[192,512]{1,0:T(8,128)(2,1)S(1)}, u32[]{:S(2)}, u32[]{:S(2)}) collective-permute-start(bf16[192,512]{1,0:T(8,128)(2,1)S(1)} %get-tuple-element.81), channel_id=1, source_target_pairs={{0,1},{1,0},{2,3},{3,2},{4,5},{5,4},{6,7},{7,6},{8,9},{9,8},{10,11... | collective-permute-start | bytes 589832 | tf_op jit(solution)/shard_map/ppermute | solution.py:306
  247.4 11.7 %collective-permute-start.35 = (bf16[512,128]{1,0:T(8,128)(2,1)}, bf16[512,128]{1,0:T(8,128)(2,1)}, u32[]{:S(2)}, u32[]{:S(2)}) collective-permute-start(bf16[512,128]{1,0:T(8,128)(2,1)} %get-tuple-element.85), channel_id=1, source_target_pairs={{0,64},{8,72},{16,80},{24,88},{32,96},{40,104},{48,112},{56,120},{... | collective-permute-start | bytes 393224 | tf_op jit(solution)/shard_map/ppermute | solution.py:312
  (22 other events, 242.9 us)
